TPU v7x, 512 devices: a whole 4x4x16 slice. The times are simulated.
512 devices in a mesh: tp: 16 (over y, x), dp: 32 (over z, core).
Axes of the slice: x: 4, y: 4, z: 16, core: 2. Of those that a mesh axis runs over, the one named last changes fastest.
Arguments:
- stream: bfloat16 [64, 4096], P('tp', 'dp'), may hold values from -48 to 48
- norm_gain: float32 [2, 4096], P(None, 'dp'), may hold values from 0.1 to 1.9
- x_weight: bfloat16 [2, 4096, 8192], P(None, 'dp', 'tp'), may hold values from -0.09375 to 0.09375
- z_weight: bfloat16 [2, 4096, 8192], P(None, 'dp', 'tp'), may hold values from -0.09375 to 0.09375
- bc_weight: bfloat16 [2, 4096, 2, 2048], P(None, 'dp', None, 'tp'), may hold values from -0.09375 to 0.09375
- step_weight: bfloat16 [2, 4096, 128], P(None, 'dp'), may hold values from -0.09375 to 0.09375
- conv_x_weight: bfloat16 [2, 5, 8192], P(None, None, 'tp'), may hold values from -2.5 to 2.5
- conv_bc_weight: bfloat16 [2, 5, 2, 2048], P(None, None, None, 'tp'), may hold values from -2.5 to 2.5
- step_bias: float32 [2, 128], P(None, 'tp'), may hold values from -4 to 0.5
- decay_log: float32 [2, 128], P(None, 'tp'), may hold values from 0 to 2.8
- skip_gain: float32 [2, 128], P(None, 'tp'), may hold values from 0.1 to 1.9
- group_gain: float32 [2, 8192], P(None, 'tp'), may hold values from 0.1 to 1.9
- out_weight: bfloat16 [2, 8192, 4096], P(None, 'tp', 'dp'), may hold values from -0.0625 to 0.0625
- scan_state: float32 [2, 64, 128, 64, 128], P(None, 'dp', 'tp'), may hold values from -1.2 to 1.2
- conv_x_state: bfloat16 [2, 64, 4, 8192], P(None, 'dp', None, 'tp'), may hold values from -6 to 6
- conv_bc_state: bfloat16 [2, 64, 4, 2, 2048], P(None, 'dp', None, None, 'tp'), may hold values from -6 to 6
Outputs:
- stream_out: bfloat16 [64, 4096], P('tp', 'dp')
- scan_state_out: float32 [2, 64, 128, 64, 128], P(None, 'dp', 'tp')
- conv_x_out: bfloat16 [2, 64, 4, 8192], P(None, 'dp', None, 'tp')
- conv_bc_out: bfloat16 [2, 64, 4, 2, 2048], P(None, 'dp', None, None, 'tp')
All inputs are finite; a program needn't handle non-finite values.
Results may differ from a plain program's by a relative error of at most 0.04.
Values may be sent and summed in bfloat16 or wider, within the bound.
No kernel may reach another device: no remote copies, remote signals or barrier semaphores. Data moves between devices by JAX's collectives and lax.ppermute only.
A program may use at most 64 MiB of HBM per device.

v0:
```python
import math

import jax
import jax.numpy as jnp
from jax import lax
from jax.sharding import PartitionSpec as P

MODEL_WIDTH = 4096
HEAD_COUNT = 128
HEAD_DIM = 64
STATE_DIM = 128
GROUPS = 16
LAYERS = 2


EPS = 1e-06


def joined_along(tiles, dim):
    tiles = jnp.moveaxis(tiles, 0, dim)
    dims = tiles.shape
    return tiles.reshape(*dims[:dim], dims[dim] * dims[dim + 1], *dims[dim + 2 :])


def sent_to_all(value, axis):
    copies = jnp.broadcast_to(value, (lax.axis_size(axis), *value.shape))
    return lax.all_to_all(copies, axis, split_axis=0, concat_axis=0, tiled=True)


def gather_directly(value, axis, dim):
    return joined_along(sent_to_all(value, axis), dim)


def cut_along(value, dim, count):
    before, after = (value.shape[:dim], value.shape[dim + 1 :])
    return jnp.moveaxis(value.reshape(*before, count, -1, *after), dim, 0)


def sent_and_summed(value, axis, dim):
    tiles = cut_along(value, dim, lax.axis_size(axis))
    arrived = lax.all_to_all(tiles, axis, split_axis=0, concat_axis=0, tiled=True)
    return arrived.astype(jnp.float32).sum(axis=0)


def side_by_side(arrays, axis, dim, along):
    widths = [math.prod(a.shape[along:]) for a in arrays]
    both = jnp.concatenate(
        [a.reshape(*a.shape[:along], w) for a, w in zip(arrays, widths)], axis=along
    )
    filled = sent_and_summed(both, axis, dim)
    tiles = jnp.split(filled, [sum(widths[:k]) for k in range(1, len(widths))], axis=along)
    return tuple(
        (b.reshape(*filled.shape[:along], *a.shape[along:]) for a, b in zip(arrays, tiles))
    )


def taken_together(value, axis):
    everything = sent_to_all(value, axis)
    return jnp.sum(everything.astype(jnp.float32), axis=0)


def shards(
    stream,
    norm_gain,
    x_weight,
    z_weight,
    bc_weight,
    step_weight,
    conv_x_weight,
    conv_bc_weight,
    step_bias,
    decay_log,
    skip_gain,
    group_gain,
    out_weight,
    scan_state,
    conv_x_state,
    conv_bc_state,
):
    tp_index = lax.axis_index("tp")
    seq_count = scan_state.shape[1]
    heads_dev = scan_state.shape[2]
    groups_dev = conv_bc_state.shape[4] // STATE_DIM
    per_group = HEAD_COUNT // GROUPS
    weight_rows = x_weight.shape[1]
    whole = None
    states_list = []
    xconv_list = []
    bcconv_list = []
    for block_index in range(LAYERS):
        if whole is None:
            whole = gather_directly(stream, "tp", 0)
        widened = whole.astype(jnp.float32)
        normed_in = (widened * norm_gain[block_index]).astype(jnp.bfloat16)
        part_sq = jnp.sum(widened * widened, axis=1)
        step_cols = lax.dynamic_slice_in_dim(
            step_weight[block_index], tp_index * heads_dev, heads_dev, 1
        )
        part_x = jnp.dot(normed_in, x_weight[block_index], preferred_element_type=jnp.float32)
        part_z = jnp.dot(normed_in, z_weight[block_index], preferred_element_type=jnp.float32)
        part_bc = jnp.dot(
            normed_in,
            bc_weight[block_index].reshape(weight_rows, -1),
            preferred_element_type=jnp.float32,
        )
        part_step = jnp.dot(normed_in, step_cols, preferred_element_type=jnp.float32)
        got_x, got_z, got_bc, got_step, got_sq = side_by_side(
            (
                part_x.astype(jnp.bfloat16),
                part_z.astype(jnp.bfloat16),
                part_bc.astype(jnp.bfloat16),
                part_step.astype(jnp.bfloat16),
                part_sq.astype(jnp.bfloat16),
            ),
            "dp",
            0,
            1,
        )
        inv_rms = lax.rsqrt(got_sq / MODEL_WIDTH + EPS)[:, None]
        proj_x = (got_x * inv_rms).astype(jnp.bfloat16)
        proj_z = (got_z * inv_rms).astype(jnp.bfloat16)
        proj_bc = (got_bc * inv_rms).astype(jnp.bfloat16).reshape(seq_count, 2, -1)
        step_raw = got_step * inv_rms
        window_x = jnp.concatenate([conv_x_state[block_index], proj_x[:, None, :]], axis=1)
        inputs_x = jax.nn.silu(
            jnp.sum(
                window_x.astype(jnp.float32) * conv_x_weight[block_index].astype(jnp.float32),
                axis=1,
            )
        )
        window_bc = jnp.concatenate([conv_bc_state[block_index], proj_bc[:, None]], axis=1)
        inputs_bc = jax.nn.silu(
            jnp.sum(
                window_bc.astype(jnp.float32) * conv_bc_weight[block_index].astype(jnp.float32),
                axis=1,
            )
        )
        b_part = inputs_bc[:, 0].reshape(seq_count, groups_dev, STATE_DIM)
        c_part = inputs_bc[:, 1].reshape(seq_count, groups_dev, STATE_DIM)
        step_size = jax.nn.softplus(step_raw + step_bias[block_index])
        decay_rate = jnp.exp(-step_size * jnp.exp(decay_log[block_index]))
        heads_x = inputs_x.reshape(seq_count, groups_dev, per_group, HEAD_DIM)
        step_heads = step_size.reshape(seq_count, groups_dev, per_group)
        decay_heads = decay_rate.reshape(seq_count, groups_dev, per_group)
        old_state = scan_state[block_index].reshape(
            seq_count, groups_dev, per_group, HEAD_DIM, STATE_DIM
        )
        state_new = (
            old_state * decay_heads[..., None, None]
            + (step_heads[..., None] * heads_x)[..., None] * b_part[:, :, None, None, :]
        )
        readout = jnp.einsum("sgepn,sgn->sgep", state_new, c_part)
        readout = (
            readout
            + skip_gain[block_index].reshape(groups_dev, per_group)[None, :, :, None] * heads_x
        )
        gated_out = readout.reshape(seq_count, -1) * jax.nn.silu(proj_z.astype(jnp.float32))
        grouped = gated_out.reshape(seq_count, groups_dev, -1)
        normed = grouped * lax.rsqrt(jnp.mean(grouped * grouped, axis=2, keepdims=True) + EPS)
        mixed_rows = (normed.reshape(seq_count, -1) * group_gain[block_index]).astype(jnp.bfloat16)
        out_block = out_weight[block_index]
        terms = jnp.dot(
            gather_directly(mixed_rows, "dp", 0), out_block, preferred_element_type=jnp.float32
        )
        summed = taken_together(terms.astype(jnp.bfloat16), "tp").astype(jnp.float32)
        whole = (widened + summed).astype(jnp.bfloat16)
        states_list.append(state_new.reshape(seq_count, heads_dev, HEAD_DIM, STATE_DIM))
        xconv_list.append(window_x[:, 1:])
        bcconv_list.append(window_bc[:, 1:])
    row_share = stream.shape[0]
    result = lax.dynamic_slice_in_dim(whole, tp_index * row_share, row_share, 0)
    return (result, jnp.stack(states_list), jnp.stack(xconv_list), jnp.stack(bcconv_list))


def solution(mesh):
    in_specs = (
        P("tp", "dp"),
        P(None, "dp"),
        P(None, "dp", "tp"),
        P(None, "dp", "tp"),
        P(None, "dp", None, "tp"),
        P(None, "dp", None),
        P(None, None, "tp"),
        P(None, None, None, "tp"),
        P(None, "tp"),
        P(None, "tp"),
        P(None, "tp"),
        P(None, "tp"),
        P(None, "tp", "dp"),
        P(None, "dp", "tp", None, None),
        P(None, "dp", None, "tp"),
        P(None, "dp", None, None, "tp"),
    )
    out_specs = (
        P("tp", "dp"),
        P(None, "dp", "tp", None, None),
        P(None, "dp", None, "tp"),
        P(None, "dp", None, None, "tp"),
    )
    return jax.shard_map(shards, mesh=mesh, in_specs=in_specs, out_specs=out_specs, check_vma=False)
```

profile of v0, /device:TPU:1, one launch (start us, length us, event | category | flops | bytes accessed | tf_op | source)
XLA Modules:
  0.0 143.8 jit_solution(13090432936949763409)
XLA Ops:
  0.7 1.3 broadcast_in_dim.14
  2.0 7.6 %all-to-all-start = ((bf16[16,4,128]{2,1,0:T(4,128)(2,1)}), bf16[16,4,128]{2,1,0:T(4,128)(2,1)S(1)}, u32[]{:S(2)}, u32[]{:S(2)}) async-start(bf16[16,4,128]{2,1,0:T(4,128)(2,1)} %broadcast_in_dim.14), calls=%async_computation | async-start | bytes 32768 | tf_op jit(solution)/shard_map/all_to_all | solution.py:27
  9.6 0.8 fusion.79
  10.3 0.7 slice_bitcast_fusion.2
  11.0 0.7 bitcast_convert_fusion.1
  11.8 0.7 slice_bitcast_fusion
  12.7 0.5 copy-done.9
  13.3 2.7 %all-to-all-done = bf16[16,4,128]{2,1,0:T(4,128)(2,1)S(1)} async-done(((bf16[16,4,128]{2,1,0:T(4,128)(2,1)}), bf16[16,4,128]{2,1,0:T(4,128)(2,1)S(1)}, u32[]{:S(2)}, u32[]{:S(2)}) %all-to-all-start) | async-done | bytes 16416 | tf_op jit(solution)/shard_map/all_to_all | solution.py:27
  16.0 0.1 multiply_reduce_fusion.2
  16.2 0.1 convolution_convert_fusion.2
  16.4 0.1 convolution_convert_fusion.3
  16.6 0.2 convolution_convert_fusion.9
  16.8 0.1 copy.48
  16.9 0.1 convolution_convert_fusion.5
  17.1 1.1 concatenate.40
  18.2 17.5 %all-to-all-start.1 = ((bf16[32,2,1289]{2,1,0:T(2,128)(2,1)}), bf16[32,2,1289]{2,1,0:T(2,128)(2,1)S(1)}, u32[]{:S(2)}, u32[]{:S(2)}) async-start(bf16[32,2,1289]{2,1,0:T(2,128)(2,1)} %concatenate.40), calls=%async_computation.1 | async-start | bytes 360448 | tf_op jit(solution)/shard_map/all_to_all | solution.py:41
  35.7 17.8 %all-to-all-done.1 = bf16[32,2,1289]{2,1,0:T(2,128)(2,1)S(1)} async-done(((bf16[32,2,1289]{2,1,0:T(2,128)(2,1)}), bf16[32,2,1289]{2,1,0:T(2,128)(2,1)S(1)}, u32[]{:S(2)}, u32[]{:S(2)}) %all-to-all-start.1) | async-done | bytes 165024 | tf_op jit(solution)/shard_map/all_to_all | solution.py:41
  53.5 0.2 convert_reduce_fusion.3
  53.7 0.2 fusion.72
  54.4 0.4 fusion.4
  54.9 0.2 multiply_reduce_fusion.6
  55.3 17.3 %all_to_all.35 = bf16[32,2,512]{2,1,0:T(2,128)(2,1)S(1)} all-to-all(bf16[32,2,512]{2,1,0:T(2,128)(2,1)S(1)} %broadcast_in_dim.16), channel_id=1, replica_groups=mesh['tp'=16,'dp'=32] {'dp'}, dimensions={0} | all-to-all | bytes 131072 | tf_op jit(solution)/shard_map/all_to_all | solution.py:27
  72.6 0.2 convolution_convert_fusion.7
  72.9 10.9 %all_to_all.36 = bf16[16,64,128]{2,1,0:T(8,128)(2,1)S(1)} all-to-all(bf16[16,64,128]{2,1,0:T(8,128)(2,1)S(1)} %broadcast_in_dim.17), channel_id=1, replica_groups=mesh['tp'=16,'dp'=32] {'tp'}, dimensions={0} | all-to-all | bytes 524288 | tf_op jit(solution)/shard_map/all_to_all | solution.py:27
  83.8 0.1 fusion.33
  83.9 0.1 convolution_convert_fusion
  84.1 0.1 convolution_convert_fusion.1
  84.2 0.1 convolution_convert_fusion.4
  84.4 0.2 convolution_convert_fusion.8
  84.9 1.1 concatenate.47
  86.0 6.6 %all-to-all-start.4 = ((bf16[32,2,1289]{2,1,0:T(2,128)(2,1)}), bf16[32,2,1289]{2,1,0:T(2,128)(2,1)S(1)}, u32[]{:S(2)}, u32[]{:S(2)}) async-start(bf16[32,2,1289]{2,1,0:T(2,128)(2,1)} %concatenate.47), calls=%async_computation.4 | async-start | bytes 360448 | tf_op jit(solution)/shard_map/all_to_all | solution.py:41
  92.6 17.9 %all-to-all-done.4 = bf16[32,2,1289]{2,1,0:T(2,128)(2,1)S(1)} async-done(((bf16[32,2,1289]{2,1,0:T(2,128)(2,1)}), bf16[32,2,1289]{2,1,0:T(2,128)(2,1)S(1)}, u32[]{:S(2)}, u32[]{:S(2)}) %all-to-all-start.4) | async-done | bytes 165024 | tf_op jit(solution)/shard_map/all_to_all | solution.py:41
  110.6 0.2 convert_reduce_fusion.2
  110.7 0.2 fusion.73
  111.5 0.4 fusion.1
  112.0 0.2 multiply_reduce_fusion.5
  112.3 0.7 broadcast_in_dim.38
  113.0 5.1 %all-to-all-start.5 = ((bf16[32,2,512]{2,1,0:T(2,128)(2,1)}), bf16[32,2,512]{2,1,0:T(2,128)(2,1)S(1)}, u32[]{:S(2)}, u32[]{:S(2)}) async-start(bf16[32,2,512]{2,1,0:T(2,128)(2,1)} %broadcast_in_dim.38), calls=%async_computation.5 | async-start | bytes 131072 | tf_op jit(solution)/shard_map/all_to_all | solution.py:27
  118.1 0.6 pad_maximum_fusion.3
  118.8 0.4 multiply_add_fusion.1
  119.2 12.0 %all-to-all-done.5 = bf16[32,2,512]{2,1,0:T(2,128)(2,1)S(1)} async-done(((bf16[32,2,512]{2,1,0:T(2,128)(2,1)}), bf16[32,2,512]{2,1,0:T(2,128)(2,1)S(1)}, u32[]{:S(2)}, u32[]{:S(2)}) %all-to-all-start.5) | async-done | bytes 65568 | tf_op jit(solution)/shard_map/all_to_all | solution.py:27
  131.2 0.2 convolution_convert_fusion.6
  131.3 0.7 broadcast_in_dim.39
  132.1 3.5 %all-to-all-start.6 = ((bf16[16,64,128]{2,1,0:T(8,128)(2,1)}), bf16[16,64,128]{2,1,0:T(8,128)(2,1)S(1)}, u32[]{:S(2)}, u32[]{:S(2)}) async-start(bf16[16,64,128]{2,1,0:T(8,128)(2,1)} %broadcast_in_dim.39), calls=%async_computation.6 | async-start | bytes 524288 | tf_op jit(solution)/shard_map/all_to_all | solution.py:27
  135.6 0.6 pad_maximum_fusion.4
  136.2 1.0 pad_maximum_fusion
  137.3 5.9 %all-to-all-done.6 = bf16[16,64,128]{2,1,0:T(8,128)(2,1)S(1)} async-done(((bf16[16,64,128]{2,1,0:T(8,128)(2,1)}), bf16[16,64,128]{2,1,0:T(8,128)(2,1)S(1)}, u32[]{:S(2)}, u32[]{:S(2)}) %all-to-all-start.6) | async-done | bytes 262176 | tf_op jit(solution)/shard_map/all_to_all | solution.py:27
  143.3 0.6 fusion.58
  (78 shorter events, 2.4 us)
Async XLA Ops:
  0.6 11.9 %copy-start.5 = (bf16[2,128,128]{2,1,0:T(8,128)(2,1)S(1)}, bf16[2,128,128]{2,1,0:T(8,128)(2,1)}, u32[]{:S(2)}) copy-start(bf16[2,128,128]{2,1,0:T(8,128)(2,1)} %param.21) | copy-start | bytes 196612
  0.6 11.9 %copy-start.4 = (bf16[2,128,2,128]{3,2,1,0:T(2,128)(2,1)S(1)}, bf16[2,128,2,128]{3,2,1,0:T(2,128)(2,1)}, u32[]{:S(2)}) copy-start(bf16[2,128,2,128]{3,2,1,0:T(2,128)(2,1)} %param.20) | copy-start | bytes 393220
  2.0 14.0 %all-to-all-start = ((bf16[16,4,128]{2,1,0:T(4,128)(2,1)}), bf16[16,4,128]{2,1,0:T(4,128)(2,1)S(1)}, u32[]{:S(2)}, u32[]{:S(2)}) async-start(bf16[16,4,128]{2,1,0:T(4,128)(2,1)} %broadcast_in_dim.14), calls=%async_computation | async-start | bytes 32768 | tf_op jit(solution)/shard_map/all_to_all | solution.py:27
  11.0 5.1 %copy-start.1 = (bf16[2,128,512]{2,1,0:T(8,128)(2,1)S(1)}, bf16[2,128,512]{2,1,0:T(8,128)(2,1)}, u32[]{:S(2)}) copy-start(bf16[2,128,512]{2,1,0:T(8,128)(2,1)} %param.19) | copy-start | bytes 786436
  12.5 0.7 copy-start.9
  12.6 0.7 copy-start.10
  12.6 0.7 copy-start.7
  13.2 3.1 %copy-start.2 = (bf16[2,128,512]{2,1,0:T(8,128)(2,1)S(1)}, bf16[2,128,512]{2,1,0:T(8,128)(2,1)}, u32[]{:S(2)}) copy-start(bf16[2,128,512]{2,1,0:T(8,128)(2,1)} %param.18) | copy-start | bytes 786436
  16.2 38.2 %copy-start = (f32[2,2,8,64,128]{4,3,2,1,0:T(8,128)S(1)}, f32[2,2,8,64,128]{4,3,2,1,0:T(8,128)}, u32[]{:S(2)}) copy-start(f32[2,2,8,64,128]{4,3,2,1,0:T(8,128)} %param.29) | copy-start | bytes 3145732
  18.2 17.5 %copy-start.8 = (f32[2,8]{1,0:T(2,128)S(1)}, f32[2,8]{1,0:T(2,128)}, u32[]{:S(2)}) copy-start(f32[2,8]{1,0:T(2,128)} %param.26) | copy-start | bytes 196
  18.2 17.5 %copy-start.6 = (bf16[2,5,512]{2,0,1:T(2,128)(2,1)S(1)}, bf16[2,5,512]{2,0,1:T(2,128)(2,1)}, u32[]{:S(2)}) copy-start(bf16[2,5,512]{2,0,1:T(2,128)(2,1)} %param.22) | copy-start | bytes 30724
  18.2 35.3 %all-to-all-start.1 = ((bf16[32,2,1289]{2,1,0:T(2,128)(2,1)}), bf16[32,2,1289]{2,1,0:T(2,128)(2,1)S(1)}, u32[]{:S(2)}, u32[]{:S(2)}) async-start(bf16[32,2,1289]{2,1,0:T(2,128)(2,1)} %concatenate.40), calls=%async_computation.1 | async-start | bytes 360448 | tf_op jit(solution)/shard_map/all_to_all | solution.py:41
  54.8 17.9 %copy-start.3 = (bf16[2,512,128]{2,1,0:T(8,128)(2,1)S(1)}, bf16[2,512,128]{2,1,0:T(8,128)(2,1)}, u32[]{:S(2)}) copy-start(bf16[2,512,128]{2,1,0:T(8,128)(2,1)} %param.28) | copy-start | bytes 786436
  86.0 24.6 %all-to-all-start.4 = ((bf16[32,2,1289]{2,1,0:T(2,128)(2,1)}), bf16[32,2,1289]{2,1,0:T(2,128)(2,1)S(1)}, u32[]{:S(2)}, u32[]{:S(2)}) async-start(bf16[32,2,1289]{2,1,0:T(2,128)(2,1)} %concatenate.47), calls=%async_computation.4 | async-start | bytes 360448 | tf_op jit(solution)/shard_map/all_to_all | solution.py:41
  113.0 18.2 %all-to-all-start.5 = ((bf16[32,2,512]{2,1,0:T(2,128)(2,1)}), bf16[32,2,512]{2,1,0:T(2,128)(2,1)S(1)}, u32[]{:S(2)}, u32[]{:S(2)}) async-start(bf16[32,2,512]{2,1,0:T(2,128)(2,1)} %broadcast_in_dim.38), calls=%async_computation.5 | async-start | bytes 131072 | tf_op jit(solution)/shard_map/all_to_all | solution.py:27
  132.1 11.1 %all-to-all-start.6 = ((bf16[16,64,128]{2,1,0:T(8,128)(2,1)}), bf16[16,64,128]{2,1,0:T(8,128)(2,1)S(1)}, u32[]{:S(2)}, u32[]{:S(2)}) async-start(bf16[16,64,128]{2,1,0:T(8,128)(2,1)} %broadcast_in_dim.39), calls=%async_computation.6 | async-start | bytes 524288 | tf_op jit(solution)/shard_map/all_to_all | solution.py:27
where the time goes:
time: 145 us; the launch traced here: 144 us
  waiting for transfers between devices  56.3 us (39%)
  starting transfers between devices  40.3 us (28%)
  blocking collectives  28.2 us (19%)
  local copies, waits for them, and re-layouts  8.92 us (6%)
  other arithmetic  6.52 us (4%)
  matrix products  2.42 us (2%)
    all_to_all x2, waiting for transfers between devices, sent_and_summed(): lax.all_to_all(tiles, axis, split_axis=0, concat_axis=0, tiled=True)  35.7 us
    all_to_all x2, blocking collectives, sent_to_all(): return lax.all_to_all(copies, axis, split_axis=0, concat_axis=0, tiled=True)  28.2 us
    all_to_all x2, starting transfers between devices, sent_and_summed(): lax.all_to_all(tiles, axis, split_axis=0, concat_axis=0, tiled=True)  24.1 us
    all_to_all x3, waiting for transfers between devices, sent_to_all(): return lax.all_to_all(copies, axis, split_axis=0, concat_axis=0, tiled=True)  20.6 us
    all_to_all x3, starting transfers between devices, sent_to_all(): return lax.all_to_all(copies, axis, split_axis=0, concat_axis=0, tiled=True)  16.2 us
  transfers between devices with their start and end apart: 5, of which 5 were waited for; matrix products, arithmetic and copies ran while one was open for 4% of the time, Pallas kernels for 0%

commit v1 on v0

v1 whole, which is shorter than its diff:
```python
import jax
import jax.numpy as jnp
from jax import lax
from jax.sharding import Mesh, PartitionSpec as P

MODEL_WIDTH = 4096
HEAD_COUNT = 128
HEAD_DIM = 64
STATE_DIM = 128
LAYERS = 2
EPS = 1e-06

TP = ("y", "x")
CTP = ("core", "y", "x")


def exchange(value, axis):
    return lax.all_to_all(value, axis, split_axis=0, concat_axis=0, tiled=True)


def to_all(value, count):
    return jnp.broadcast_to(value, (count, *value.shape))


def shards(
    stream,
    norm_gain,
    x_weight,
    z_weight,
    bc_weight,
    step_weight,
    conv_x_weight,
    conv_bc_weight,
    step_bias,
    decay_log,
    skip_gain,
    group_gain,
    out_weight,
    scan_state,
    conv_x_state,
    conv_bc_state,
):
    f32, bf16 = jnp.float32, jnp.bfloat16
    n_tp, n_z = lax.axis_size(TP), lax.axis_size("z")
    tp_index = lax.axis_index(TP)
    rows_dev = stream.shape[0]
    cols_dev = stream.shape[1]
    seq_count = scan_state.shape[1]
    heads_dev = scan_state.shape[2]
    x_width = x_weight.shape[2]
    bc_width = 2 * bc_weight.shape[3]
    groups_dev = conv_bc_state.shape[4] // STATE_DIM
    per_group = heads_dev // groups_dev
    seqs = n_z * seq_count

    def in_weights(l):
        step_cols = lax.dynamic_slice_in_dim(step_weight[l], tp_index * heads_dev, heads_dev, 1)
        return jnp.concatenate(
            [x_weight[l], z_weight[l], bc_weight[l].reshape(cols_dev, bc_width), step_cols], axis=1
        )

    own = jnp.broadcast_to(
        stream.reshape(2, 1, rows_dev // 2, cols_dev), (2, n_tp, rows_dev // 2, cols_dev)
    )
    hidden = exchange(own.reshape(2 * n_tp, rows_dev // 2, cols_dev), CTP).reshape(2, seqs, cols_dev)
    w_in = [exchange(to_all(in_weights(l), 2), "core") for l in range(LAYERS)]
    w_out = exchange(to_all(out_weight, 2), "core")
    gain = exchange(to_all(norm_gain, 2), "core")

    states_list, xconv_list, bcconv_list = [], [], []
    result = None
    for l in range(LAYERS):
        widened = hidden.astype(f32)
        normed_in = (widened * gain[:, l][:, None, :]).astype(bf16)
        part_sq = jnp.sum(widened * widened, axis=(0, 2))[:, None]
        part = sum(
            jnp.dot(normed_in[c], w_in[l][c], preferred_element_type=f32) for c in range(2)
        )
        part = jnp.concatenate([part, part_sq], axis=1).astype(bf16)
        got = exchange(part.reshape(n_z, seq_count, -1), "z").astype(f32).sum(axis=0)
        inv_rms = lax.rsqrt(got[:, -1:] / MODEL_WIDTH + EPS)
        proj = got * inv_rms
        proj_x = proj[:, :x_width].astype(bf16)
        proj_z = proj[:, x_width : 2 * x_width].astype(bf16)
        proj_bc = proj[:, 2 * x_width : 2 * x_width + bc_width].astype(bf16)
        proj_bc = proj_bc.reshape(seq_count, 2, -1)
        step_raw = proj[:, 2 * x_width + bc_width : -1]
        window_x = jnp.concatenate([conv_x_state[l], proj_x[:, None, :]], axis=1)
        inputs_x = jax.nn.silu(
            jnp.sum(window_x.astype(f32) * conv_x_weight[l].astype(f32), axis=1)
        )
        window_bc = jnp.concatenate([conv_bc_state[l], proj_bc[:, None]], axis=1)
        inputs_bc = jax.nn.silu(
            jnp.sum(window_bc.astype(f32) * conv_bc_weight[l].astype(f32), axis=1)
        )
        b_part = inputs_bc[:, 0].reshape(seq_count, groups_dev, STATE_DIM)
        c_part = inputs_bc[:, 1].reshape(seq_count, groups_dev, STATE_DIM)
        step_size = jax.nn.softplus(step_raw + step_bias[l])
        decay_rate = jnp.exp(-step_size * jnp.exp(decay_log[l]))
        heads_x = inputs_x.reshape(seq_count, groups_dev, per_group, HEAD_DIM)
        step_heads = step_size.reshape(seq_count, groups_dev, per_group)
        decay_heads = decay_rate.reshape(seq_count, groups_dev, per_group)
        old_state = scan_state[l].reshape(seq_count, groups_dev, per_group, HEAD_DIM, STATE_DIM)
        state_new = (
            old_state * decay_heads[..., None, None]
            + (step_heads[..., None] * heads_x)[..., None] * b_part[:, :, None, None, :]
        )
        readout = jnp.einsum("sgepn,sgn->sgep", state_new, c_part)
        readout = (
            readout + skip_gain[l].reshape(groups_dev, per_group)[None, :, :, None] * heads_x
        )
        gated_out = readout.reshape(seq_count, -1) * jax.nn.silu(proj_z.astype(f32))
        grouped = gated_out.reshape(seq_count, groups_dev, -1)
        normed = grouped * lax.rsqrt(jnp.mean(grouped * grouped, axis=2, keepdims=True) + EPS)
        mixed_rows = (normed.reshape(seq_count, -1) * group_gain[l]).astype(bf16)
        states_list.append(state_new.reshape(seq_count, heads_dev, HEAD_DIM, STATE_DIM))
        xconv_list.append(window_x[:, 1:])
        bcconv_list.append(window_bc[:, 1:])

        mixed = exchange(to_all(mixed_rows, n_z), "z").reshape(seqs, -1)
        terms = jnp.stack(
            [jnp.dot(mixed, w_out[c, l], preferred_element_type=f32) for c in range(2)]
        ).astype(bf16)
        if l + 1 < LAYERS:
            summed = exchange(to_all(terms, n_tp), TP).astype(f32).sum(axis=0)
            hidden = (widened + summed).astype(bf16)
        else:
            both = jnp.concatenate(
                [
                    terms.reshape(2 * n_tp, rows_dev // 2, cols_dev),
                    hidden.reshape(2 * n_tp, rows_dev // 2, cols_dev),
                ],
                axis=1,
            )
            arrived = exchange(both, CTP).reshape(2, n_tp, rows_dev, cols_dev).astype(f32)
            result = arrived[:, :, : rows_dev // 2].sum(axis=1) + arrived[:, 0, rows_dev // 2 :]
            result = result.astype(bf16).reshape(rows_dev, cols_dev)
    return (result, jnp.stack(states_list), jnp.stack(xconv_list), jnp.stack(bcconv_list))


def solution(mesh):
    fine = Mesh(mesh.devices.reshape(4, 4, -1, 2), ("y", "x", "z", "core"))
    dp = ("z", "core")
    in_specs = (
        P(TP, dp),
        P(None, dp),
        P(None, dp, TP),
        P(None, dp, TP),
        P(None, dp, None, TP),
        P(None, dp, None),
        P(None, None, TP),
        P(None, None, None, TP),
        P(None, TP),
        P(None, TP),
        P(None, TP),
        P(None, TP),
        P(None, TP, dp),
        P(None, dp, TP, None, None),
        P(None, dp, None, TP),
        P(None, dp, None, None, TP),
    )
    out_specs = (
        P(TP, dp),
        P(None, dp, TP, None, None),
        P(None, dp, None, TP),
        P(None, dp, None, None, TP),
    )
    return jax.shard_map(shards, mesh=fine, in_specs=in_specs, out_specs=out_specs, check_vma=False)
```

time: 145 us -> 157 us (1.083)
  starting transfers between devices: 40.3 us -> 59.4 us
  blocking collectives: 28.2 us -> 15.8 us
  local copies, waits for them, and re-layouts: 8.92 us -> 11.3 us
  other arithmetic: 6.52 us -> 8.21 us
  waiting for transfers between devices: 56.3 us -> 57.9 us
    all_to_all x5 -> x10, starting transfers between devices: 40.3 us -> 59.4 us  [exchange(): return lax.all_to_all(value, axis, split_axis=0, concat_axis=0, tiled=True)]
    all_to_all x2 -> x1, blocking collectives: 28.2 us -> 15.8 us  [exchange(): return lax.all_to_all(value, axis, split_axis=0, concat_axis=0, tiled=True)]
    broadcast_in_dim x7 -> x12, local copies, waits for them, and re-layouts: 2.87 us -> 5.99 us  [the longest x7 5.35 us: to_all(): return jnp.broadcast_to(value, (count, *value.shape))]
    concatenate x0 -> x5, other arithmetic: none -> 2.18 us  [the longest x2 1.47 us: shards(): part = jnp.concatenate([part, part_sq], axis=1).astype(bf16)]
    all_to_all x5 -> x10, waiting for transfers between devices: 56.3 us -> 57.9 us  [exchange(): return lax.all_to_all(value, axis, split_axis=0, concat_axis=0, tiled=True)]
  transfers between devices with their start and end apart: 5 -> 10, of which waited for: 5 -> 9; matrix products, arithmetic and copies ran while one was open for 4% -> 4% of each run, Pallas kernels for 0% -> 0%
where the time goes in v1:
time: 157 us; the launch traced here: 156 us
  starting transfers between devices  59.4 us (38%)
  waiting for transfers between devices  57.9 us (37%)
  blocking collectives  15.8 us (10%)
  local copies, waits for them, and re-layouts  11.3 us (7%)
  other arithmetic  8.21 us (5%)
  matrix products  2.28 us (1%)
    all_to_all x10, starting transfers between devices, exchange(): return lax.all_to_all(value, axis, split_axis=0, concat_axis=0, tiled=True)  59.4 us
    all_to_all x10, waiting for transfers between devices, exchange(): return lax.all_to_all(value, axis, split_axis=0, concat_axis=0, tiled=True)  57.9 us
    all_to_all x1, blocking collectives, exchange(): return lax.all_to_all(value, axis, split_axis=0, concat_axis=0, tiled=True)  15.8 us
    broadcast_in_dim x7, local copies, waits for them, and re-layouts, to_all(): return jnp.broadcast_to(value, (count, *value.shape))  5.35 us
  transfers between devices with their start and end apart: 10, of which 9 were waited for; matrix products, arithmetic and copies ran while one was open for 4% of the time, Pallas kernels for 0%

profile of v1, /device:TPU:1, one launch (start us, length us, event | category | flops | bytes accessed | tf_op | source)
XLA Modules:
  0.0 155.9 jit_solution(10495254300608993881)
XLA Ops:
  0.6 1.3 broadcast_in_dim.48
  1.9 10.0 %all-to-all-start.1 = ((f32[2,2,128]{2,1,0:T(2,128)}), f32[2,2,128]{2,1,0:T(2,128)S(1)}, u32[]{:S(2)}, u32[]{:S(2)}) async-start(f32[2,2,128]{2,1,0:T(2,128)} %broadcast_in_dim.48), calls=%async_computation.1 | async-start | bytes 4096 | tf_op jit(solution)/shard_map/all_to_all | solution.py:18
  12.0 0.7 bitcast_convert_fusion
  12.7 0.8 fusion.53
  13.7 0.7 slice_bitcast_fusion.28
  14.4 0.8 fusion.55
  15.3 0.6 copy-done.9
  16.1 0.7 copy-done.7
  16.7 0.6 broadcast_in_dim.23
  17.4 3.6 %all-to-all-start = ((bf16[32,2,128]{2,1,0:T(2,128)(2,1)}), bf16[32,2,128]{2,1,0:T(2,128)(2,1)S(1)}, u32[]{:S(2)}, u32[]{:S(2)}) async-start(bf16[32,2,128]{2,1,0:T(2,128)(2,1)} %bitcast.2), calls=%async_computation | async-start | bytes 32768 | tf_op jit(solution)/shard_map/all_to_all | solution.py:18
  21.2 6.5 %all-to-all-done = bf16[32,2,128]{2,1,0:T(2,128)(2,1)S(1)} async-done(((bf16[32,2,128]{2,1,0:T(2,128)(2,1)}), bf16[32,2,128]{2,1,0:T(2,128)(2,1)S(1)}, u32[]{:S(2)}, u32[]{:S(2)}) %all-to-all-start) | async-done | bytes 16416 | tf_op jit(solution)/shard_map/all_to_all | solution.py:18
  27.8 0.9 broadcast_in_dim.49
  28.6 4.2 %all-to-all-start.2 = ((bf16[2,128,1288]{1,2,0:T(8,128)(2,1)}), bf16[2,128,1288]{1,2,0:T(8,128)(2,1)S(1)}, u32[]{:S(2)}, u32[]{:S(2)}) async-start(bf16[2,128,1288]{1,2,0:T(8,128)(2,1)} %broadcast_in_dim.49), calls=%async_computation.2 | async-start | bytes 1318912 | tf_op jit(solution)/shard_map/all_to_all | solution.py:18
  33.2 1.1 all-to-all-done.2
  34.3 0.2 fusion.17
  34.5 0.2 fusion
  34.8 0.7 pad_maximum_fusion.3
  35.6 13.3 %all-to-all-start.3 = ((bf16[16,2,1289]{2,1,0:T(2,128)(2,1)}), bf16[16,2,1289]{2,1,0:T(2,128)(2,1)S(1)}, u32[]{:S(2)}, u32[]{:S(2)}) async-start(bf16[16,2,1289]{2,1,0:T(2,128)(2,1)} %pad_maximum_fusion.3), calls=%async_computation.3 | async-start | bytes 180224 | tf_op jit(solution)/shard_map/all_to_all | solution.py:18
  49.0 11.9 %all-to-all-done.3 = bf16[16,2,1289]{2,1,0:T(2,128)(2,1)S(1)} async-done(((bf16[16,2,1289]{2,1,0:T(2,128)(2,1)}), bf16[16,2,1289]{2,1,0:T(2,128)(2,1)S(1)}, u32[]{:S(2)}, u32[]{:S(2)}) %all-to-all-start.3) | async-done | bytes 82528 | tf_op jit(solution)/shard_map/all_to_all | solution.py:18
  61.5 0.4 fusion.7
  62.3 15.8 %all_to_all.55 = bf16[16,2,512]{2,1,0:T(2,128)(2,1)S(1)} all-to-all(bf16[16,2,512]{2,1,0:T(2,128)(2,1)S(1)} %broadcast_in_dim.51), channel_id=1, replica_groups=mesh['y'=4,'x'=4,'z'=16,'core'=2] {'z'}, dimensions={0} | all-to-all | bytes 65536 | tf_op jit(solution)/shard_map/all_to_all | solution.py:18
  78.1 0.9 broadcast_in_dim.52
  79.0 5.9 %all-to-all-start.5 = ((bf16[2,2,512,128]{3,2,1,0:T(8,128)(2,1)}), bf16[2,2,512,128]{3,2,1,0:T(8,128)(2,1)S(1)}, u32[]{:S(2)}, u32[]{:S(2)}) async-start(bf16[2,2,512,128]{3,2,1,0:T(8,128)(2,1)} %broadcast_in_dim.52), calls=%async_computation.5 | async-start | bytes 1048576 | tf_op jit(solution)/shard_map/all_to_all | solution.py:18
  84.9 1.4 all-to-all-done.5
  86.6 0.8 broadcast_in_dim.53
  87.3 3.5 %all-to-all-start.6 = ((bf16[16,2,32,128]{3,2,1,0:T(8,128)(2,1)}), bf16[16,2,32,128]{3,2,1,0:T(8,128)(2,1)S(1)}, u32[]{:S(2)}, u32[]{:S(2)}) async-start(bf16[16,2,32,128]{3,2,1,0:T(8,128)(2,1)} %broadcast_in_dim.53), calls=%async_computation.6 | async-start | bytes 524288 | tf_op jit(solution)/shard_map/all_to_all | solution.py:18
  90.9 0.2 copy.50
  91.2 8.1 %all-to-all-done.6 = bf16[16,2,32,128]{3,2,1,0:T(8,128)(2,1)S(1)} async-done(((bf16[16,2,32,128]{3,2,1,0:T(8,128)(2,1)}), bf16[16,2,32,128]{3,2,1,0:T(8,128)(2,1)S(1)}, u32[]{:S(2)}, u32[]{:S(2)}) %all-to-all-start.6) | async-done | bytes 262176 | tf_op jit(solution)/shard_map/all_to_all | solution.py:18
  99.2 0.9 broadcast_in_dim.54
  100.1 4.7 %all-to-all-start.7 = ((bf16[2,128,1288]{1,2,0:T(8,128)(2,1)}), bf16[2,128,1288]{1,2,0:T(8,128)(2,1)S(1)}, u32[]{:S(2)}, u32[]{:S(2)}) async-start(bf16[2,128,1288]{1,2,0:T(8,128)(2,1)} %broadcast_in_dim.54), calls=%async_computation.7 | async-start | bytes 1318912 | tf_op jit(solution)/shard_map/all_to_all | solution.py:18
  105.3 1.1 all-to-all-done.7
  106.3 0.2 fusion.16
  106.5 0.2 fusion.1
  106.8 0.7 pad_maximum_fusion.4
  107.6 3.5 %all-to-all-start.8 = ((bf16[16,2,1289]{2,1,0:T(2,128)(2,1)}), bf16[16,2,1289]{2,1,0:T(2,128)(2,1)S(1)}, u32[]{:S(2)}, u32[]{:S(2)}) async-start(bf16[16,2,1289]{2,1,0:T(2,128)(2,1)} %pad_maximum_fusion.4), calls=%async_computation.8 | async-start | bytes 180224 | tf_op jit(solution)/shard_map/all_to_all | solution.py:18
  111.1 11.8 %all-to-all-done.8 = bf16[16,2,1289]{2,1,0:T(2,128)(2,1)S(1)} async-done(((bf16[16,2,1289]{2,1,0:T(2,128)(2,1)}), bf16[16,2,1289]{2,1,0:T(2,128)(2,1)S(1)}, u32[]{:S(2)}, u32[]{:S(2)}) %all-to-all-start.8) | async-done | bytes 82528 | tf_op jit(solution)/shard_map/all_to_all | solution.py:18
  123.5 0.4 fusion.10
  123.9 0.4 multiply_add_fusion.1
  124.8 0.6 broadcast_in_dim.56
  125.4 4.8 %all-to-all-start.9 = ((bf16[16,2,512]{2,1,0:T(2,128)(2,1)}), bf16[16,2,512]{2,1,0:T(2,128)(2,1)S(1)}, u32[]{:S(2)}, u32[]{:S(2)}) async-start(bf16[16,2,512]{2,1,0:T(2,128)(2,1)} %broadcast_in_dim.56), calls=%async_computation.9 | async-start | bytes 65536 | tf_op jit(solution)/shard_map/all_to_all | solution.py:18
  130.2 1.1 pad_maximum_fusion
  131.3 0.6 pad_maximum_fusion.10
  131.9 9.8 %all-to-all-done.9 = bf16[16,2,512]{2,1,0:T(2,128)(2,1)S(1)} async-done(((bf16[16,2,512]{2,1,0:T(2,128)(2,1)}), bf16[16,2,512]{2,1,0:T(2,128)(2,1)S(1)}, u32[]{:S(2)}, u32[]{:S(2)}) %all-to-all-start.9) | async-done | bytes 32800 | tf_op jit(solution)/shard_map/all_to_all | solution.py:18
  142.0 0.7 pad_maximum_fusion.5
  142.7 5.7 %all-to-all-start.10 = ((bf16[32,4,128]{2,1,0:T(4,128)(2,1)}), bf16[32,4,128]{2,1,0:T(4,128)(2,1)S(1)}, u32[]{:S(2)}, u32[]{:S(2)}) async-start(bf16[32,4,128]{2,1,0:T(4,128)(2,1)} %pad_maximum_fusion.5), calls=%async_computation.10 | async-start | bytes 65536 | tf_op jit(solution)/shard_map/all_to_all | solution.py:18
  148.4 0.6 pad_maximum_fusion.11
  149.0 6.4 %all-to-all-done.10 = bf16[32,4,128]{2,1,0:T(4,128)(2,1)S(1)} async-done(((bf16[32,4,128]{2,1,0:T(4,128)(2,1)}), bf16[32,4,128]{2,1,0:T(4,128)(2,1)S(1)}, u32[]{:S(2)}, u32[]{:S(2)}) %all-to-all-start.10) | async-done | bytes 32800 | tf_op jit(solution)/shard_map/all_to_all | solution.py:18
  155.4 0.6 add_convert_fusion.1
  (103 shorter events, 4.2 us)
Async XLA Ops:
  0.6 12.9 %copy-start.4 = (bf16[2,128,2,128]{3,2,1,0:T(2,128)(2,1)S(1)}, bf16[2,128,2,128]{3,2,1,0:T(2,128)(2,1)}, u32[]{:S(2)}) copy-start(bf16[2,128,2,128]{3,2,1,0:T(2,128)(2,1)} %param.20) | copy-start | bytes 393220
  1.9 14.1 %all-to-all-start.1 = ((f32[2,2,128]{2,1,0:T(2,128)}), f32[2,2,128]{2,1,0:T(2,128)S(1)}, u32[]{:S(2)}, u32[]{:S(2)}) async-start(f32[2,2,128]{2,1,0:T(2,128)} %broadcast_in_dim.48), calls=%async_computation.1 | async-start | bytes 4096 | tf_op jit(solution)/shard_map/all_to_all | solution.py:18
  12.7 1.0 copy-start.6
  12.7 1.7 %copy-start.5 = (bf16[2,5,512]{2,0,1:T(2,128)(2,1)S(1)}, bf16[2,5,512]{2,0,1:T(2,128)(2,1)}, u32[]{:S(2)}) copy-start(bf16[2,5,512]{2,0,1:T(2,128)(2,1)} %param.22) | copy-start | bytes 30724
  12.7 2.5 %copy-start.3 = (bf16[2,128,512]{2,1,0:T(8,128)(2,1)S(1)}, bf16[2,128,512]{2,1,0:T(8,128)(2,1)}, u32[]{:S(2)}) copy-start(bf16[2,128,512]{2,1,0:T(8,128)(2,1)} %param.18) | copy-start | bytes 786436
  13.5 1.7 %copy-start.2 = (bf16[2,128,512]{2,1,0:T(8,128)(2,1)S(1)}, bf16[2,128,512]{2,1,0:T(8,128)(2,1)}, u32[]{:S(2)}) copy-start(bf16[2,128,512]{2,1,0:T(8,128)(2,1)} %param.19) | copy-start | bytes 786436
  15.2 0.7 copy-start.9
  15.2 0.7 copy-start.10
  16.1 0.7 copy-start.7
  17.4 10.4 %all-to-all-start = ((bf16[32,2,128]{2,1,0:T(2,128)(2,1)}), bf16[32,2,128]{2,1,0:T(2,128)(2,1)S(1)}, u32[]{:S(2)}, u32[]{:S(2)}) async-start(bf16[32,2,128]{2,1,0:T(2,128)(2,1)} %bitcast.2), calls=%async_computation | async-start | bytes 32768 | tf_op jit(solution)/shard_map/all_to_all | solution.py:18
  28.6 5.7 %all-to-all-start.2 = ((bf16[2,128,1288]{1,2,0:T(8,128)(2,1)}), bf16[2,128,1288]{1,2,0:T(8,128)(2,1)S(1)}, u32[]{:S(2)}, u32[]{:S(2)}) async-start(bf16[2,128,1288]{1,2,0:T(8,128)(2,1)} %broadcast_in_dim.49), calls=%async_computation.2 | async-start | bytes 1318912 | tf_op jit(solution)/shard_map/all_to_all | solution.py:18
  33.1 28.4 %copy-start = (f32[2,2,8,64,128]{4,3,2,1,0:T(8,128)S(1)}, f32[2,2,8,64,128]{4,3,2,1,0:T(8,128)}, u32[]{:S(2)}) copy-start(f32[2,2,8,64,128]{4,3,2,1,0:T(8,128)} %param.29) | copy-start | bytes 3145732
  35.6 13.3 %copy-start.8 = (f32[2,8]{1,0:T(2,128)S(1)}, f32[2,8]{1,0:T(2,128)}, u32[]{:S(2)}) copy-start(f32[2,8]{1,0:T(2,128)} %param.26) | copy-start | bytes 196
  35.6 25.2 %all-to-all-start.3 = ((bf16[16,2,1289]{2,1,0:T(2,128)(2,1)}), bf16[16,2,1289]{2,1,0:T(2,128)(2,1)S(1)}, u32[]{:S(2)}, u32[]{:S(2)}) async-start(bf16[16,2,1289]{2,1,0:T(2,128)(2,1)} %pad_maximum_fusion.3), calls=%async_computation.3 | async-start | bytes 180224 | tf_op jit(solution)/shard_map/all_to_all | solution.py:18
  61.5 16.7 %copy-start.1 = (bf16[2,512,128]{2,1,0:T(8,128)(2,1)S(1)}, bf16[2,512,128]{2,1,0:T(8,128)(2,1)}, u32[]{:S(2)}) copy-start(bf16[2,512,128]{2,1,0:T(8,128)(2,1)} %param.28) | copy-start | bytes 786436
  79.0 7.3 %all-to-all-start.5 = ((bf16[2,2,512,128]{3,2,1,0:T(8,128)(2,1)}), bf16[2,2,512,128]{3,2,1,0:T(8,128)(2,1)S(1)}, u32[]{:S(2)}, u32[]{:S(2)}) async-start(bf16[2,2,512,128]{3,2,1,0:T(8,128)(2,1)} %broadcast_in_dim.52), calls=%async_computation.5 | async-start | bytes 1048576 | tf_op jit(solution)/shard_map/all_to_all | solution.py:18
  87.3 11.9 %all-to-all-start.6 = ((bf16[16,2,32,128]{3,2,1,0:T(8,128)(2,1)}), bf16[16,2,32,128]{3,2,1,0:T(8,128)(2,1)S(1)}, u32[]{:S(2)}, u32[]{:S(2)}) async-start(bf16[16,2,32,128]{3,2,1,0:T(8,128)(2,1)} %broadcast_in_dim.53), calls=%async_computation.6 | async-start | bytes 524288 | tf_op jit(solution)/shard_map/all_to_all | solution.py:18
  100.1 6.2 %all-to-all-start.7 = ((bf16[2,128,1288]{1,2,0:T(8,128)(2,1)}), bf16[2,128,1288]{1,2,0:T(8,128)(2,1)S(1)}, u32[]{:S(2)}, u32[]{:S(2)}) async-start(bf16[2,128,1288]{1,2,0:T(8,128)(2,1)} %broadcast_in_dim.54), calls=%async_computation.7 | async-start | bytes 1318912 | tf_op jit(solution)/shard_map/all_to_all | solution.py:18
  107.6 15.3 %all-to-all-start.8 = ((bf16[16,2,1289]{2,1,0:T(2,128)(2,1)}), bf16[16,2,1289]{2,1,0:T(2,128)(2,1)S(1)}, u32[]{:S(2)}, u32[]{:S(2)}) async-start(bf16[16,2,1289]{2,1,0:T(2,128)(2,1)} %pad_maximum_fusion.4), calls=%async_computation.8 | async-start | bytes 180224 | tf_op jit(solution)/shard_map/all_to_all | solution.py:18
  125.4 16.3 %all-to-all-start.9 = ((bf16[16,2,512]{2,1,0:T(2,128)(2,1)}), bf16[16,2,512]{2,1,0:T(2,128)(2,1)S(1)}, u32[]{:S(2)}, u32[]{:S(2)}) async-start(bf16[16,2,512]{2,1,0:T(2,128)(2,1)} %broadcast_in_dim.56), calls=%async_computation.9 | async-start | bytes 65536 | tf_op jit(solution)/shard_map/all_to_all | solution.py:18
  142.7 12.7 %all-to-all-start.10 = ((bf16[32,4,128]{2,1,0:T(4,128)(2,1)}), bf16[32,4,128]{2,1,0:T(4,128)(2,1)S(1)}, u32[]{:S(2)}, u32[]{:S(2)}) async-start(bf16[32,4,128]{2,1,0:T(4,128)(2,1)} %pad_maximum_fusion.5), calls=%async_computation.10 | async-start | bytes 65536 | tf_op jit(solution)/shard_map/all_to_all | solution.py:18

commit v2 on v1

v2 whole, which is shorter than its diff:
```python
import functools

import jax
import jax.numpy as jnp
from jax import lax
from jax.experimental import pallas as pl
from jax.experimental.pallas import tpu as pltpu
from jax.sharding import Mesh, PartitionSpec as P


MODEL_WIDTH = 4096
HEAD_DIM = 64
STATE_DIM = 128
LAYERS = 2
EPS = 1e-06
LANES = 128

TP = ("y", "x")
CTP = ("core", "y", "x")
VMEM = pl.BlockSpec(memory_space=pltpu.VMEM)
SMEM = pl.BlockSpec(memory_space=pltpu.SMEM)
f32, bf16 = jnp.float32, jnp.bfloat16


def exchange(value, axis):
    return lax.all_to_all(value, axis, split_axis=0, concat_axis=0, tiled=True)


def swap_cores(value):
    return lax.ppermute(value, "core", [(0, 1), (1, 0)])


def to_all(value, count):
    return jnp.broadcast_to(value, (count, *value.shape))


def call(body, out_shape, n_in, flops, size, smem=0):
    return pl.pallas_call(
        body,
        out_shape=out_shape,
        in_specs=[SMEM] * smem + [VMEM] * (n_in - smem),
        out_specs=jax.tree.map(lambda _: VMEM, out_shape),
        compiler_params=pltpu.CompilerParams(vmem_limit_bytes=8 * 1024 * 1024),
        cost_estimate=pl.CostEstimate(flops=flops, bytes_accessed=size, transcendentals=0),
    )


def put_projections(layer, x_ref, z_ref, bc_ref, step_ref, out_ref):
    at = 0
    for ref in (x_ref, z_ref, bc_ref, step_ref):
        for k in range(ref.shape[2] // LANES):
            out_ref[at] = ref[layer, :, k * LANES : (k + 1) * LANES]
            at += 1
    return at


def pack_first(x_ref, z_ref, bc_ref, step_ref, out_ref):
    put_projections(0, x_ref, z_ref, bc_ref, step_ref, out_ref)


def pack_rest(x_ref, z_ref, bc_ref, step_ref, w_ref, gain_ref, out_ref):
    at = put_projections(1, x_ref, z_ref, bc_ref, step_ref, out_ref)
    for l in range(LAYERS):
        for k in range(w_ref.shape[1] // LANES):
            out_ref[at] = w_ref[l, k * LANES : (k + 1) * LANES, :]
            at += 1
    gain = gain_ref[1:2, :]
    first = gain.astype(bf16)
    left = gain - first.astype(f32)
    second = left.astype(bf16)
    third = (left - second.astype(f32)).astype(bf16)
    row = lax.broadcasted_iota(jnp.int32, (LANES, LANES), 0)
    pieces = jnp.where(
        row == 0,
        first.astype(f32),
        jnp.where(row == 1, second.astype(f32), jnp.where(row == 2, third.astype(f32), 0.0)),
    ).astype(bf16)
    out_ref[at] = pieces


def project(normed, squares, first, weights, place, out_ref, blocks):
    total = None
    for rows, w_ref in zip(normed, weights):
        block = jnp.concatenate([w_ref[k] for k in range(blocks)], axis=1)
        term = jnp.dot(rows, block, preferred_element_type=f32)
        total = term if total is None else total + term
    wide = (blocks - 1) * LANES
    out_ref[:, :wide] = total[:, :wide].astype(bf16)
    lane = lax.broadcasted_iota(jnp.int32, (total.shape[0], LANES), 1)
    tail = pltpu.roll(total[:, wide:], LANES - place, 1)
    tail = jnp.where(lane == first, squares, tail)
    out_ref[:, wide:] = tail.astype(bf16)


def project_first(blocks, heads, place_ref, hidden_ref, normed_ref, own_ref, other_ref, out_ref):
    core = place_ref[1]
    wide = [hidden_ref[c].astype(f32) for c in range(2)]
    squares = jnp.sum(wide[0] * wide[0] + wide[1] * wide[1], axis=1, keepdims=True)
    normed = [normed_ref[core], normed_ref[1 - core]]
    project(normed, squares, heads, (own_ref, other_ref), place_ref[0], out_ref, blocks)


def project_next(
    blocks, heads, place_ref, arrived_ref, hidden_ref, own_ref, other_ref, out_ref, next_ref
):
    core = place_ref[1]
    wide, normed = [], []
    last = own_ref.shape[0] - 1
    for c, w_ref in ((core, own_ref), (1 - core, other_ref)):
        summed = arrived_ref[0, c].astype(f32)
        for j in range(1, arrived_ref.shape[0]):
            summed = summed + arrived_ref[j, c].astype(f32)
        new = (hidden_ref[c].astype(f32) + summed).astype(bf16)
        next_ref[c] = new
        pieces = w_ref[last].astype(f32)
        gain = pieces[0:1] + pieces[1:2] + pieces[2:3]
        wide.append(new.astype(f32))
        normed.append((new.astype(f32) * gain).astype(bf16))
    squares = jnp.sum(wide[0] * wide[0] + wide[1] * wide[1], axis=1, keepdims=True)
    project(normed, squares, heads, (own_ref, other_ref), place_ref[0], out_ref, blocks)


def out_terms(mixed_ref, w_ref, at, blocks):
    weights = jnp.concatenate([w_ref[at + k] for k in range(blocks)], axis=0)
    return jnp.dot(mixed_ref[...], weights, preferred_element_type=f32).astype(bf16)


def mix_to_all(at, blocks, place_ref, mixed_ref, own_ref, other_ref, out_ref):
    core = place_ref[1]
    for c, w_ref in ((core, own_ref), (1 - core, other_ref)):
        terms = out_terms(mixed_ref, w_ref, at, blocks)
        for j in range(out_ref.shape[0]):
            out_ref[j, c] = terms


def mix_last(at, blocks, place_ref, mixed_ref, own_ref, other_ref, out_ref):
    core = place_ref[1]
    for c, w_ref in ((core, own_ref), (1 - core, other_ref)):
        out_ref[c] = out_terms(mixed_ref, w_ref, at, blocks)


def shards(
    stream,
    norm_gain,
    x_weight,
    z_weight,
    bc_weight,
    step_weight,
    conv_x_weight,
    conv_bc_weight,
    step_bias,
    decay_log,
    skip_gain,
    group_gain,
    out_weight,
    scan_state,
    conv_x_state,
    conv_bc_state,
):
    n_tp, n_z = lax.axis_size(TP), lax.axis_size("z")
    tp_index = lax.axis_index(TP)
    rows_dev, cols_dev = stream.shape
    half = rows_dev // 2
    seq_count, heads_dev = scan_state.shape[1:3]
    x_width = x_weight.shape[2]
    bc_width = 2 * bc_weight.shape[3]
    groups_dev = conv_bc_state.shape[4] // STATE_DIM
    per_group = heads_dev // groups_dev
    seqs = n_z * seq_count
    in_blocks = (2 * x_width + bc_width) // LANES + 1
    out_blocks = x_width // LANES
    rest = in_blocks + LAYERS * out_blocks + 1
    wide = in_blocks * LANES
    place = jnp.stack([tp_index * heads_dev, lax.axis_index("core")]).astype(jnp.int32)
    shape = jax.ShapeDtypeStruct

    normed_own = (stream.astype(f32) * norm_gain[0]).astype(bf16)
    own = jnp.stack([stream.reshape(2, half, cols_dev), normed_own.reshape(2, half, cols_dev)], 1)
    own = own.reshape(2, 1, rows_dev, cols_dev)
    own = jnp.broadcast_to(own, (2, n_tp, rows_dev, cols_dev))
    rows = exchange(own.reshape(2 * n_tp, rows_dev, cols_dev), CTP)
    bc_flat = bc_weight.reshape(LAYERS, cols_dev, bc_width)
    packed = call(
        pack_first, shape((in_blocks, cols_dev, LANES), bf16), 4, 1000000, 1000000
    )(x_weight, z_weight, bc_flat, step_weight)
    w_first = (packed, swap_cores(packed))
    packed = call(
        pack_rest, shape((rest, cols_dev, LANES), bf16), 6, 1000000, 1000000
    )(x_weight, z_weight, bc_flat, step_weight, out_weight, norm_gain)
    w_rest = (packed, swap_cores(packed))
    x_tap = conv_x_weight.astype(f32)
    bc_tap = conv_bc_weight.astype(f32)
    x_base = jnp.sum(conv_x_state.astype(f32) * x_tap[:, None, :-1], axis=2)
    bc_base = jnp.sum(conv_bc_state.astype(f32) * bc_tap[:, None, :-1], axis=2)
    rate = jnp.exp(decay_log)

    states_list, xconv_list, bcconv_list = [], [], []
    result = None
    hidden = None
    for l in range(LAYERS):
        if l == 0:
            rows = rows.reshape(2, n_tp, 2, half, cols_dev)
            hidden = rows[:, :, 0].reshape(2, seqs, cols_dev)
            normed_in = rows[:, :, 1].reshape(2, seqs, cols_dev)
            part = call(
                functools.partial(project_first, in_blocks, heads_dev),
                shape((seqs, wide), bf16), 5, 10000000, 1000000, smem=1,
            )(place, hidden, normed_in, *w_first)
        else:
            part, hidden = call(
                functools.partial(project_next, in_blocks, heads_dev),
                (shape((seqs, wide), bf16), shape((2, seqs, cols_dev), bf16)), 5, 10000000, 1000000, smem=1,
            )(place, arrived, hidden, *w_rest)
        got = exchange(part.reshape(n_z, seq_count, wide), "z")
        got = got.astype(f32).sum(axis=0)
        tail = wide - LANES
        inv_rms = lax.rsqrt(got[:, tail + heads_dev : tail + heads_dev + 1] / MODEL_WIDTH + EPS)
        proj_x = (got[:, :x_width] * inv_rms).astype(bf16)
        proj_z = (got[:, x_width : 2 * x_width] * inv_rms).astype(bf16)
        proj_bc = (got[:, 2 * x_width : tail] * inv_rms).astype(bf16).reshape(seq_count, 2, -1)
        step_raw = got[:, tail : tail + heads_dev] * inv_rms
        inputs_x = jax.nn.silu(x_base[l] + proj_x.astype(f32) * x_tap[l, -1])
        inputs_bc = jax.nn.silu(bc_base[l] + proj_bc.astype(f32) * bc_tap[l, -1])
        b_part = inputs_bc[:, 0].reshape(seq_count, groups_dev, STATE_DIM)
        c_part = inputs_bc[:, 1].reshape(seq_count, groups_dev, STATE_DIM)
        step_size = jax.nn.softplus(step_raw + step_bias[l])
        decay_rate = jnp.exp(-step_size * rate[l])
        heads_x = inputs_x.reshape(seq_count, groups_dev, per_group, HEAD_DIM)
        step_heads = step_size.reshape(seq_count, groups_dev, per_group)
        decay_heads = decay_rate.reshape(seq_count, groups_dev, per_group)
        old_state = scan_state[l].reshape(seq_count, groups_dev, per_group, HEAD_DIM, STATE_DIM)
        state_new = (
            old_state * decay_heads[..., None, None]
            + (step_heads[..., None] * heads_x)[..., None] * b_part[:, :, None, None, :]
        )
        readout = jnp.einsum("sgepn,sgn->sgep", state_new, c_part)
        readout = (
            readout + skip_gain[l].reshape(groups_dev, per_group)[None, :, :, None] * heads_x
        )
        gated_out = readout.reshape(seq_count, -1) * jax.nn.silu(proj_z.astype(f32))
        grouped = gated_out.reshape(seq_count, groups_dev, -1)
        normed = grouped * lax.rsqrt(jnp.mean(grouped * grouped, axis=2, keepdims=True) + EPS)
        mixed_rows = (normed.reshape(seq_count, -1) * group_gain[l]).astype(bf16)
        states_list.append(state_new.reshape(seq_count, heads_dev, HEAD_DIM, STATE_DIM))
        xconv_list.append(jnp.concatenate([conv_x_state[l, :, 1:], proj_x[:, None]], axis=1))
        bcconv_list.append(jnp.concatenate([conv_bc_state[l, :, 1:], proj_bc[:, None]], axis=1))

        mixed = exchange(to_all(mixed_rows, n_z), "z").reshape(seqs, -1)
        at = in_blocks + l * out_blocks
        if l + 1 < LAYERS:
            terms = call(
                functools.partial(mix_to_all, at, out_blocks),
                shape((n_tp, 2, seqs, cols_dev), bf16), 4, 10000000, 1000000, smem=1,
            )(place, mixed, *w_rest)
            arrived = exchange(terms, TP)
        else:
            terms = call(
                functools.partial(mix_last, at, out_blocks),
                shape((2, seqs, cols_dev), bf16), 4, 10000000, 1000000, smem=1,
            )(place, mixed, *w_rest)
            both = jnp.concatenate(
                [terms.reshape(2 * n_tp, half, cols_dev), hidden.reshape(2 * n_tp, half, cols_dev)],
                axis=1,
            )
            got = exchange(both, CTP).reshape(2, n_tp, rows_dev, cols_dev).astype(f32)
            result = got[:, :, :half].sum(axis=1) + got[:, 0, half:]
            result = result.astype(bf16).reshape(rows_dev, cols_dev)
    outs = (jnp.stack(states_list), jnp.stack(xconv_list), jnp.stack(bcconv_list))
    return (result, *outs)


def solution(mesh):
    fine = Mesh(mesh.devices.reshape(4, 4, -1, 2), ("y", "x", "z", "core"))
    dp = ("z", "core")
    in_specs = (
        P(TP, dp),
        P(None, dp),
        P(None, dp, TP),
        P(None, dp, TP),
        P(None, dp, None, TP),
        P(None, dp, None),
        P(None, None, TP),
        P(None, None, None, TP),
        P(None, TP),
        P(None, TP),
        P(None, TP),
        P(None, TP),
        P(None, TP, dp),
        P(None, dp, TP, None, None),
        P(None, dp, None, TP),
        P(None, dp, None, None, TP),
    )
    out_specs = (
        P(TP, dp),
        P(None, dp, TP, None, None),
        P(None, dp, None, TP),
        P(None, dp, None, None, TP),
    )
    return jax.shard_map(shards, mesh=fine, in_specs=in_specs, out_specs=out_specs, check_vma=False)
```

time: 157 us -> 133 us (0.85)
  waiting for transfers between devices: 57.9 us -> 46.4 us
  starting transfers between devices: 59.4 us -> 51.7 us
  local copies, waits for them, and re-layouts: 11.3 us -> 6.66 us
  Pallas kernels: 0 us -> 3.94 us
  other arithmetic: 8.21 us -> 6.13 us
    all_to_all x10 -> x6, starting transfers between devices: 59.4 us -> 47.1 us  [exchange(): return lax.all_to_all(value, axis, split_axis=0, concat_axis=0, tiled=True)]
    all_to_all x10 -> x6, waiting for transfers between devices: 57.9 us -> 46.4 us  [exchange(): return lax.all_to_all(value, axis, split_axis=0, concat_axis=0, tiled=True)]
    broadcast_in_dim x7 -> x2, local copies, waits for them, and re-layouts: 5.35 us -> 0.68 us  [to_all(): return jnp.broadcast_to(value, (count, *value.shape))]
    ppermute x0 -> x2, starting transfers between devices: none -> 4.59 us  [swap_cores(): return lax.ppermute(value, 'core', [(0, 1), (1, 0)])]
    pallas_call x0 -> x6, Pallas kernels: none -> 3.94 us  [the longest x1 1.42 us: shards(): call(functools.partial(mix_to_all, at, out_blocks), shape((n_tp, 2, seqs,...]
    reshape x0 -> x5, local copies, waits for them, and re-layouts: none -> 2.56 us  [the longest x2 1.38 us: shards(): got = exchange(part.reshape(n_z, seq_count, wide), 'z')]
  transfers between devices with their start and end apart: 10 -> 8, of which waited for: 9 -> 5; matrix products, arithmetic and copies ran while one was open for 4% -> 4% of each run, Pallas kernels for 0% -> 1%
where the time goes in v2:
time: 133 us
  starting transfers between devices  51.7 us (39%)
  waiting for transfers between devices  46.4 us (35%)
  blocking collectives  15.9 us (12%)
  local copies, waits for them, and re-layouts  6.66 us (5%)
  other arithmetic  6.13 us (5%)
  Pallas kernels  3.94 us (3%)
    all_to_all x6, starting transfers between devices, exchange(): return lax.all_to_all(value, axis, split_axis=0, concat_axis=0, tiled=True)  47.1 us
    all_to_all x6, waiting for transfers between devices, exchange(): return lax.all_to_all(value, axis, split_axis=0, concat_axis=0, tiled=True)  46.4 us
    all_to_all x1, blocking collectives, exchange(): return lax.all_to_all(value, axis, split_axis=0, concat_axis=0, tiled=True)  15.9 us
    ppermute x2, starting transfers between devices, swap_cores(): return lax.ppermute(value, 'core', [(0, 1), (1, 0)])  4.59 us
  transfers between devices with their start and end apart: 8, of which 5 were waited for; matrix products, arithmetic and copies ran while one was open for 4% of the time, Pallas kernels for 1%

profile of v2, /device:TPU:1, one launch (start us, length us, event | category | flops | bytes accessed | tf_op | source)
XLA Modules:
  0.0 132.7 jit_solution(6071822054114520689)
XLA Ops:
  0.7 0.7 slice_bitcast_fusion.20
  1.4 0.6 broadcast_in_dim.26
  2.0 10.4 %all-to-all-start = ((bf16[32,4,128]{2,1,0:T(4,128)(2,1)}), bf16[32,4,128]{2,1,0:T(4,128)(2,1)S(1)}, u32[]{:S(2)}, u32[]{:S(2)}) async-start(bf16[32,4,128]{2,1,0:T(4,128)(2,1)} %bitcast.10), calls=%async_computation | async-start | bytes 65536 | tf_op jit(solution)/shard_map/all_to_all | solution.py:26
  12.5 1.0 reshape.185.bc_ref
  13.6 0.9 copy-done.1
  14.6 2.3 %collective-permute-start = (bf16[11,128,128]{2,1,0:T(8,128)(2,1)S(1)}, bf16[11,128,128]{2,1,0:T(8,128)(2,1)S(1)}, u32[]{:S(2)}, u32[]{:S(2)}) collective-permute-start(bf16[11,128,128]{2,1,0:T(8,128)(2,1)S(1)} %shard_map.183.own_ref), channel_id=1, source_target_pairs={{0,1},{1,0},{2,3},{3,2},{4,5},{5,4},{6,7},{7,6},{8,9},{9,8},{10,11... | collective-permute-start | bytes 1081352 | tf_op jit(solution)/shard_map/ppermute | solution.py:30
  16.9 0.1 shard_map.185.own_ref
  17.1 2.3 %collective-permute-start.1 = (bf16[20,128,128]{2,1,0:T(8,128)(2,1)S(1)}, bf16[20,128,128]{2,1,0:T(8,128)(2,1)S(1)}, u32[]{:S(2)}, u32[]{:S(2)}) collective-permute-start(bf16[20,128,128]{2,1,0:T(8,128)(2,1)S(1)} %shard_map.185.own_ref), channel_id=1, source_target_pairs={{0,1},{1,0},{2,3},{3,2},{4,5},{5,4},{6,7},{7,6},{8,9},{9,8},{10,11... | collective-permute-start | bytes 1966088 | tf_op jit(solution)/shard_map/ppermute | solution.py:30
  19.7 0.8 shard_map.184
  20.6 0.7 reshape.186
  21.3 13.2 %all-to-all-start.1 = ((bf16[16,2,1408]{2,1,0:T(2,128)(2,1)}), bf16[16,2,1408]{2,1,0:T(2,128)(2,1)S(1)}, u32[]{:S(2)}, u32[]{:S(2)}) async-start(bf16[16,2,1408]{2,1,0:T(2,128)(2,1)} %reshape.186), calls=%async_computation.1 | async-start | bytes 180224 | tf_op jit(solution)/shard_map/all_to_all | solution.py:26
  34.5 0.7 copy-done.10
  35.2 11.1 %all-to-all-done.1 = bf16[16,2,1408]{2,1,0:T(2,128)(2,1)S(1)} async-done(((bf16[16,2,1408]{2,1,0:T(2,128)(2,1)}), bf16[16,2,1408]{2,1,0:T(2,128)(2,1)S(1)}, u32[]{:S(2)}, u32[]{:S(2)}) %all-to-all-start.1) | async-done | bytes 90144 | tf_op jit(solution)/shard_map/all_to_all | solution.py:26
  46.3 0.1 convert_reduce_fusion.1
  46.4 0.2 fusion.38
  46.7 0.1 divide_multiply_fusion.1
  46.8 0.1 reshape.187
  46.9 0.1 multiply_exponential_fusion.1
  47.0 0.4 fusion.1
  47.5 0.1 reshape.189
  47.6 0.2 multiply_reduce_fusion.3
  47.9 15.9 %all_to_all.35 = bf16[16,2,512]{2,1,0:T(2,128)(2,1)S(1)} all-to-all(bf16[16,2,512]{2,1,0:T(2,128)(2,1)S(1)} %broadcast_in_dim.27), channel_id=1, replica_groups=mesh['y'=4,'x'=4,'z'=16,'core'=2] {'z'}, dimensions={0} | all-to-all | bytes 65536 | tf_op jit(solution)/shard_map/all_to_all | solution.py:26
  63.8 1.4 %shard_map.186 = bf16[16,2,32,128]{3,2,1,0:T(8,128)(2,1)} custom-call(s32[2]{0:T(128)S(1)} %pad_add_fusion.place_ref, bf16[32,512]{1,0:T(8,128)(2,1)S(1)} %reshape.190.mixed_ref, bf16[20,128,128]{2,1,0:T(8,128)(2,1)S(1)} %shard_map.185.own_ref, bf16[20,128,128]{2,1,0:T(8,128)(2,1)S(1)} %collective-permute-done.1.other_ref), custom_call_target="tpu_custom_call" | custom-call | flops 10000000 | bytes 1000000 | tf_op jit(solution)/shard_map/pallas_call | solution.py:251
  65.3 6.7 %all-to-all-start.3 = ((bf16[16,2,32,128]{3,2,1,0:T(8,128)(2,1)}), bf16[16,2,32,128]{3,2,1,0:T(8,128)(2,1)S(1)}, u32[]{:S(2)}, u32[]{:S(2)}) async-start(bf16[16,2,32,128]{3,2,1,0:T(8,128)(2,1)} %shard_map.186), calls=%async_computation.3 | async-start | bytes 524288 | tf_op jit(solution)/shard_map/all_to_all | solution.py:26
  72.0 7.6 %all-to-all-done.3.arrived_ref = bf16[16,2,32,128]{3,2,1,0:T(8,128)(2,1)S(1)} async-done(((bf16[16,2,32,128]{3,2,1,0:T(8,128)(2,1)}), bf16[16,2,32,128]{3,2,1,0:T(8,128)(2,1)S(1)}, u32[]{:S(2)}, u32[]{:S(2)}) %all-to-all-start.3) | async-done | bytes 262176 | tf_op jit(solution)/shard_map/all_to_all | solution.py:26
  79.7 0.8 shard_map.187
  80.5 0.7 reshape.191
  81.2 3.5 %all-to-all-start.4 = ((bf16[16,2,1408]{2,1,0:T(2,128)(2,1)}), bf16[16,2,1408]{2,1,0:T(2,128)(2,1)S(1)}, u32[]{:S(2)}, u32[]{:S(2)}) async-start(bf16[16,2,1408]{2,1,0:T(2,128)(2,1)} %reshape.191), calls=%async_computation.4 | async-start | bytes 180224 | tf_op jit(solution)/shard_map/all_to_all | solution.py:26
  84.8 11.6 %all-to-all-done.4 = bf16[16,2,1408]{2,1,0:T(2,128)(2,1)S(1)} async-done(((bf16[16,2,1408]{2,1,0:T(2,128)(2,1)}), bf16[16,2,1408]{2,1,0:T(2,128)(2,1)S(1)}, u32[]{:S(2)}, u32[]{:S(2)}) %all-to-all-start.4) | async-done | bytes 90144 | tf_op jit(solution)/shard_map/all_to_all | solution.py:26
  96.4 0.1 convert_reduce_fusion
  96.5 0.2 fusion.39
  96.8 0.1 divide_multiply_fusion
  97.0 0.1 multiply_exponential_fusion
  97.1 0.4 fusion.4
  97.5 0.4 multiply_add_fusion.1
  98.0 0.1 reshape.194
  98.1 0.2 multiply_reduce_fusion.2
  98.4 0.7 broadcast_in_dim.28
  99.0 3.5 %all-to-all-start.5 = ((bf16[16,2,512]{2,1,0:T(2,128)(2,1)}), bf16[16,2,512]{2,1,0:T(2,128)(2,1)S(1)}, u32[]{:S(2)}, u32[]{:S(2)}) async-start(bf16[16,2,512]{2,1,0:T(2,128)(2,1)} %broadcast_in_dim.28), calls=%async_computation.5 | async-start | bytes 65536 | tf_op jit(solution)/shard_map/all_to_all | solution.py:26
  102.6 1.1 pad_maximum_fusion
  103.7 0.6 pad_maximum_fusion.2
  104.3 9.6 %all-to-all-done.5 = bf16[16,2,512]{2,1,0:T(2,128)(2,1)S(1)} async-done(((bf16[16,2,512]{2,1,0:T(2,128)(2,1)}), bf16[16,2,512]{2,1,0:T(2,128)(2,1)S(1)}, u32[]{:S(2)}, u32[]{:S(2)}) %all-to-all-start.5) | async-done | bytes 32800 | tf_op jit(solution)/shard_map/all_to_all | solution.py:26
  114.0 0.7 shard_map.188
  114.7 0.7 pad_maximum_fusion.1
  115.3 9.8 %all-to-all-start.6 = ((bf16[32,4,128]{2,1,0:T(4,128)(2,1)}), bf16[32,4,128]{2,1,0:T(4,128)(2,1)S(1)}, u32[]{:S(2)}, u32[]{:S(2)}) async-start(bf16[32,4,128]{2,1,0:T(4,128)(2,1)} %pad_maximum_fusion.1), calls=%async_computation.6 | async-start | bytes 65536 | tf_op jit(solution)/shard_map/all_to_all | solution.py:26
  125.1 0.6 pad_maximum_fusion.3
  125.7 6.4 %all-to-all-done.6 = bf16[32,4,128]{2,1,0:T(4,128)(2,1)S(1)} async-done(((bf16[32,4,128]{2,1,0:T(4,128)(2,1)}), bf16[32,4,128]{2,1,0:T(4,128)(2,1)S(1)}, u32[]{:S(2)}, u32[]{:S(2)}) %all-to-all-start.6) | async-done | bytes 32800 | tf_op jit(solution)/shard_map/all_to_all | solution.py:26
  132.1 0.6 add_convert_fusion
  (84 shorter events, 1.4 us)
Async XLA Ops:
  0.6 0.7 copy-start.11
  0.6 12.9 %copy-start = (bf16[2,128,512]{2,1,0:T(8,128)(2,1)S(1)}, bf16[2,128,512]{2,1,0:T(8,128)(2,1)}, u32[]{:S(2)}) copy-start(bf16[2,128,512]{2,1,0:T(8,128)(2,1)} %x_ref.3) | copy-start | bytes 786436
  2.0 17.6 %all-to-all-start = ((bf16[32,4,128]{2,1,0:T(4,128)(2,1)}), bf16[32,4,128]{2,1,0:T(4,128)(2,1)S(1)}, u32[]{:S(2)}, u32[]{:S(2)}) async-start(bf16[32,4,128]{2,1,0:T(4,128)(2,1)} %bitcast.10), calls=%async_computation | async-start | bytes 65536 | tf_op jit(solution)/shard_map/all_to_all | solution.py:26
  12.5 1.1 copy-start.2
  13.5 1.0 copy-start.1
  14.5 2.4 %copy-start.3 = (bf16[2,512,128]{2,1,0:T(8,128)(2,1)S(1)}, bf16[2,512,128]{2,1,0:T(8,128)(2,1)}, u32[]{:S(2)}) copy-start(bf16[2,512,128]{2,1,0:T(8,128)(2,1)} %w_ref.1) | copy-start | bytes 786436
  14.5 2.4 %copy-start.4 = (f32[2,128]{1,0:T(2,128)S(1)}, f32[2,128]{1,0:T(2,128)}, u32[]{:S(2)}) copy-start(f32[2,128]{1,0:T(2,128)} %gain_ref.1) | copy-start | bytes 3076
  14.6 5.2 %collective-permute-start = (bf16[11,128,128]{2,1,0:T(8,128)(2,1)S(1)}, bf16[11,128,128]{2,1,0:T(8,128)(2,1)S(1)}, u32[]{:S(2)}, u32[]{:S(2)}) collective-permute-start(bf16[11,128,128]{2,1,0:T(8,128)(2,1)S(1)} %shard_map.183.own_ref), channel_id=1, source_target_pairs={{0,1},{1,0},{2,3},{3,2},{4,5},{5,4},{6,7},{7,6},{8,9},{9,8},{10,11... | collective-permute-start | bytes 1081352 | tf_op jit(solution)/shard_map/ppermute | solution.py:30
  16.9 2.5 %copy-start.7 = (bf16[2,5,512]{2,0,1:T(2,128)(2,1)S(1)}, bf16[2,5,512]{2,0,1:T(2,128)(2,1)}, u32[]{:S(2)}) copy-start(bf16[2,5,512]{2,0,1:T(2,128)(2,1)} %param.22) | copy-start | bytes 30724
  16.9 2.5 %copy-start.8 = (bf16[2,5,2,128]{3,2,1,0:T(2,128)(2,1)S(1)}, bf16[2,5,2,128]{3,2,1,0:T(2,128)(2,1)}, u32[]{:S(2)}) copy-start(bf16[2,5,2,128]{3,2,1,0:T(2,128)(2,1)} %param.23) | copy-start | bytes 15364
  16.9 2.6 %copy-start.12 = (f32[2,8]{1,0:T(2,128)S(1)}, f32[2,8]{1,0:T(2,128)}, u32[]{:S(2)}) copy-start(f32[2,8]{1,0:T(2,128)} %param.25) | copy-start | bytes 196
  16.9 2.6 %copy-start.13 = (f32[2,8]{1,0:T(2,128)S(1)}, f32[2,8]{1,0:T(2,128)}, u32[]{:S(2)}) copy-start(f32[2,8]{1,0:T(2,128)} %param.26) | copy-start | bytes 196
  16.9 2.6 %copy-start.14 = (f32[2,8]{1,0:T(2,128)S(1)}, f32[2,8]{1,0:T(2,128)}, u32[]{:S(2)}) copy-start(f32[2,8]{1,0:T(2,128)} %param.24) | copy-start | bytes 196
  16.9 2.6 %copy-start.6 = (bf16[2,2,4,512]{3,2,1,0:T(4,128)(2,1)S(1)}, bf16[2,2,4,512]{3,2,1,0:T(4,128)(2,1)}, u32[]{:S(2)}) copy-start(bf16[2,2,4,512]{3,2,1,0:T(4,128)(2,1)} %param.30) | copy-start | bytes 49156
  17.0 30.0 %copy-start.5 = (f32[2,2,8,64,128]{4,3,2,1,0:T(8,128)S(1)}, f32[2,2,8,64,128]{4,3,2,1,0:T(8,128)}, u32[]{:S(2)}) copy-start(f32[2,2,8,64,128]{4,3,2,1,0:T(8,128)} %param.29) | copy-start | bytes 3145732
  17.1 46.8 %collective-permute-start.1 = (bf16[20,128,128]{2,1,0:T(8,128)(2,1)S(1)}, bf16[20,128,128]{2,1,0:T(8,128)(2,1)S(1)}, u32[]{:S(2)}, u32[]{:S(2)}) collective-permute-start(bf16[20,128,128]{2,1,0:T(8,128)(2,1)S(1)} %shard_map.185.own_ref), channel_id=1, source_target_pairs={{0,1},{1,0},{2,3},{3,2},{4,5},{5,4},{6,7},{7,6},{8,9},{9,8},{10,11... | collective-permute-start | bytes 1966088 | tf_op jit(solution)/shard_map/ppermute | solution.py:30
  21.3 13.2 %copy-start.9 = (bf16[2,2,4,2,128]{4,3,2,1,0:T(2,128)(2,1)S(1)}, bf16[2,2,4,2,128]{4,3,2,1,0:T(2,128)(2,1)}, u32[]{:S(2)}) copy-start(bf16[2,2,4,2,128]{4,3,2,1,0:T(2,128)(2,1)} %param.31) | copy-start | bytes 24580
  21.3 25.0 %all-to-all-start.1 = ((bf16[16,2,1408]{2,1,0:T(2,128)(2,1)}), bf16[16,2,1408]{2,1,0:T(2,128)(2,1)S(1)}, u32[]{:S(2)}, u32[]{:S(2)}) async-start(bf16[16,2,1408]{2,1,0:T(2,128)(2,1)} %reshape.186), calls=%async_computation.1 | async-start | bytes 180224 | tf_op jit(solution)/shard_map/all_to_all | solution.py:26
  34.5 0.7 copy-start.10
  65.3 14.4 %all-to-all-start.3 = ((bf16[16,2,32,128]{3,2,1,0:T(8,128)(2,1)}), bf16[16,2,32,128]{3,2,1,0:T(8,128)(2,1)S(1)}, u32[]{:S(2)}, u32[]{:S(2)}) async-start(bf16[16,2,32,128]{3,2,1,0:T(8,128)(2,1)} %shard_map.186), calls=%async_computation.3 | async-start | bytes 524288 | tf_op jit(solution)/shard_map/all_to_all | solution.py:26
  81.2 15.2 %all-to-all-start.4 = ((bf16[16,2,1408]{2,1,0:T(2,128)(2,1)}), bf16[16,2,1408]{2,1,0:T(2,128)(2,1)S(1)}, u32[]{:S(2)}, u32[]{:S(2)}) async-start(bf16[16,2,1408]{2,1,0:T(2,128)(2,1)} %reshape.191), calls=%async_computation.4 | async-start | bytes 180224 | tf_op jit(solution)/shard_map/all_to_all | solution.py:26
  99.0 14.9 %all-to-all-start.5 = ((bf16[16,2,512]{2,1,0:T(2,128)(2,1)}), bf16[16,2,512]{2,1,0:T(2,128)(2,1)S(1)}, u32[]{:S(2)}, u32[]{:S(2)}) async-start(bf16[16,2,512]{2,1,0:T(2,128)(2,1)} %broadcast_in_dim.28), calls=%async_computation.5 | async-start | bytes 65536 | tf_op jit(solution)/shard_map/all_to_all | solution.py:26
  115.3 16.7 %all-to-all-start.6 = ((bf16[32,4,128]{2,1,0:T(4,128)(2,1)}), bf16[32,4,128]{2,1,0:T(4,128)(2,1)S(1)}, u32[]{:S(2)}, u32[]{:S(2)}) async-start(bf16[32,4,128]{2,1,0:T(4,128)(2,1)} %pad_maximum_fusion.1), calls=%async_computation.6 | async-start | bytes 65536 | tf_op jit(solution)/shard_map/all_to_all | solution.py:26

commit v3 on v2

--- a/solution.py
+++ b/solution.py
@@ -24,6 +24,13 @@
 
 def exchange(value, axis):
     return lax.all_to_all(value, axis, split_axis=0, concat_axis=0, tiled=True)
+
+
+def exchange_from_middle(value, count):
+    order = [(count // 2 + k) % count for k in range(count)]
+    return lax.all_to_all(
+        value, "z", split_axis=0, concat_axis=0, axis_index_groups=[order], tiled=True
+    )
 
 
 def swap_cores(value):
@@ -54,28 +61,29 @@
     return at
 
 
-def pack_first(x_ref, z_ref, bc_ref, step_ref, out_ref):
-    put_projections(0, x_ref, z_ref, bc_ref, step_ref, out_ref)
-
-
-def pack_rest(x_ref, z_ref, bc_ref, step_ref, w_ref, gain_ref, out_ref):
-    at = put_projections(1, x_ref, z_ref, bc_ref, step_ref, out_ref)
-    for l in range(LAYERS):
-        for k in range(w_ref.shape[1] // LANES):
-            out_ref[at] = w_ref[l, k * LANES : (k + 1) * LANES, :]
-            at += 1
-    gain = gain_ref[1:2, :]
+def put_gain(gain, out_ref, at):
     first = gain.astype(bf16)
     left = gain - first.astype(f32)
     second = left.astype(bf16)
     third = (left - second.astype(f32)).astype(bf16)
     row = lax.broadcasted_iota(jnp.int32, (LANES, LANES), 0)
-    pieces = jnp.where(
-        row == 0,
-        first.astype(f32),
-        jnp.where(row == 1, second.astype(f32), jnp.where(row == 2, third.astype(f32), 0.0)),
-    ).astype(bf16)
-    out_ref[at] = pieces
+    pieces = jnp.where(row == 1, second.astype(f32), jnp.where(row == 2, third.astype(f32), 0.0))
+    out_ref[at] = jnp.where(row == 0, first.astype(f32), pieces).astype(bf16)
+
+
+def pack_first(x_ref, z_ref, bc_ref, step_ref, gain_ref, out_ref):
+    at = put_projections(0, x_ref, z_ref, bc_ref, step_ref, out_ref)
+    put_gain(gain_ref[0:1, :], out_ref, at)
+
+
+def pack_rest(x_ref, z_ref, bc_ref, step_ref, w_ref, gain_ref, out_ref):
+    at = put_projections(1, x_ref, z_ref, bc_ref, step_ref, out_ref)
+    put_gain(gain_ref[1:2, :], out_ref, at)
+    at += 1
+    for l in range(LAYERS):
+        for k in range(w_ref.shape[1] // LANES):
+            out_ref[at] = w_ref[l, k * LANES : (k + 1) * LANES, :]
+            at += 1
 
 
 def project(normed, squares, first, weights, place, out_ref, blocks):
@@ -85,44 +93,55 @@
         term = jnp.dot(rows, block, preferred_element_type=f32)
         total = term if total is None else total + term
     wide = (blocks - 1) * LANES
-    out_ref[:, :wide] = total[:, :wide].astype(bf16)
+    half = total.shape[0] // 2
     lane = lax.broadcasted_iota(jnp.int32, (total.shape[0], LANES), 1)
     tail = pltpu.roll(total[:, wide:], LANES - place, 1)
     tail = jnp.where(lane == first, squares, tail)
-    out_ref[:, wide:] = tail.astype(bf16)
-
-
-def project_first(blocks, heads, place_ref, hidden_ref, normed_ref, own_ref, other_ref, out_ref):
+    for to, rows in ((0, slice(half, None)), (half, slice(0, half))):
+        out_ref[to : to + half, :wide] = total[rows, :wide].astype(bf16)
+        out_ref[to : to + half, wide:] = tail[rows].astype(bf16)
+
+
+def scaled(rows, w_ref, blocks):
+    pieces = w_ref[blocks, :8].astype(f32)
+    gain = pieces[0:1] + pieces[1:2] + pieces[2:3]
+    return (rows.astype(f32) * gain).astype(bf16)
+
+
+def project_first(blocks, heads, place_ref, hidden_ref, own_ref, other_ref, out_ref):
     core = place_ref[1]
-    wide = [hidden_ref[c].astype(f32) for c in range(2)]
+    rows = [hidden_ref[core], hidden_ref[1 - core]]
+    wide = [r.astype(f32) for r in rows]
     squares = jnp.sum(wide[0] * wide[0] + wide[1] * wide[1], axis=1, keepdims=True)
-    normed = [normed_ref[core], normed_ref[1 - core]]
-    project(normed, squares, heads, (own_ref, other_ref), place_ref[0], out_ref, blocks)
+    weights = (own_ref, other_ref)
+    normed = [scaled(r, w, blocks) for r, w in zip(rows, weights)]
+    project(normed, squares, heads, weights, place_ref[0], out_ref, blocks)
 
 
 def project_next(
     blocks, heads, place_ref, arrived_ref, hidden_ref, own_ref, other_ref, out_ref, next_ref
 ):
     core = place_ref[1]
-    wide, normed = [], []
-    last = own_ref.shape[0] - 1
-    for c, w_ref in ((core, own_ref), (1 - core, other_ref)):
+    rows = []
+    weights = (own_ref, other_ref)
+    for c in (core, 1 - core):
         summed = arrived_ref[0, c].astype(f32)
         for j in range(1, arrived_ref.shape[0]):
             summed = summed + arrived_ref[j, c].astype(f32)
         new = (hidden_ref[c].astype(f32) + summed).astype(bf16)
         next_ref[c] = new
-        pieces = w_ref[last].astype(f32)
-        gain = pieces[0:1] + pieces[1:2] + pieces[2:3]
-        wide.append(new.astype(f32))
-        normed.append((new.astype(f32) * gain).astype(bf16))
+        rows.append(new)
+    wide = [r.astype(f32) for r in rows]
     squares = jnp.sum(wide[0] * wide[0] + wide[1] * wide[1], axis=1, keepdims=True)
-    project(normed, squares, heads, (own_ref, other_ref), place_ref[0], out_ref, blocks)
+    normed = [scaled(r, w, blocks) for r, w in zip(rows, weights)]
+    project(normed, squares, heads, weights, place_ref[0], out_ref, blocks)
 
 
 def out_terms(mixed_ref, w_ref, at, blocks):
     weights = jnp.concatenate([w_ref[at + k] for k in range(blocks)], axis=0)
-    return jnp.dot(mixed_ref[...], weights, preferred_element_type=f32).astype(bf16)
+    half = mixed_ref.shape[0] // 2
+    mixed = jnp.concatenate([mixed_ref[half:], mixed_ref[:half]], axis=0)
+    return jnp.dot(mixed, weights, preferred_element_type=f32).astype(bf16)
 
 
 def mix_to_all(at, blocks, place_ref, mixed_ref, own_ref, other_ref, out_ref):
@@ -174,15 +193,14 @@
     place = jnp.stack([tp_index * heads_dev, lax.axis_index("core")]).astype(jnp.int32)
     shape = jax.ShapeDtypeStruct
 
-    normed_own = (stream.astype(f32) * norm_gain[0]).astype(bf16)
-    own = jnp.stack([stream.reshape(2, half, cols_dev), normed_own.reshape(2, half, cols_dev)], 1)
-    own = own.reshape(2, 1, rows_dev, cols_dev)
-    own = jnp.broadcast_to(own, (2, n_tp, rows_dev, cols_dev))
-    rows = exchange(own.reshape(2 * n_tp, rows_dev, cols_dev), CTP)
+    own = jnp.broadcast_to(
+        stream.reshape(2, 1, half, cols_dev), (2, n_tp, half, cols_dev)
+    )
+    rows = exchange(own.reshape(2 * n_tp, half, cols_dev), CTP)
     bc_flat = bc_weight.reshape(LAYERS, cols_dev, bc_width)
     packed = call(
-        pack_first, shape((in_blocks, cols_dev, LANES), bf16), 4, 1000000, 1000000
-    )(x_weight, z_weight, bc_flat, step_weight)
+        pack_first, shape((in_blocks + 1, cols_dev, LANES), bf16), 5, 1000000, 1000000
+    )(x_weight, z_weight, bc_flat, step_weight, norm_gain)
     w_first = (packed, swap_cores(packed))
     packed = call(
         pack_rest, shape((rest, cols_dev, LANES), bf16), 6, 1000000, 1000000
@@ -199,19 +217,17 @@
     hidden = None
     for l in range(LAYERS):
         if l == 0:
-            rows = rows.reshape(2, n_tp, 2, half, cols_dev)
-            hidden = rows[:, :, 0].reshape(2, seqs, cols_dev)
-            normed_in = rows[:, :, 1].reshape(2, seqs, cols_dev)
+            hidden = rows.reshape(2, seqs, cols_dev)
             part = call(
                 functools.partial(project_first, in_blocks, heads_dev),
-                shape((seqs, wide), bf16), 5, 10000000, 1000000, smem=1,
-            )(place, hidden, normed_in, *w_first)
+                shape((seqs, wide), bf16), 4, 10000000, 1000000, smem=1,
+            )(place, hidden, *w_first)
         else:
             part, hidden = call(
                 functools.partial(project_next, in_blocks, heads_dev),
                 (shape((seqs, wide), bf16), shape((2, seqs, cols_dev), bf16)), 5, 10000000, 1000000, smem=1,
             )(place, arrived, hidden, *w_rest)
-        got = exchange(part.reshape(n_z, seq_count, wide), "z")
+        got = exchange_from_middle(part.reshape(n_z, seq_count, wide), n_z)
         got = got.astype(f32).sum(axis=0)
         tail = wide - LANES
         inv_rms = lax.rsqrt(got[:, tail + heads_dev : tail + heads_dev + 1] / MODEL_WIDTH + EPS)
@@ -242,11 +258,11 @@
         normed = grouped * lax.rsqrt(jnp.mean(grouped * grouped, axis=2, keepdims=True) + EPS)
         mixed_rows = (normed.reshape(seq_count, -1) * group_gain[l]).astype(bf16)
         states_list.append(state_new.reshape(seq_count, heads_dev, HEAD_DIM, STATE_DIM))
-        xconv_list.append(jnp.concatenate([conv_x_state[l, :, 1:], proj_x[:, None]], axis=1))
-        bcconv_list.append(jnp.concatenate([conv_bc_state[l, :, 1:], proj_bc[:, None]], axis=1))
-
-        mixed = exchange(to_all(mixed_rows, n_z), "z").reshape(seqs, -1)
-        at = in_blocks + l * out_blocks
+        xconv_list.append(proj_x)
+        bcconv_list.append(proj_bc)
+
+        mixed = exchange_from_middle(to_all(mixed_rows, n_z), n_z).reshape(seqs, -1)
+        at = in_blocks + 1 + l * out_blocks
         if l + 1 < LAYERS:
             terms = call(
                 functools.partial(mix_to_all, at, out_blocks),
@@ -265,7 +281,11 @@
             got = exchange(both, CTP).reshape(2, n_tp, rows_dev, cols_dev).astype(f32)
             result = got[:, :, :half].sum(axis=1) + got[:, 0, half:]
             result = result.astype(bf16).reshape(rows_dev, cols_dev)
-    outs = (jnp.stack(states_list), jnp.stack(xconv_list), jnp.stack(bcconv_list))
+    outs = (
+        jnp.stack(states_list),
+        jnp.concatenate([conv_x_state[:, :, 1:], jnp.stack(xconv_list)[:, :, None]], axis=2),
+        jnp.concatenate([conv_bc_state[:, :, 1:], jnp.stack(bcconv_list)[:, :, None]], axis=2),
+    )
     return (result, *outs)
 
 

time: 133 us -> 127 us (0.955)
  waiting for transfers between devices: 46.4 us -> 15.1 us
  starting transfers between devices: 51.7 us -> 65.2 us
  blocking collectives: 15.9 us -> 27.7 us
    all_to_all x0 -> x3, starting transfers between devices: none -> 40.7 us  [exchange_from_middle(): lax.all_to_all(value, 'z', split_axis=0, concat_axis=0, axis_index_groups...]
    all_to_all x6 -> x2, waiting for transfers between devices: 46.4 us -> 6.35 us  [exchange(): return lax.all_to_all(value, axis, split_axis=0, concat_axis=0, tiled=True)]
    all_to_all x6 -> x2, starting transfers between devices: 47.1 us -> 20 us  [exchange(): return lax.all_to_all(value, axis, split_axis=0, concat_axis=0, tiled=True)]
    all_to_all x0 -> x1, blocking collectives: none -> 13.7 us  [exchange_from_middle(): lax.all_to_all(value, 'z', split_axis=0, concat_axis=0, axis_index_groups...]
    all_to_all x0 -> x3, waiting for transfers between devices: none -> 8.7 us  [exchange_from_middle(): lax.all_to_all(value, 'z', split_axis=0, concat_axis=0, axis_index_groups...]
    all_to_all x1, blocking collectives: 15.9 us -> 14 us  [exchange(): return lax.all_to_all(value, axis, split_axis=0, concat_axis=0, tiled=True)]
    unnamed x30, local copies, waits for them, and re-layouts: 1.67 us -> 3.16 us
  transfers between devices with their start and end apart: 8 -> 7, of which waited for: 5 -> 4; matrix products, arithmetic and copies ran while one was open for 4% -> 5% of each run, Pallas kernels for 1% -> 1%
where the time goes in v3:
time: 127 us; the launch traced here: 126 us
  starting transfers between devices  65.2 us (51%)
  blocking collectives  27.7 us (22%)
  waiting for transfers between devices  15.1 us (12%)
  local copies, waits for them, and re-layouts  7.32 us (6%)
  other arithmetic  6.04 us (5%)
  Pallas kernels  3.24 us (3%)
    all_to_all x3, starting transfers between devices, exchange_from_middle(): lax.all_to_all(value, 'z', split_axis=0, concat_axis=0, axis_index_groups...  40.7 us
    all_to_all x2, starting transfers between devices, exchange(): return lax.all_to_all(value, axis, split_axis=0, concat_axis=0, tiled=True)  20 us
    all_to_all x1, blocking collectives, exchange(): return lax.all_to_all(value, axis, split_axis=0, concat_axis=0, tiled=True)  14 us
    all_to_all x1, blocking collectives, exchange_from_middle(): lax.all_to_all(value, 'z', split_axis=0, concat_axis=0, axis_index_groups...  13.7 us
    all_to_all x3, waiting for transfers between devices, exchange_from_middle(): lax.all_to_all(value, 'z', split_axis=0, concat_axis=0, axis_index_groups...  8.7 us
    all_to_all x2, waiting for transfers between devices, exchange(): return lax.all_to_all(value, axis, split_axis=0, concat_axis=0, tiled=True)  6.35 us
    ppermute x2, starting transfers between devices, swap_cores(): return lax.ppermute(value, 'core', [(0, 1), (1, 0)])  4.46 us
    unnamed x30, local copies, waits for them, and re-layouts  3.16 us
  transfers between devices with their start and end apart: 7, of which 4 were waited for; matrix products, arithmetic and copies ran while one was open for 5% of the time, Pallas kernels for 1%

profile of v3, /device:TPU:1, one launch (start us, length us, event | category | flops | bytes accessed | tf_op | source)
XLA Modules:
  0.0 126.4 jit_solution(421677084290565126)
XLA Ops:
  0.7 0.7 copy-done.11
  1.3 0.6 broadcast_in_dim.26
  1.9 10.4 %all-to-all-start = ((bf16[32,2,128]{2,1,0:T(2,128)(2,1)}), bf16[32,2,128]{2,1,0:T(2,128)(2,1)S(1)}, u32[]{:S(2)}, u32[]{:S(2)}) async-start(bf16[32,2,128]{2,1,0:T(2,128)(2,1)} %bitcast.5), calls=%async_computation | async-start | bytes 32768 | tf_op jit(solution)/shard_map/all_to_all | solution.py:26
  12.4 1.0 reshape.185.bc_ref
  13.4 0.9 copy-done.1
  14.3 0.8 copy-done.2
  15.3 2.2 %collective-permute-start = (bf16[12,128,128]{2,1,0:T(8,128)(2,1)S(1)}, bf16[12,128,128]{2,1,0:T(8,128)(2,1)S(1)}, u32[]{:S(2)}, u32[]{:S(2)}) collective-permute-start(bf16[12,128,128]{2,1,0:T(8,128)(2,1)S(1)} %shard_map.183.own_ref), channel_id=1, source_target_pairs={{0,1},{1,0},{2,3},{3,2},{4,5},{5,4},{6,7},{7,6},{8,9},{9,8},{10,11... | collective-permute-start | bytes 1179656 | tf_op jit(solution)/shard_map/ppermute | solution.py:37
  17.5 0.1 shard_map.185.own_ref
  17.6 2.3 %collective-permute-start.1 = (bf16[20,128,128]{2,1,0:T(8,128)(2,1)S(1)}, bf16[20,128,128]{2,1,0:T(8,128)(2,1)S(1)}, u32[]{:S(2)}, u32[]{:S(2)}) collective-permute-start(bf16[20,128,128]{2,1,0:T(8,128)(2,1)S(1)} %shard_map.185.own_ref), channel_id=1, source_target_pairs={{0,1},{1,0},{2,3},{3,2},{4,5},{5,4},{6,7},{7,6},{8,9},{9,8},{10,11... | collective-permute-start | bytes 1966088 | tf_op jit(solution)/shard_map/ppermute | solution.py:37
  20.1 0.1 pad_add_fusion.place_ref
  20.2 0.8 shard_map.184
  21.1 0.7 reshape.186
  21.7 16.6 %all-to-all-start.1 = ((bf16[16,2,1408]{2,1,0:T(2,128)(2,1)}), bf16[16,2,1408]{2,1,0:T(2,128)(2,1)S(1)}, u32[]{:S(2)}, u32[]{:S(2)}) async-start(bf16[16,2,1408]{2,1,0:T(2,128)(2,1)} %reshape.186), calls=%async_computation.1 | async-start | bytes 180224 | tf_op jit(solution)/shard_map/all_to_all | solution.py:31
  38.4 0.7 copy-done.10
  39.0 4.3 %all-to-all-done.1 = bf16[16,2,1408]{2,1,0:T(2,128)(2,1)S(1)} async-done(((bf16[16,2,1408]{2,1,0:T(2,128)(2,1)}), bf16[16,2,1408]{2,1,0:T(2,128)(2,1)S(1)}, u32[]{:S(2)}, u32[]{:S(2)}) %all-to-all-start.1) | async-done | bytes 90144 | tf_op jit(solution)/shard_map/all_to_all | solution.py:31
  43.4 0.1 convert_reduce_fusion.1
  43.5 0.2 fusion.38
  43.8 0.1 divide_multiply_fusion.1
  44.0 0.1 multiply_exponential_fusion.1
  44.1 0.4 fusion.1
  44.6 0.1 reshape.189
  44.7 0.2 multiply_reduce_fusion.3
  45.0 13.7 %all_to_all.35 = bf16[16,2,512]{2,1,0:T(2,128)(2,1)S(1)} all-to-all(bf16[16,2,512]{2,1,0:T(2,128)(2,1)S(1)} %broadcast_in_dim.27), channel_id=1, replica_groups={{16,18,20,22,24,26,28,30,0,2,4,6,8,10,12,14},{17,19,21,23,25,27,29,31,1..., dimensions={0} | all-to-all | bytes 65536 | tf_op jit(solution)/shard_map/all_to_all | solution.py:31
  58.7 0.7 shard_map.186
  59.5 14.0 %all_to_all.36.arrived_ref = bf16[16,2,32,128]{3,2,1,0:T(8,128)(2,1)S(1)} all-to-all(bf16[16,2,32,128]{3,2,1,0:T(8,128)(2,1)S(1)} %shard_map.186), channel_id=1, replica_groups=mesh['y'=4,'x'=4,'z'=16,'core'=2] {'y','x'}, dimensions={0} | all-to-all | bytes 524288 | tf_op jit(solution)/shard_map/all_to_all | solution.py:26
  73.4 0.8 shard_map.187
  74.3 0.7 reshape.191
  75.0 12.6 %all-to-all-start.4 = ((bf16[16,2,1408]{2,1,0:T(2,128)(2,1)}), bf16[16,2,1408]{2,1,0:T(2,128)(2,1)S(1)}, u32[]{:S(2)}, u32[]{:S(2)}) async-start(bf16[16,2,1408]{2,1,0:T(2,128)(2,1)} %reshape.191), calls=%async_computation.4 | async-start | bytes 180224 | tf_op jit(solution)/shard_map/all_to_all | solution.py:31
  87.6 3.6 %all-to-all-done.4 = bf16[16,2,1408]{2,1,0:T(2,128)(2,1)S(1)} async-done(((bf16[16,2,1408]{2,1,0:T(2,128)(2,1)}), bf16[16,2,1408]{2,1,0:T(2,128)(2,1)S(1)}, u32[]{:S(2)}, u32[]{:S(2)}) %all-to-all-start.4) | async-done | bytes 90144 | tf_op jit(solution)/shard_map/all_to_all | solution.py:31
  91.3 0.1 convert_reduce_fusion
  91.4 0.2 fusion.39
  91.7 0.1 divide_multiply_fusion
  91.9 0.1 multiply_exponential_fusion
  92.0 0.4 fusion.4
  92.4 0.4 multiply_add_fusion.1
  92.9 0.1 reshape.194
  93.0 0.2 multiply_reduce_fusion.2
  93.3 0.6 broadcast_in_dim.28
  93.9 11.5 %all-to-all-start.5 = ((bf16[16,2,512]{2,1,0:T(2,128)(2,1)}), bf16[16,2,512]{2,1,0:T(2,128)(2,1)S(1)}, u32[]{:S(2)}, u32[]{:S(2)}) async-start(bf16[16,2,512]{2,1,0:T(2,128)(2,1)} %broadcast_in_dim.28), calls=%async_computation.5 | async-start | bytes 65536 | tf_op jit(solution)/shard_map/all_to_all | solution.py:31
  105.4 1.0 pad_maximum_fusion
  106.5 0.6 pad_maximum_fusion.2
  107.1 0.7 all-to-all-done.5
  107.9 0.7 shard_map.188
  108.6 0.7 pad_maximum_fusion.1
  109.2 9.6 %all-to-all-start.6 = ((bf16[32,4,128]{2,1,0:T(4,128)(2,1)}), bf16[32,4,128]{2,1,0:T(4,128)(2,1)S(1)}, u32[]{:S(2)}, u32[]{:S(2)}) async-start(bf16[32,4,128]{2,1,0:T(4,128)(2,1)} %pad_maximum_fusion.1), calls=%async_computation.6 | async-start | bytes 65536 | tf_op jit(solution)/shard_map/all_to_all | solution.py:26
  118.8 0.6 pad_maximum_fusion.3
  119.4 6.3 %all-to-all-done.6 = bf16[32,4,128]{2,1,0:T(4,128)(2,1)S(1)} async-done(((bf16[32,4,128]{2,1,0:T(4,128)(2,1)}), bf16[32,4,128]{2,1,0:T(4,128)(2,1)S(1)}, u32[]{:S(2)}, u32[]{:S(2)}) %all-to-all-start.6) | async-done | bytes 32800 | tf_op jit(solution)/shard_map/all_to_all | solution.py:26
  125.8 0.6 add_convert_fusion
  (74 shorter events, 1.3 us)
Async XLA Ops:
  0.6 0.7 copy-start.11
  0.6 12.7 %copy-start = (bf16[2,128,512]{2,1,0:T(8,128)(2,1)S(1)}, bf16[2,128,512]{2,1,0:T(8,128)(2,1)}, u32[]{:S(2)}) copy-start(bf16[2,128,512]{2,1,0:T(8,128)(2,1)} %x_ref.3) | copy-start | bytes 786436
  1.9 18.3 %all-to-all-start = ((bf16[32,2,128]{2,1,0:T(2,128)(2,1)}), bf16[32,2,128]{2,1,0:T(2,128)(2,1)S(1)}, u32[]{:S(2)}, u32[]{:S(2)}) async-start(bf16[32,2,128]{2,1,0:T(2,128)(2,1)} %bitcast.5), calls=%async_computation | async-start | bytes 32768 | tf_op jit(solution)/shard_map/all_to_all | solution.py:26
  12.4 1.0 copy-start.4
  13.4 1.0 copy-start.1
  14.3 0.8 copy-start.2
  15.2 2.3 %copy-start.3 = (bf16[2,512,128]{2,1,0:T(8,128)(2,1)S(1)}, bf16[2,512,128]{2,1,0:T(8,128)(2,1)}, u32[]{:S(2)}) copy-start(bf16[2,512,128]{2,1,0:T(8,128)(2,1)} %w_ref.1) | copy-start | bytes 786436
  15.3 4.7 %copy-start.8 = (bf16[2,5,2,128]{3,2,1,0:T(2,128)(2,1)S(1)}, bf16[2,5,2,128]{3,2,1,0:T(2,128)(2,1)}, u32[]{:S(2)}) copy-start(bf16[2,5,2,128]{3,2,1,0:T(2,128)(2,1)} %param.23) | copy-start | bytes 15364
  15.3 4.9 %collective-permute-start = (bf16[12,128,128]{2,1,0:T(8,128)(2,1)S(1)}, bf16[12,128,128]{2,1,0:T(8,128)(2,1)S(1)}, u32[]{:S(2)}, u32[]{:S(2)}) collective-permute-start(bf16[12,128,128]{2,1,0:T(8,128)(2,1)S(1)} %shard_map.183.own_ref), channel_id=1, source_target_pairs={{0,1},{1,0},{2,3},{3,2},{4,5},{5,4},{6,7},{7,6},{8,9},{9,8},{10,11... | collective-permute-start | bytes 1179656 | tf_op jit(solution)/shard_map/ppermute | solution.py:37
  17.4 2.5 %copy-start.7 = (bf16[2,5,512]{2,0,1:T(2,128)(2,1)S(1)}, bf16[2,5,512]{2,0,1:T(2,128)(2,1)}, u32[]{:S(2)}) copy-start(bf16[2,5,512]{2,0,1:T(2,128)(2,1)} %param.22) | copy-start | bytes 30724
  17.5 2.5 %copy-start.12 = (f32[2,8]{1,0:T(2,128)S(1)}, f32[2,8]{1,0:T(2,128)}, u32[]{:S(2)}) copy-start(f32[2,8]{1,0:T(2,128)} %param.25) | copy-start | bytes 196
  17.5 2.5 %copy-start.13 = (f32[2,8]{1,0:T(2,128)S(1)}, f32[2,8]{1,0:T(2,128)}, u32[]{:S(2)}) copy-start(f32[2,8]{1,0:T(2,128)} %param.26) | copy-start | bytes 196
  17.5 2.6 %copy-start.14 = (f32[2,8]{1,0:T(2,128)S(1)}, f32[2,8]{1,0:T(2,128)}, u32[]{:S(2)}) copy-start(f32[2,8]{1,0:T(2,128)} %param.24) | copy-start | bytes 196
  17.5 2.6 %copy-start.6 = (bf16[2,2,4,512]{3,2,1,0:T(4,128)(2,1)S(1)}, bf16[2,2,4,512]{3,2,1,0:T(4,128)(2,1)}, u32[]{:S(2)}) copy-start(bf16[2,2,4,512]{3,2,1,0:T(4,128)(2,1)} %param.30) | copy-start | bytes 49156
  17.6 26.5 %copy-start.5 = (f32[2,2,8,64,128]{4,3,2,1,0:T(8,128)S(1)}, f32[2,2,8,64,128]{4,3,2,1,0:T(8,128)}, u32[]{:S(2)}) copy-start(f32[2,2,8,64,128]{4,3,2,1,0:T(8,128)} %param.29) | copy-start | bytes 3145732
  17.6 41.1 %collective-permute-start.1 = (bf16[20,128,128]{2,1,0:T(8,128)(2,1)S(1)}, bf16[20,128,128]{2,1,0:T(8,128)(2,1)S(1)}, u32[]{:S(2)}, u32[]{:S(2)}) collective-permute-start(bf16[20,128,128]{2,1,0:T(8,128)(2,1)S(1)} %shard_map.185.own_ref), channel_id=1, source_target_pairs={{0,1},{1,0},{2,3},{3,2},{4,5},{5,4},{6,7},{7,6},{8,9},{9,8},{10,11... | collective-permute-start | bytes 1966088 | tf_op jit(solution)/shard_map/ppermute | solution.py:37
  21.7 16.6 %copy-start.9 = (bf16[2,2,4,2,128]{4,3,2,1,0:T(2,128)(2,1)S(1)}, bf16[2,2,4,2,128]{4,3,2,1,0:T(2,128)(2,1)}, u32[]{:S(2)}) copy-start(bf16[2,2,4,2,128]{4,3,2,1,0:T(2,128)(2,1)} %param.31) | copy-start | bytes 24580
  21.7 21.6 %all-to-all-start.1 = ((bf16[16,2,1408]{2,1,0:T(2,128)(2,1)}), bf16[16,2,1408]{2,1,0:T(2,128)(2,1)S(1)}, u32[]{:S(2)}, u32[]{:S(2)}) async-start(bf16[16,2,1408]{2,1,0:T(2,128)(2,1)} %reshape.186), calls=%async_computation.1 | async-start | bytes 180224 | tf_op jit(solution)/shard_map/all_to_all | solution.py:31
  38.3 0.7 copy-start.10
  75.0 16.3 %all-to-all-start.4 = ((bf16[16,2,1408]{2,1,0:T(2,128)(2,1)}), bf16[16,2,1408]{2,1,0:T(2,128)(2,1)S(1)}, u32[]{:S(2)}, u32[]{:S(2)}) async-start(bf16[16,2,1408]{2,1,0:T(2,128)(2,1)} %reshape.191), calls=%async_computation.4 | async-start | bytes 180224 | tf_op jit(solution)/shard_map/all_to_all | solution.py:31
  93.9 13.9 %all-to-all-start.5 = ((bf16[16,2,512]{2,1,0:T(2,128)(2,1)}), bf16[16,2,512]{2,1,0:T(2,128)(2,1)S(1)}, u32[]{:S(2)}, u32[]{:S(2)}) async-start(bf16[16,2,512]{2,1,0:T(2,128)(2,1)} %broadcast_in_dim.28), calls=%async_computation.5 | async-start | bytes 65536 | tf_op jit(solution)/shard_map/all_to_all | solution.py:31
  109.2 9.6 %slice-start = ((bf16[2,2,4,2,128]{4,3,2,1,0:T(2,128)(2,1)}), bf16[2,2,3,2,128]{4,3,2,1,0:T(2,128)(2,1)S(1)}, s32[]{:S(2)}) async-start(bf16[2,2,4,2,128]{4,3,2,1,0:T(2,128)(2,1)} %param.31), calls=%async_computation.7 | async-start | bytes 12288 | tf_op jit(solution)/shard_map/slice | solution.py:287
  109.2 16.6 %all-to-all-start.6 = ((bf16[32,4,128]{2,1,0:T(4,128)(2,1)}), bf16[32,4,128]{2,1,0:T(4,128)(2,1)S(1)}, u32[]{:S(2)}, u32[]{:S(2)}) async-start(bf16[32,4,128]{2,1,0:T(4,128)(2,1)} %pad_maximum_fusion.1), calls=%async_computation.6 | async-start | bytes 65536 | tf_op jit(solution)/shard_map/all_to_all | solution.py:26

commit v4 on v3

--- a/solution.py
+++ b/solution.py
@@ -18,18 +18,26 @@
 TP = ("y", "x")
 CTP = ("core", "y", "x")
 VMEM = pl.BlockSpec(memory_space=pltpu.VMEM)
-SMEM = pl.BlockSpec(memory_space=pltpu.SMEM)
 f32, bf16 = jnp.float32, jnp.bfloat16
 
 
-def exchange(value, axis):
-    return lax.all_to_all(value, axis, split_axis=0, concat_axis=0, tiled=True)
-
-
-def exchange_from_middle(value, count):
-    order = [(count // 2 + k) % count for k in range(count)]
+def from_middle(count):
+    return [(count // 2 + k) % count for k in range(count)]
+
+
+def exchange_z(value, count):
     return lax.all_to_all(
-        value, "z", split_axis=0, concat_axis=0, axis_index_groups=[order], tiled=True
+        value, "z", split_axis=0, concat_axis=0, axis_index_groups=[from_middle(count)], tiled=True
+    )
+
+
+def exchange_plane(value, axis, sizes):
+    order = [0]
+    for name, size in zip(axis, sizes):
+        inner = from_middle(size) if name != "core" else range(size)
+        order = [at * size + k for at in order for k in inner]
+    return lax.all_to_all(
+        value, axis, split_axis=0, concat_axis=0, axis_index_groups=[order], tiled=True
     )
 
 
@@ -41,11 +49,11 @@
     return jnp.broadcast_to(value, (count, *value.shape))
 
 
-def call(body, out_shape, n_in, flops, size, smem=0):
+def call(body, out_shape, n_in, flops, size):
     return pl.pallas_call(
         body,
         out_shape=out_shape,
-        in_specs=[SMEM] * smem + [VMEM] * (n_in - smem),
+        in_specs=[VMEM] * n_in,
         out_specs=jax.tree.map(lambda _: VMEM, out_shape),
         compiler_params=pltpu.CompilerParams(vmem_limit_bytes=8 * 1024 * 1024),
         cost_estimate=pl.CostEstimate(flops=flops, bytes_accessed=size, transcendentals=0),
@@ -86,42 +94,46 @@
             at += 1
 
 
-def project(normed, squares, first, weights, place, out_ref, blocks):
+def swapped(rows):
+    tiles = [pltpu.roll(rows[k : k + 8], 4, 0) for k in range(0, rows.shape[0], 8)]
+    return jnp.concatenate(tiles, axis=0)
+
+
+def project(normed, squares, first, weights, out_ref, blocks):
     total = None
+    place = (lax.axis_index("y") * lax.axis_size("x") + lax.axis_index("x")) * first
     for rows, w_ref in zip(normed, weights):
         block = jnp.concatenate([w_ref[k] for k in range(blocks)], axis=1)
         term = jnp.dot(rows, block, preferred_element_type=f32)
         total = term if total is None else total + term
     wide = (blocks - 1) * LANES
-    half = total.shape[0] // 2
     lane = lax.broadcasted_iota(jnp.int32, (total.shape[0], LANES), 1)
     tail = pltpu.roll(total[:, wide:], LANES - place, 1)
     tail = jnp.where(lane == first, squares, tail)
-    for to, rows in ((0, slice(half, None)), (half, slice(0, half))):
-        out_ref[to : to + half, :wide] = total[rows, :wide].astype(bf16)
-        out_ref[to : to + half, wide:] = tail[rows].astype(bf16)
+    out_ref[:, :wide] = total[:, :wide].astype(bf16)
+    out_ref[:, wide:] = tail.astype(bf16)
 
 
 def scaled(rows, w_ref, blocks):
     pieces = w_ref[blocks, :8].astype(f32)
     gain = pieces[0:1] + pieces[1:2] + pieces[2:3]
-    return (rows.astype(f32) * gain).astype(bf16)
-
-
-def project_first(blocks, heads, place_ref, hidden_ref, own_ref, other_ref, out_ref):
-    core = place_ref[1]
+    return (rows * gain).astype(bf16)
+
+
+def project_first(blocks, heads, hidden_ref, own_ref, other_ref, out_ref):
+    core = lax.axis_index("core")
     rows = [hidden_ref[core], hidden_ref[1 - core]]
-    wide = [r.astype(f32) for r in rows]
+    wide = [swapped(r.astype(f32)) for r in rows]
     squares = jnp.sum(wide[0] * wide[0] + wide[1] * wide[1], axis=1, keepdims=True)
     weights = (own_ref, other_ref)
-    normed = [scaled(r, w, blocks) for r, w in zip(rows, weights)]
-    project(normed, squares, heads, weights, place_ref[0], out_ref, blocks)
+    normed = [scaled(r, w, blocks) for r, w in zip(wide, weights)]
+    project(normed, squares, heads, weights, out_ref, blocks)
 
 
 def project_next(
-    blocks, heads, place_ref, arrived_ref, hidden_ref, own_ref, other_ref, out_ref, next_ref
+    blocks, heads, arrived_ref, hidden_ref, own_ref, other_ref, out_ref, next_ref
 ):
-    core = place_ref[1]
+    core = lax.axis_index("core")
     rows = []
     weights = (own_ref, other_ref)
     for c in (core, 1 - core):
@@ -131,29 +143,27 @@
         new = (hidden_ref[c].astype(f32) + summed).astype(bf16)
         next_ref[c] = new
         rows.append(new)
-    wide = [r.astype(f32) for r in rows]
+    wide = [swapped(r.astype(f32)) for r in rows]
     squares = jnp.sum(wide[0] * wide[0] + wide[1] * wide[1], axis=1, keepdims=True)
-    normed = [scaled(r, w, blocks) for r, w in zip(rows, weights)]
-    project(normed, squares, heads, weights, place_ref[0], out_ref, blocks)
+    normed = [scaled(r, w, blocks) for r, w in zip(wide, weights)]
+    project(normed, squares, heads, weights, out_ref, blocks)
 
 
 def out_terms(mixed_ref, w_ref, at, blocks):
     weights = jnp.concatenate([w_ref[at + k] for k in range(blocks)], axis=0)
-    half = mixed_ref.shape[0] // 2
-    mixed = jnp.concatenate([mixed_ref[half:], mixed_ref[:half]], axis=0)
-    return jnp.dot(mixed, weights, preferred_element_type=f32).astype(bf16)
-
-
-def mix_to_all(at, blocks, place_ref, mixed_ref, own_ref, other_ref, out_ref):
-    core = place_ref[1]
+    return swapped(jnp.dot(mixed_ref[...], weights, preferred_element_type=f32)).astype(bf16)
+
+
+def mix_to_all(at, blocks, mixed_ref, own_ref, other_ref, out_ref):
+    core = lax.axis_index("core")
     for c, w_ref in ((core, own_ref), (1 - core, other_ref)):
         terms = out_terms(mixed_ref, w_ref, at, blocks)
         for j in range(out_ref.shape[0]):
             out_ref[j, c] = terms
 
 
-def mix_last(at, blocks, place_ref, mixed_ref, own_ref, other_ref, out_ref):
-    core = place_ref[1]
+def mix_last(at, blocks, mixed_ref, own_ref, other_ref, out_ref):
+    core = lax.axis_index("core")
     for c, w_ref in ((core, own_ref), (1 - core, other_ref)):
         out_ref[c] = out_terms(mixed_ref, w_ref, at, blocks)
 
@@ -177,7 +187,7 @@
     conv_bc_state,
 ):
     n_tp, n_z = lax.axis_size(TP), lax.axis_size("z")
-    tp_index = lax.axis_index(TP)
+    plane = tuple(lax.axis_size(name) for name in CTP)
     rows_dev, cols_dev = stream.shape
     half = rows_dev // 2
     seq_count, heads_dev = scan_state.shape[1:3]
@@ -190,13 +200,12 @@
     out_blocks = x_width // LANES
     rest = in_blocks + LAYERS * out_blocks + 1
     wide = in_blocks * LANES
-    place = jnp.stack([tp_index * heads_dev, lax.axis_index("core")]).astype(jnp.int32)
     shape = jax.ShapeDtypeStruct
 
     own = jnp.broadcast_to(
         stream.reshape(2, 1, half, cols_dev), (2, n_tp, half, cols_dev)
     )
-    rows = exchange(own.reshape(2 * n_tp, half, cols_dev), CTP)
+    rows = exchange_plane(own.reshape(2 * n_tp, half, cols_dev), CTP, plane)
     bc_flat = bc_weight.reshape(LAYERS, cols_dev, bc_width)
     packed = call(
         pack_first, shape((in_blocks + 1, cols_dev, LANES), bf16), 5, 1000000, 1000000
@@ -220,14 +229,14 @@
             hidden = rows.reshape(2, seqs, cols_dev)
             part = call(
                 functools.partial(project_first, in_blocks, heads_dev),
-                shape((seqs, wide), bf16), 4, 10000000, 1000000, smem=1,
-            )(place, hidden, *w_first)
+                shape((seqs, wide), bf16), 3, 10000000, 1000000,
+            )(hidden, *w_first)
         else:
             part, hidden = call(
                 functools.partial(project_next, in_blocks, heads_dev),
-                (shape((seqs, wide), bf16), shape((2, seqs, cols_dev), bf16)), 5, 10000000, 1000000, smem=1,
-            )(place, arrived, hidden, *w_rest)
-        got = exchange_from_middle(part.reshape(n_z, seq_count, wide), n_z)
+                (shape((seqs, wide), bf16), shape((2, seqs, cols_dev), bf16)), 4, 10000000, 1000000,
+            )(arrived, hidden, *w_rest)
+        got = exchange_z(part.reshape(n_z, seq_count, wide), n_z)
         got = got.astype(f32).sum(axis=0)
         tail = wide - LANES
         inv_rms = lax.rsqrt(got[:, tail + heads_dev : tail + heads_dev + 1] / MODEL_WIDTH + EPS)
@@ -261,24 +270,24 @@
         xconv_list.append(proj_x)
         bcconv_list.append(proj_bc)
 
-        mixed = exchange_from_middle(to_all(mixed_rows, n_z), n_z).reshape(seqs, -1)
+        mixed = exchange_z(to_all(mixed_rows, n_z), n_z).reshape(seqs, -1)
         at = in_blocks + 1 + l * out_blocks
         if l + 1 < LAYERS:
             terms = call(
                 functools.partial(mix_to_all, at, out_blocks),
-                shape((n_tp, 2, seqs, cols_dev), bf16), 4, 10000000, 1000000, smem=1,
-            )(place, mixed, *w_rest)
-            arrived = exchange(terms, TP)
+                shape((n_tp, 2, seqs, cols_dev), bf16), 3, 10000000, 1000000,
+            )(mixed, *w_rest)
+            arrived = exchange_plane(terms, TP, plane[1:])
         else:
             terms = call(
                 functools.partial(mix_last, at, out_blocks),
-                shape((2, seqs, cols_dev), bf16), 4, 10000000, 1000000, smem=1,
-            )(place, mixed, *w_rest)
+                shape((2, seqs, cols_dev), bf16), 3, 10000000, 1000000,
+            )(mixed, *w_rest)
             both = jnp.concatenate(
                 [terms.reshape(2 * n_tp, half, cols_dev), hidden.reshape(2 * n_tp, half, cols_dev)],
                 axis=1,
             )
-            got = exchange(both, CTP).reshape(2, n_tp, rows_dev, cols_dev).astype(f32)
+            got = exchange_plane(both, CTP, plane).reshape(2, n_tp, rows_dev, cols_dev).astype(f32)
             result = got[:, :, :half].sum(axis=1) + got[:, 0, half:]
             result = result.astype(bf16).reshape(rows_dev, cols_dev)
     outs = (

time: 127 us -> 124 us (0.976)
  waiting for transfers between devices: 15.1 us -> 9.1 us
  starting transfers between devices: 65.2 us -> 69.9 us
  blocking collectives: 27.7 us -> 23.3 us
  local copies, waits for them, and re-layouts: 7.32 us -> 11.1 us
  Pallas kernels: 3.24 us -> 1.07 us
    all_to_all x5, waiting for transfers between devices: 15.1 us -> 9.09 us  [the longest x3 7.44 us: exchange_z(): lax.all_to_all(value, 'z', split_axis=0, concat_axis=0, axis_index_groups...]
    all_to_all x5, starting transfers between devices: 60.7 us -> 65.4 us  [the longest x3 38.9 us: exchange_z(): lax.all_to_all(value, 'z', split_axis=0, concat_axis=0, axis_index_groups...]
    all_to_all x2, blocking collectives: 27.7 us -> 23.3 us  [the longest x1 13.7 us: exchange_z(): lax.all_to_all(value, 'z', split_axis=0, concat_axis=0, axis_index_groups...]
    unnamed x30 -> x44, local copies, waits for them, and re-layouts: 3.16 us -> 5.91 us
  transfers between devices with their start and end apart: 7 -> 7, of which waited for: 4 -> 3; matrix products, arithmetic and copies ran while one was open for 5% -> 6% of each run, Pallas kernels for 1% -> 0%
where the time goes in v4:
time: 124 us; the launch traced here: 123 us
  starting transfers between devices  69.9 us (56%)
  blocking collectives  23.3 us (19%)
  local copies, waits for them, and re-layouts  11.1 us (9%)
  waiting for transfers between devices  9.1 us (7%)
  other arithmetic  6.52 us (5%)
    all_to_all x3, starting transfers between devices, exchange_z(): lax.all_to_all(value, 'z', split_axis=0, concat_axis=0, axis_index_groups...  38.9 us
    all_to_all x2, starting transfers between devices, exchange_plane(): lax.all_to_all(value, axis, split_axis=0, concat_axis=0, axis_index_group...  26.5 us
    all_to_all x1, blocking collectives, exchange_z(): lax.all_to_all(value, 'z', split_axis=0, concat_axis=0, axis_index_groups...  13.7 us
    all_to_all x1, blocking collectives, exchange_plane(): lax.all_to_all(value, axis, split_axis=0, concat_axis=0, axis_index_group...  9.59 us
    all_to_all x3, waiting for transfers between devices, exchange_z(): lax.all_to_all(value, 'z', split_axis=0, concat_axis=0, axis_index_groups...  7.44 us
    unnamed x44, local copies, waits for them, and re-layouts  5.91 us
    ppermute x2, starting transfers between devices, swap_cores(): return lax.ppermute(value, 'core', [(0, 1), (1, 0)])  4.46 us
  transfers between devices with their start and end apart: 7, of which 3 were waited for; matrix products, arithmetic and copies ran while one was open for 6% of the time, Pallas kernels for 0%

profile of v4, /device:TPU:1, one launch (start us, length us, event | category | flops | bytes accessed | tf_op | source)
XLA Modules:
  0.0 122.9 jit_solution(15755388132185383467)
XLA Ops:
  0.7 0.7 copy-done.18
  1.3 0.6 broadcast_in_dim.26
  1.9 13.9 %all-to-all-start = ((bf16[32,2,128]{2,1,0:T(2,128)(2,1)}), bf16[32,2,128]{2,1,0:T(2,128)(2,1)S(1)}, u32[]{:S(2)}, u32[]{:S(2)}) async-start(bf16[32,2,128]{2,1,0:T(2,128)(2,1)} %bitcast.3), calls=%async_computation | async-start | bytes 32768 | tf_op jit(solution)/shard_map/all_to_all | solution.py:39
  15.8 1.0 reshape.185.bc_ref
  16.8 0.9 copy-done.1
  17.8 0.8 copy-done.2
  18.7 2.2 %collective-permute-start = (bf16[12,128,128]{2,1,0:T(8,128)(2,1)S(1)}, bf16[12,128,128]{2,1,0:T(8,128)(2,1)S(1)}, u32[]{:S(2)}, u32[]{:S(2)}) collective-permute-start(bf16[12,128,128]{2,1,0:T(8,128)(2,1)S(1)} %shard_map.183.own_ref), channel_id=1, source_target_pairs={{0,1},{1,0},{2,3},{3,2},{4,5},{5,4},{6,7},{7,6},{8,9},{9,8},{10,11... | collective-permute-start | bytes 1179656 | tf_op jit(solution)/shard_map/ppermute | solution.py:45
  21.1 2.2 %collective-permute-start.1 = (bf16[20,128,128]{2,1,0:T(8,128)(2,1)S(1)}, bf16[20,128,128]{2,1,0:T(8,128)(2,1)S(1)}, u32[]{:S(2)}, u32[]{:S(2)}) collective-permute-start(bf16[20,128,128]{2,1,0:T(8,128)(2,1)S(1)} %shard_map.185.own_ref), channel_id=1, source_target_pairs={{0,1},{1,0},{2,3},{3,2},{4,5},{5,4},{6,7},{7,6},{8,9},{9,8},{10,11... | collective-permute-start | bytes 1966088 | tf_op jit(solution)/shard_map/ppermute | solution.py:45
  23.5 0.5 slice_bitcast_fusion.10
  24.1 0.3 shard_map.184
  24.4 0.7 reshape.186
  25.1 15.0 %all-to-all-start.1 = ((bf16[16,2,1408]{2,1,0:T(2,128)(2,1)}), bf16[16,2,1408]{2,1,0:T(2,128)(2,1)S(1)}, u32[]{:S(2)}, u32[]{:S(2)}) async-start(bf16[16,2,1408]{2,1,0:T(2,128)(2,1)} %reshape.186), calls=%async_computation.1 | async-start | bytes 180224 | tf_op jit(solution)/shard_map/all_to_all | solution.py:29
  40.1 0.7 copy-done.15
  40.8 4.3 %all-to-all-done.1 = bf16[16,2,1408]{2,1,0:T(2,128)(2,1)S(1)} async-done(((bf16[16,2,1408]{2,1,0:T(2,128)(2,1)}), bf16[16,2,1408]{2,1,0:T(2,128)(2,1)S(1)}, u32[]{:S(2)}, u32[]{:S(2)}) %all-to-all-start.1) | async-done | bytes 90144 | tf_op jit(solution)/shard_map/all_to_all | solution.py:29
  45.1 0.1 convert_reduce_fusion.1
  45.2 0.2 fusion.38
  45.5 0.7 divide_multiply_fusion.1
  46.3 0.1 multiply_exponential_fusion.1
  46.4 0.5 copy-done.13
  46.9 0.4 fusion.1
  47.5 0.2 multiply_reduce_fusion.3
  47.8 13.7 %all_to_all.35 = bf16[16,2,512]{2,1,0:T(2,128)(2,1)S(1)} all-to-all(bf16[16,2,512]{2,1,0:T(2,128)(2,1)S(1)} %broadcast_in_dim.27), channel_id=1, replica_groups={{16,18,20,22,24,26,28,30,0,2,4,6,8,10,12,14},{17,19,21,23,25,27,29,31,1..., dimensions={0} | all-to-all | bytes 65536 | tf_op jit(solution)/shard_map/all_to_all | solution.py:29
  61.5 0.2 shard_map.186
  61.7 9.6 %all_to_all.36.arrived_ref = bf16[16,2,32,128]{3,2,1,0:T(8,128)(2,1)S(1)} all-to-all(bf16[16,2,32,128]{3,2,1,0:T(8,128)(2,1)S(1)} %shard_map.186), channel_id=1, replica_groups={{320,352,256,288,448,480,384,416,64,96,0,32,192,224,128,160},{321,353,2..., dimensions={0} | all-to-all | bytes 524288 | tf_op jit(solution)/shard_map/all_to_all | solution.py:39
  71.3 0.3 shard_map.187
  71.6 0.7 reshape.191
  72.3 12.5 %all-to-all-start.4 = ((bf16[16,2,1408]{2,1,0:T(2,128)(2,1)}), bf16[16,2,1408]{2,1,0:T(2,128)(2,1)S(1)}, u32[]{:S(2)}, u32[]{:S(2)}) async-start(bf16[16,2,1408]{2,1,0:T(2,128)(2,1)} %reshape.191), calls=%async_computation.4 | async-start | bytes 180224 | tf_op jit(solution)/shard_map/all_to_all | solution.py:29
  84.8 0.6 stack_reshape.8
  85.3 3.1 %all-to-all-done.4 = bf16[16,2,1408]{2,1,0:T(2,128)(2,1)S(1)} async-done(((bf16[16,2,1408]{2,1,0:T(2,128)(2,1)}), bf16[16,2,1408]{2,1,0:T(2,128)(2,1)S(1)}, u32[]{:S(2)}, u32[]{:S(2)}) %all-to-all-start.4) | async-done | bytes 90144 | tf_op jit(solution)/shard_map/all_to_all | solution.py:29
  88.4 0.1 convert_reduce_fusion
  88.5 0.2 fusion.39
  89.2 0.4 fusion.4
  89.6 0.3 copy-done.12
  89.9 0.4 multiply_add_fusion.1
  90.3 0.6 copy-done.17
  91.1 0.2 multiply_reduce_fusion.2
  91.4 0.6 broadcast_in_dim.28
  92.0 11.5 %all-to-all-start.5 = ((bf16[16,2,512]{2,1,0:T(2,128)(2,1)}), bf16[16,2,512]{2,1,0:T(2,128)(2,1)S(1)}, u32[]{:S(2)}, u32[]{:S(2)}) async-start(bf16[16,2,512]{2,1,0:T(2,128)(2,1)} %broadcast_in_dim.28), calls=%async_computation.5 | async-start | bytes 65536 | tf_op jit(solution)/shard_map/all_to_all | solution.py:29
  103.5 1.0 pad_maximum_fusion
  104.6 0.7 copy-done.10
  105.2 0.6 copy-done.16
  105.9 0.6 pad_maximum_fusion.2
  106.5 0.2 shard_map.188
  106.7 0.7 pad_maximum_fusion.1
  107.4 12.6 %all-to-all-start.6 = ((bf16[32,4,128]{2,1,0:T(4,128)(2,1)}), bf16[32,4,128]{2,1,0:T(4,128)(2,1)S(1)}, u32[]{:S(2)}, u32[]{:S(2)}) async-start(bf16[32,4,128]{2,1,0:T(4,128)(2,1)} %pad_maximum_fusion.1), calls=%async_computation.6 | async-start | bytes 65536 | tf_op jit(solution)/shard_map/all_to_all | solution.py:39
  120.0 0.6 pad_maximum_fusion.3
  120.6 1.6 %all-to-all-done.6 = bf16[32,4,128]{2,1,0:T(4,128)(2,1)S(1)} async-done(((bf16[32,4,128]{2,1,0:T(4,128)(2,1)}), bf16[32,4,128]{2,1,0:T(4,128)(2,1)S(1)}, u32[]{:S(2)}, u32[]{:S(2)}) %all-to-all-start.6) | async-done | bytes 32800 | tf_op jit(solution)/shard_map/all_to_all | solution.py:39
  122.3 0.6 add_convert_fusion
  (87 shorter events, 1.7 us)
Async XLA Ops:
  0.6 0.7 copy-start.18
  0.6 16.2 %copy-start = (bf16[2,128,512]{2,1,0:T(8,128)(2,1)S(1)}, bf16[2,128,512]{2,1,0:T(8,128)(2,1)}, u32[]{:S(2)}) copy-start(bf16[2,128,512]{2,1,0:T(8,128)(2,1)} %x_ref.3) | copy-start | bytes 786436
  1.9 22.2 %all-to-all-start = ((bf16[32,2,128]{2,1,0:T(2,128)(2,1)}), bf16[32,2,128]{2,1,0:T(2,128)(2,1)S(1)}, u32[]{:S(2)}, u32[]{:S(2)}) async-start(bf16[32,2,128]{2,1,0:T(2,128)(2,1)} %bitcast.3), calls=%async_computation | async-start | bytes 32768 | tf_op jit(solution)/shard_map/all_to_all | solution.py:39
  15.8 1.0 copy-start.4
  16.8 1.0 copy-start.1
  17.8 0.8 copy-start.2
  18.6 2.3 %copy-start.3 = (bf16[2,512,128]{2,1,0:T(8,128)(2,1)S(1)}, bf16[2,512,128]{2,1,0:T(8,128)(2,1)}, u32[]{:S(2)}) copy-start(bf16[2,512,128]{2,1,0:T(8,128)(2,1)} %w_ref.1) | copy-start | bytes 786436
  18.7 4.7 %copy-start.8 = (bf16[2,5,2,128]{3,2,1,0:T(2,128)(2,1)S(1)}, bf16[2,5,2,128]{3,2,1,0:T(2,128)(2,1)}, u32[]{:S(2)}) copy-start(bf16[2,5,2,128]{3,2,1,0:T(2,128)(2,1)} %param.23) | copy-start | bytes 15364
  18.7 5.4 %collective-permute-start = (bf16[12,128,128]{2,1,0:T(8,128)(2,1)S(1)}, bf16[12,128,128]{2,1,0:T(8,128)(2,1)S(1)}, u32[]{:S(2)}, u32[]{:S(2)}) collective-permute-start(bf16[12,128,128]{2,1,0:T(8,128)(2,1)S(1)} %shard_map.183.own_ref), channel_id=1, source_target_pairs={{0,1},{1,0},{2,3},{3,2},{4,5},{5,4},{6,7},{7,6},{8,9},{9,8},{10,11... | collective-permute-start | bytes 1179656 | tf_op jit(solution)/shard_map/ppermute | solution.py:45
  21.0 2.4 %copy-start.19 = (f32[2,8]{1,0:T(2,128)S(1)}, f32[2,8]{1,0:T(2,128)}, u32[]{:S(2)}) copy-start(f32[2,8]{1,0:T(2,128)} %param.25) | copy-start | bytes 196
  21.0 2.4 %copy-start.21 = (f32[2,8]{1,0:T(2,128)S(1)}, f32[2,8]{1,0:T(2,128)}, u32[]{:S(2)}) copy-start(f32[2,8]{1,0:T(2,128)} %param.24) | copy-start | bytes 196
  21.0 2.4 %copy-start.20 = (f32[2,8]{1,0:T(2,128)S(1)}, f32[2,8]{1,0:T(2,128)}, u32[]{:S(2)}) copy-start(f32[2,8]{1,0:T(2,128)} %param.26) | copy-start | bytes 196
  21.0 3.0 %copy-start.7 = (bf16[2,5,512]{2,0,1:T(2,128)(2,1)S(1)}, bf16[2,5,512]{2,0,1:T(2,128)(2,1)}, u32[]{:S(2)}) copy-start(bf16[2,5,512]{2,0,1:T(2,128)(2,1)} %param.22) | copy-start | bytes 30724
  21.0 3.0 %copy-start.6 = (bf16[2,2,4,512]{3,2,1,0:T(4,128)(2,1)S(1)}, bf16[2,2,4,512]{3,2,1,0:T(4,128)(2,1)}, u32[]{:S(2)}) copy-start(bf16[2,2,4,512]{3,2,1,0:T(4,128)(2,1)} %param.30) | copy-start | bytes 49156
  21.1 25.8 %copy-start.5 = (f32[2,2,8,64,128]{4,3,2,1,0:T(8,128)S(1)}, f32[2,2,8,64,128]{4,3,2,1,0:T(8,128)}, u32[]{:S(2)}) copy-start(f32[2,2,8,64,128]{4,3,2,1,0:T(8,128)} %param.29) | copy-start | bytes 3145732
  21.1 40.4 %collective-permute-start.1 = (bf16[20,128,128]{2,1,0:T(8,128)(2,1)S(1)}, bf16[20,128,128]{2,1,0:T(8,128)(2,1)S(1)}, u32[]{:S(2)}, u32[]{:S(2)}) collective-permute-start(bf16[20,128,128]{2,1,0:T(8,128)(2,1)S(1)} %shard_map.185.own_ref), channel_id=1, source_target_pairs={{0,1},{1,0},{2,3},{3,2},{4,5},{5,4},{6,7},{7,6},{8,9},{9,8},{10,11... | collective-permute-start | bytes 1966088 | tf_op jit(solution)/shard_map/ppermute | solution.py:45
  25.1 15.0 %copy-start.9 = (bf16[2,2,4,2,128]{4,3,2,1,0:T(2,128)(2,1)S(1)}, bf16[2,2,4,2,128]{4,3,2,1,0:T(2,128)(2,1)}, u32[]{:S(2)}) copy-start(bf16[2,2,4,2,128]{4,3,2,1,0:T(2,128)(2,1)} %param.31) | copy-start | bytes 24580
  25.1 20.0 %all-to-all-start.1 = ((bf16[16,2,1408]{2,1,0:T(2,128)(2,1)}), bf16[16,2,1408]{2,1,0:T(2,128)(2,1)S(1)}, u32[]{:S(2)}, u32[]{:S(2)}) async-start(bf16[16,2,1408]{2,1,0:T(2,128)(2,1)} %reshape.186), calls=%async_computation.1 | async-start | bytes 180224 | tf_op jit(solution)/shard_map/all_to_all | solution.py:29
  40.1 0.7 copy-start.15
  45.5 0.9 copy-start.11
  46.3 0.6 copy-start.13
  72.3 16.1 %all-to-all-start.4 = ((bf16[16,2,1408]{2,1,0:T(2,128)(2,1)}), bf16[16,2,1408]{2,1,0:T(2,128)(2,1)S(1)}, u32[]{:S(2)}, u32[]{:S(2)}) async-start(bf16[16,2,1408]{2,1,0:T(2,128)(2,1)} %reshape.191), calls=%async_computation.4 | async-start | bytes 180224 | tf_op jit(solution)/shard_map/all_to_all | solution.py:29
  89.2 0.7 copy-start.12
  89.2 0.7 copy-start.14
  90.3 0.6 copy-start.17
  92.0 14.5 %all-to-all-start.5 = ((bf16[16,2,512]{2,1,0:T(2,128)(2,1)}), bf16[16,2,512]{2,1,0:T(2,128)(2,1)S(1)}, u32[]{:S(2)}, u32[]{:S(2)}) async-start(bf16[16,2,512]{2,1,0:T(2,128)(2,1)} %broadcast_in_dim.28), calls=%async_computation.5 | async-start | bytes 65536 | tf_op jit(solution)/shard_map/all_to_all | solution.py:29
  104.6 0.7 copy-start.10
  105.2 0.6 copy-start.16
  107.4 12.7 %slice-start = ((bf16[2,2,4,2,128]{4,3,2,1,0:T(2,128)(2,1)}), bf16[2,2,3,2,128]{4,3,2,1,0:T(2,128)(2,1)S(1)}, s32[]{:S(2)}) async-start(bf16[2,2,4,2,128]{4,3,2,1,0:T(2,128)(2,1)} %param.31), calls=%async_computation.7 | async-start | bytes 12288 | tf_op jit(solution)/shard_map/slice | solution.py:296
  107.4 14.9 %all-to-all-start.6 = ((bf16[32,4,128]{2,1,0:T(4,128)(2,1)}), bf16[32,4,128]{2,1,0:T(4,128)(2,1)S(1)}, u32[]{:S(2)}, u32[]{:S(2)}) async-start(bf16[32,4,128]{2,1,0:T(4,128)(2,1)} %pad_maximum_fusion.1), calls=%async_computation.6 | async-start | bytes 65536 | tf_op jit(solution)/shard_map/all_to_all | solution.py:39

commit v5 on v4

--- a/solution.py
+++ b/solution.py
@@ -60,13 +60,36 @@
     )
 
 
-def put_projections(layer, x_ref, z_ref, bc_ref, step_ref, out_ref):
+def projection_copies(layer, x_ref, z_ref, step_ref, out_ref, sems):
+    copies = []
     at = 0
-    for ref in (x_ref, z_ref, bc_ref, step_ref):
+    for ref in (x_ref, z_ref, None, step_ref):
+        if ref is None:
+            at += 2
+            continue
         for k in range(ref.shape[2] // LANES):
-            out_ref[at] = ref[layer, :, k * LANES : (k + 1) * LANES]
+            block = ref.at[layer, :, pl.ds(k * LANES, LANES)]
+            copies.append(pltpu.make_async_copy(block, out_ref.at[at], sems.at[at]))
             at += 1
-    return at
+    return copies, at
+
+
+def fill(layer, copies, x_ref, bc_ref, gain_ref, out_ref, gain_at, bc_buf, gain_buf, sems):
+    last = sems.shape[0] - 1
+    small = [
+        pltpu.make_async_copy(bc_ref.at[layer], bc_buf, sems.at[last - 1]),
+        pltpu.make_async_copy(gain_ref, gain_buf, sems.at[last]),
+    ]
+    for copy in small + copies:
+        copy.start()
+    small[0].wait()
+    at = 2 * (x_ref.shape[2] // LANES)
+    for i in range(2):
+        out_ref[at + i] = bc_buf[:, i, :]
+    small[1].wait()
+    put_gain(gain_buf[layer : layer + 1, :], out_ref, gain_at)
+    for copy in copies:
+        copy.wait()
 
 
 def put_gain(gain, out_ref, at):
@@ -79,19 +102,38 @@
     out_ref[at] = jnp.where(row == 0, first.astype(f32), pieces).astype(bf16)
 
 
-def pack_first(x_ref, z_ref, bc_ref, step_ref, gain_ref, out_ref):
-    at = put_projections(0, x_ref, z_ref, bc_ref, step_ref, out_ref)
-    put_gain(gain_ref[0:1, :], out_ref, at)
-
-
-def pack_rest(x_ref, z_ref, bc_ref, step_ref, w_ref, gain_ref, out_ref):
-    at = put_projections(1, x_ref, z_ref, bc_ref, step_ref, out_ref)
-    put_gain(gain_ref[1:2, :], out_ref, at)
-    at += 1
+def pack_first(x_ref, z_ref, step_ref, bc_ref, gain_ref, out_ref, bc_buf, gain_buf, sems):
+    copies, at = projection_copies(0, x_ref, z_ref, step_ref, out_ref, sems)
+    fill(0, copies, x_ref, bc_ref, gain_ref, out_ref, at, bc_buf, gain_buf, sems)
+
+
+def pack_rest(x_ref, z_ref, step_ref, w_ref, bc_ref, gain_ref, out_ref, bc_buf, gain_buf, sems):
+    copies, gain_at = projection_copies(1, x_ref, z_ref, step_ref, out_ref, sems)
+    at = gain_at + 1
     for l in range(LAYERS):
         for k in range(w_ref.shape[1] // LANES):
-            out_ref[at] = w_ref[l, k * LANES : (k + 1) * LANES, :]
+            block = w_ref.at[l, pl.ds(k * LANES, LANES), :]
+            copies.append(pltpu.make_async_copy(block, out_ref.at[at], sems.at[at]))
             at += 1
+    fill(1, copies, x_ref, bc_ref, gain_ref, out_ref, gain_at, bc_buf, gain_buf, sems)
+
+
+def pack(body, count, *arrays):
+    bc, gain = arrays[-2:]
+    rows = bc.shape[1]
+    return pl.pallas_call(
+        body,
+        out_shape=jax.ShapeDtypeStruct((count, rows, LANES), bf16),
+        in_specs=[pl.BlockSpec(memory_space=pltpu.HBM)] * len(arrays),
+        out_specs=VMEM,
+        scratch_shapes=[
+            pltpu.VMEM(bc.shape[1:], bf16),
+            pltpu.VMEM(gain.shape, f32),
+            pltpu.SemaphoreType.DMA((count + 2,)),
+        ],
+        compiler_params=pltpu.CompilerParams(vmem_limit_bytes=8 * 1024 * 1024),
+        cost_estimate=pl.CostEstimate(flops=1000000, bytes_accessed=1000000, transcendentals=0),
+    )(*(pltpu.with_memory_space_constraint(a, pltpu.HBM) for a in arrays))
 
 
 def swapped(rows):
@@ -206,14 +248,15 @@
         stream.reshape(2, 1, half, cols_dev), (2, n_tp, half, cols_dev)
     )
     rows = exchange_plane(own.reshape(2 * n_tp, half, cols_dev), CTP, plane)
-    bc_flat = bc_weight.reshape(LAYERS, cols_dev, bc_width)
-    packed = call(
-        pack_first, shape((in_blocks + 1, cols_dev, LANES), bf16), 5, 1000000, 1000000
-    )(x_weight, z_weight, bc_flat, step_weight, norm_gain)
+    packed = pack(
+        pack_first, in_blocks + 1,
+        x_weight, z_weight, step_weight, bc_weight, norm_gain,
+    )
     w_first = (packed, swap_cores(packed))
-    packed = call(
-        pack_rest, shape((rest, cols_dev, LANES), bf16), 6, 1000000, 1000000
-    )(x_weight, z_weight, bc_flat, step_weight, out_weight, norm_gain)
+    packed = pack(
+        pack_rest, rest,
+        x_weight, z_weight, step_weight, out_weight, bc_weight, norm_gain,
+    )
     w_rest = (packed, swap_cores(packed))
     x_tap = conv_x_weight.astype(f32)
     bc_tap = conv_bc_weight.astype(f32)

time: 124 us -> 123 us (level)
  local copies, waits for them, and re-layouts: 11.1 us -> 8.33 us
  Pallas kernels: 1.07 us -> 3.39 us
    pallas_call x2, Pallas kernels: 0.16 us -> 2.47 us  [pack(): pl.pallas_call(body, out_shape=jax.ShapeDtypeStruct((count, rows, LANES),...]
    unnamed x44 -> x34, local copies, waits for them, and re-layouts: 5.91 us -> 4.1 us
  transfers between devices with their start and end apart: 7 -> 7, of which waited for: 3 -> 3; matrix products, arithmetic and copies ran while one was open for 6% -> 5% of each run, Pallas kernels for 0% -> 2%
where the time goes in v5:
time: 123 us; the launch traced here: 122 us
  starting transfers between devices  69.9 us (57%)
  blocking collectives  23.3 us (19%)
  waiting for transfers between devices  9.04 us (7%)
  local copies, waits for them, and re-layouts  8.33 us (7%)
  other arithmetic  6.52 us (5%)
  Pallas kernels  3.39 us (3%)
    all_to_all x3, starting transfers between devices, exchange_z(): lax.all_to_all(value, 'z', split_axis=0, concat_axis=0, axis_index_groups...  39 us
    all_to_all x2, starting transfers between devices, exchange_plane(): lax.all_to_all(value, axis, split_axis=0, concat_axis=0, axis_index_group...  26.5 us
    all_to_all x1, blocking collectives, exchange_z(): lax.all_to_all(value, 'z', split_axis=0, concat_axis=0, axis_index_groups...  13.7 us
    all_to_all x1, blocking collectives, exchange_plane(): lax.all_to_all(value, axis, split_axis=0, concat_axis=0, axis_index_group...  9.59 us
    all_to_all x3, waiting for transfers between devices, exchange_z(): lax.all_to_all(value, 'z', split_axis=0, concat_axis=0, axis_index_groups...  7.4 us
    ppermute x2, starting transfers between devices, swap_cores(): return lax.ppermute(value, 'core', [(0, 1), (1, 0)])  4.46 us
    unnamed x34, local copies, waits for them, and re-layouts  4.1 us
    pallas_call x2, Pallas kernels, pack(): pl.pallas_call(body, out_shape=jax.ShapeDtypeStruct((count, rows, LANES),...  2.47 us
  transfers between devices with their start and end apart: 7, of which 3 were waited for; matrix products, arithmetic and copies ran while one was open for 5% of the time, Pallas kernels for 2%

profile of v5, /device:TPU:1, one launch (start us, length us, event | category | flops | bytes accessed | tf_op | source)
XLA Modules:
  0.0 122.3 jit_solution(17634651038726799999)
XLA Ops:
  0.6 0.7 copy-done.13
  1.3 0.6 broadcast_in_dim.26
  1.9 13.9 %all-to-all-start = ((bf16[32,2,128]{2,1,0:T(2,128)(2,1)}), bf16[32,2,128]{2,1,0:T(2,128)(2,1)S(1)}, u32[]{:S(2)}, u32[]{:S(2)}) async-start(bf16[32,2,128]{2,1,0:T(2,128)(2,1)} %bitcast.3), calls=%async_computation | async-start | bytes 32768 | tf_op jit(solution)/shard_map/all_to_all | solution.py:39
  15.8 1.2 shard_map.183.own_ref
  17.0 2.2 %collective-permute-start = (bf16[12,128,128]{2,1,0:T(8,128)(2,1)S(1)}, bf16[12,128,128]{2,1,0:T(8,128)(2,1)S(1)}, u32[]{:S(2)}, u32[]{:S(2)}) collective-permute-start(bf16[12,128,128]{2,1,0:T(8,128)(2,1)S(1)} %shard_map.183.own_ref), channel_id=1, source_target_pairs={{0,1},{1,0},{2,3},{3,2},{4,5},{5,4},{6,7},{7,6},{8,9},{9,8},{10,11... | collective-permute-start | bytes 1179656 | tf_op jit(solution)/shard_map/ppermute | solution.py:45
  19.3 1.3 %shard_map.185.own_ref = bf16[20,128,128]{2,1,0:T(8,128)(2,1)S(1)} custom-call(bf16[2,128,512]{2,1,0:T(8,128)(2,1)} %x_ref.3, bf16[2,128,512]{2,1,0:T(8,128)(2,1)} %z_ref.3, bf16[2,128,128]{2,1,0:T(8,128)(2,1)} %step_ref.3, bf16[2,512,128]{2,1,0:T(8,128)(2,1)} %w_ref.1, bf16[2,128,2,128]{3,2,1,0:T(2,128)(2,1)} %bc_ref.3, f32[2,128]{1,0:T(2,128)} %gain_ref.3), custom_call_target="tpu_custom_call" | custom-call | flops 1000000 | bytes 1000000 | tf_op jit(solution)/shard_map/pallas_call | solution.py:124
  20.6 2.2 %collective-permute-start.1 = (bf16[20,128,128]{2,1,0:T(8,128)(2,1)S(1)}, bf16[20,128,128]{2,1,0:T(8,128)(2,1)S(1)}, u32[]{:S(2)}, u32[]{:S(2)}) collective-permute-start(bf16[20,128,128]{2,1,0:T(8,128)(2,1)S(1)} %shard_map.185.own_ref), channel_id=1, source_target_pairs={{0,1},{1,0},{2,3},{3,2},{4,5},{5,4},{6,7},{7,6},{8,9},{9,8},{10,11... | collective-permute-start | bytes 1966088 | tf_op jit(solution)/shard_map/ppermute | solution.py:45
  22.9 0.5 slice_bitcast_fusion.10
  23.5 0.3 shard_map.184
  23.8 0.7 reshape.182
  24.5 15.0 %all-to-all-start.1 = ((bf16[16,2,1408]{2,1,0:T(2,128)(2,1)}), bf16[16,2,1408]{2,1,0:T(2,128)(2,1)S(1)}, u32[]{:S(2)}, u32[]{:S(2)}) async-start(bf16[16,2,1408]{2,1,0:T(2,128)(2,1)} %reshape.182), calls=%async_computation.1 | async-start | bytes 180224 | tf_op jit(solution)/shard_map/all_to_all | solution.py:29
  39.5 0.7 copy-done.10
  40.2 4.3 %all-to-all-done.1 = bf16[16,2,1408]{2,1,0:T(2,128)(2,1)S(1)} async-done(((bf16[16,2,1408]{2,1,0:T(2,128)(2,1)}), bf16[16,2,1408]{2,1,0:T(2,128)(2,1)S(1)}, u32[]{:S(2)}, u32[]{:S(2)}) %all-to-all-start.1) | async-done | bytes 90144 | tf_op jit(solution)/shard_map/all_to_all | solution.py:29
  44.5 0.1 convert_reduce_fusion.1
  44.6 0.2 fusion.38
  45.0 0.7 divide_multiply_fusion.1
  45.7 0.1 multiply_exponential_fusion.1
  45.9 0.5 copy-done.8
  46.3 0.4 fusion.1
  46.9 0.2 multiply_reduce_fusion.3
  47.2 13.7 %all_to_all.35 = bf16[16,2,512]{2,1,0:T(2,128)(2,1)S(1)} all-to-all(bf16[16,2,512]{2,1,0:T(2,128)(2,1)S(1)} %broadcast_in_dim.27), channel_id=1, replica_groups={{16,18,20,22,24,26,28,30,0,2,4,6,8,10,12,14},{17,19,21,23,25,27,29,31,1..., dimensions={0} | all-to-all | bytes 65536 | tf_op jit(solution)/shard_map/all_to_all | solution.py:29
  60.9 0.2 shard_map.186
  61.1 9.6 %all_to_all.36.arrived_ref = bf16[16,2,32,128]{3,2,1,0:T(8,128)(2,1)S(1)} all-to-all(bf16[16,2,32,128]{3,2,1,0:T(8,128)(2,1)S(1)} %shard_map.186), channel_id=1, replica_groups={{320,352,256,288,448,480,384,416,64,96,0,32,192,224,128,160},{321,353,2..., dimensions={0} | all-to-all | bytes 524288 | tf_op jit(solution)/shard_map/all_to_all | solution.py:39
  70.7 0.3 shard_map.187
  71.0 0.7 reshape.187
  71.7 12.5 %all-to-all-start.4 = ((bf16[16,2,1408]{2,1,0:T(2,128)(2,1)}), bf16[16,2,1408]{2,1,0:T(2,128)(2,1)S(1)}, u32[]{:S(2)}, u32[]{:S(2)}) async-start(bf16[16,2,1408]{2,1,0:T(2,128)(2,1)} %reshape.187), calls=%async_computation.4 | async-start | bytes 180224 | tf_op jit(solution)/shard_map/all_to_all | solution.py:29
  84.2 0.6 stack_reshape.8
  84.8 3.0 %all-to-all-done.4 = bf16[16,2,1408]{2,1,0:T(2,128)(2,1)S(1)} async-done(((bf16[16,2,1408]{2,1,0:T(2,128)(2,1)}), bf16[16,2,1408]{2,1,0:T(2,128)(2,1)S(1)}, u32[]{:S(2)}, u32[]{:S(2)}) %all-to-all-start.4) | async-done | bytes 90144 | tf_op jit(solution)/shard_map/all_to_all | solution.py:29
  87.9 0.1 convert_reduce_fusion
  87.9 0.2 fusion.39
  88.4 0.1 multiply_exponential_fusion
  88.6 0.4 fusion.4
  89.0 0.3 copy-done.7
  89.3 0.4 multiply_add_fusion.1
  89.7 0.6 copy-done.12
  90.5 0.2 multiply_reduce_fusion.2
  90.7 0.6 broadcast_in_dim.28
  91.4 11.5 %all-to-all-start.5 = ((bf16[16,2,512]{2,1,0:T(2,128)(2,1)}), bf16[16,2,512]{2,1,0:T(2,128)(2,1)S(1)}, u32[]{:S(2)}, u32[]{:S(2)}) async-start(bf16[16,2,512]{2,1,0:T(2,128)(2,1)} %broadcast_in_dim.28), calls=%async_computation.5 | async-start | bytes 65536 | tf_op jit(solution)/shard_map/all_to_all | solution.py:29
  102.9 1.0 pad_maximum_fusion
  103.9 0.7 copy-done.5
  104.6 0.7 copy-done.11
  105.3 0.6 pad_maximum_fusion.2
  106.0 0.2 shard_map.188
  106.1 0.7 pad_maximum_fusion.1
  106.8 12.6 %all-to-all-start.6 = ((bf16[32,4,128]{2,1,0:T(4,128)(2,1)}), bf16[32,4,128]{2,1,0:T(4,128)(2,1)S(1)}, u32[]{:S(2)}, u32[]{:S(2)}) async-start(bf16[32,4,128]{2,1,0:T(4,128)(2,1)} %pad_maximum_fusion.1), calls=%async_computation.6 | async-start | bytes 65536 | tf_op jit(solution)/shard_map/all_to_all | solution.py:39
  119.4 0.6 pad_maximum_fusion.3
  120.0 1.6 %all-to-all-done.6 = bf16[32,4,128]{2,1,0:T(4,128)(2,1)S(1)} async-done(((bf16[32,4,128]{2,1,0:T(4,128)(2,1)}), bf16[32,4,128]{2,1,0:T(4,128)(2,1)S(1)}, u32[]{:S(2)}, u32[]{:S(2)}) %all-to-all-start.6) | async-done | bytes 32800 | tf_op jit(solution)/shard_map/all_to_all | solution.py:39
  121.7 0.6 add_convert_fusion
  (76 shorter events, 1.4 us)
Async XLA Ops:
  0.6 0.7 copy-start.13
  1.9 21.6 %all-to-all-start = ((bf16[32,2,128]{2,1,0:T(2,128)(2,1)}), bf16[32,2,128]{2,1,0:T(2,128)(2,1)S(1)}, u32[]{:S(2)}, u32[]{:S(2)}) async-start(bf16[32,2,128]{2,1,0:T(2,128)(2,1)} %bitcast.3), calls=%async_computation | async-start | bytes 32768 | tf_op jit(solution)/shard_map/all_to_all | solution.py:39
  17.0 5.9 %copy-start.3 = (bf16[2,5,2,128]{3,2,1,0:T(2,128)(2,1)S(1)}, bf16[2,5,2,128]{3,2,1,0:T(2,128)(2,1)}, u32[]{:S(2)}) copy-start(bf16[2,5,2,128]{3,2,1,0:T(2,128)(2,1)} %param.23) | copy-start | bytes 15364
  17.0 6.5 %collective-permute-start = (bf16[12,128,128]{2,1,0:T(8,128)(2,1)S(1)}, bf16[12,128,128]{2,1,0:T(8,128)(2,1)S(1)}, u32[]{:S(2)}, u32[]{:S(2)}) collective-permute-start(bf16[12,128,128]{2,1,0:T(8,128)(2,1)S(1)} %shard_map.183.own_ref), channel_id=1, source_target_pairs={{0,1},{1,0},{2,3},{3,2},{4,5},{5,4},{6,7},{7,6},{8,9},{9,8},{10,11... | collective-permute-start | bytes 1179656 | tf_op jit(solution)/shard_map/ppermute | solution.py:45
  19.3 3.6 %copy-start.14 = (f32[2,8]{1,0:T(2,128)S(1)}, f32[2,8]{1,0:T(2,128)}, u32[]{:S(2)}) copy-start(f32[2,8]{1,0:T(2,128)} %param.25) | copy-start | bytes 196
  19.3 3.6 %copy-start.16 = (f32[2,8]{1,0:T(2,128)S(1)}, f32[2,8]{1,0:T(2,128)}, u32[]{:S(2)}) copy-start(f32[2,8]{1,0:T(2,128)} %param.24) | copy-start | bytes 196
  19.3 3.6 %copy-start.15 = (f32[2,8]{1,0:T(2,128)S(1)}, f32[2,8]{1,0:T(2,128)}, u32[]{:S(2)}) copy-start(f32[2,8]{1,0:T(2,128)} %param.26) | copy-start | bytes 196
  19.3 4.1 %copy-start.2 = (bf16[2,5,512]{2,0,1:T(2,128)(2,1)S(1)}, bf16[2,5,512]{2,0,1:T(2,128)(2,1)}, u32[]{:S(2)}) copy-start(bf16[2,5,512]{2,0,1:T(2,128)(2,1)} %param.22) | copy-start | bytes 30724
  19.3 4.2 %copy-start.1 = (bf16[2,2,4,512]{3,2,1,0:T(4,128)(2,1)S(1)}, bf16[2,2,4,512]{3,2,1,0:T(4,128)(2,1)}, u32[]{:S(2)}) copy-start(bf16[2,2,4,512]{3,2,1,0:T(4,128)(2,1)} %param.30) | copy-start | bytes 49156
  20.6 25.7 %copy-start = (f32[2,2,8,64,128]{4,3,2,1,0:T(8,128)S(1)}, f32[2,2,8,64,128]{4,3,2,1,0:T(8,128)}, u32[]{:S(2)}) copy-start(f32[2,2,8,64,128]{4,3,2,1,0:T(8,128)} %param.29) | copy-start | bytes 3145732
  20.6 40.3 %collective-permute-start.1 = (bf16[20,128,128]{2,1,0:T(8,128)(2,1)S(1)}, bf16[20,128,128]{2,1,0:T(8,128)(2,1)S(1)}, u32[]{:S(2)}, u32[]{:S(2)}) collective-permute-start(bf16[20,128,128]{2,1,0:T(8,128)(2,1)S(1)} %shard_map.185.own_ref), channel_id=1, source_target_pairs={{0,1},{1,0},{2,3},{3,2},{4,5},{5,4},{6,7},{7,6},{8,9},{9,8},{10,11... | collective-permute-start | bytes 1966088 | tf_op jit(solution)/shard_map/ppermute | solution.py:45
  24.5 15.0 %copy-start.4 = (bf16[2,2,4,2,128]{4,3,2,1,0:T(2,128)(2,1)S(1)}, bf16[2,2,4,2,128]{4,3,2,1,0:T(2,128)(2,1)}, u32[]{:S(2)}) copy-start(bf16[2,2,4,2,128]{4,3,2,1,0:T(2,128)(2,1)} %param.31) | copy-start | bytes 24580
  24.5 20.0 %all-to-all-start.1 = ((bf16[16,2,1408]{2,1,0:T(2,128)(2,1)}), bf16[16,2,1408]{2,1,0:T(2,128)(2,1)S(1)}, u32[]{:S(2)}, u32[]{:S(2)}) async-start(bf16[16,2,1408]{2,1,0:T(2,128)(2,1)} %reshape.182), calls=%async_computation.1 | async-start | bytes 180224 | tf_op jit(solution)/shard_map/all_to_all | solution.py:29
  39.5 0.7 copy-start.10
  44.9 0.9 copy-start.6
  45.8 0.6 copy-start.8
  71.7 16.1 %all-to-all-start.4 = ((bf16[16,2,1408]{2,1,0:T(2,128)(2,1)}), bf16[16,2,1408]{2,1,0:T(2,128)(2,1)S(1)}, u32[]{:S(2)}, u32[]{:S(2)}) async-start(bf16[16,2,1408]{2,1,0:T(2,128)(2,1)} %reshape.187), calls=%async_computation.4 | async-start | bytes 180224 | tf_op jit(solution)/shard_map/all_to_all | solution.py:29
  88.6 0.7 copy-start.7
  88.6 0.7 copy-start.9
  89.7 0.6 copy-start.12
  91.4 14.6 %all-to-all-start.5 = ((bf16[16,2,512]{2,1,0:T(2,128)(2,1)}), bf16[16,2,512]{2,1,0:T(2,128)(2,1)S(1)}, u32[]{:S(2)}, u32[]{:S(2)}) async-start(bf16[16,2,512]{2,1,0:T(2,128)(2,1)} %broadcast_in_dim.28), calls=%async_computation.5 | async-start | bytes 65536 | tf_op jit(solution)/shard_map/all_to_all | solution.py:29
  103.9 0.7 copy-start.5
  104.6 0.7 copy-start.11
  106.8 12.7 %slice-start = ((bf16[2,2,4,2,128]{4,3,2,1,0:T(2,128)(2,1)}), bf16[2,2,3,2,128]{4,3,2,1,0:T(2,128)(2,1)S(1)}, s32[]{:S(2)}) async-start(bf16[2,2,4,2,128]{4,3,2,1,0:T(2,128)(2,1)} %param.31), calls=%async_computation.7 | async-start | bytes 12288 | tf_op jit(solution)/shard_map/slice | solution.py:339
  106.8 14.9 %all-to-all-start.6 = ((bf16[32,4,128]{2,1,0:T(4,128)(2,1)}), bf16[32,4,128]{2,1,0:T(4,128)(2,1)S(1)}, u32[]{:S(2)}, u32[]{:S(2)}) async-start(bf16[32,4,128]{2,1,0:T(4,128)(2,1)} %pad_maximum_fusion.1), calls=%async_computation.6 | async-start | bytes 65536 | tf_op jit(solution)/shard_map/all_to_all | solution.py:39

commit v6 on v5

--- a/solution.py
+++ b/solution.py
@@ -43,10 +43,6 @@
 
 def swap_cores(value):
     return lax.ppermute(value, "core", [(0, 1), (1, 0)])
-
-
-def to_all(value, count):
-    return jnp.broadcast_to(value, (count, *value.shape))
 
 
 def call(body, out_shape, n_in, flops, size):
@@ -208,6 +204,124 @@
     core = lax.axis_index("core")
     for c, w_ref in ((core, own_ref), (1 - core, other_ref)):
         out_ref[c] = out_terms(mixed_ref, w_ref, at, blocks)
+
+
+def head_spread(values, head_dim, count):
+    lane = lax.broadcasted_iota(jnp.int32, (values.shape[0], LANES), 1)
+    pieces = []
+    for k in range(count // 2):
+        low = jnp.broadcast_to(values[:, 2 * k : 2 * k + 1], lane.shape)
+        high = jnp.broadcast_to(values[:, 2 * k + 1 : 2 * k + 2], lane.shape)
+        pieces.append(jnp.where(lane < head_dim, low, high))
+    return jnp.concatenate(pieces, axis=1)
+
+
+def columns(rows):
+    pad = jnp.zeros((8 - rows.shape[0], rows.shape[1]), f32)
+    return jnp.transpose(jnp.concatenate([rows, pad], axis=0))
+
+
+def silu(v):
+    return v * jax.nn.sigmoid(v)
+
+
+def projected(got_ref):
+    total = got_ref[0].astype(f32)
+    for z in range(1, got_ref.shape[0]):
+        total = total + got_ref[z].astype(f32)
+    return total
+
+
+def scan(layer, total, heads, par_ref, state_ref, proj_done, state_done):
+    width = par_ref.shape[2]
+    seqs = total.shape[0]
+    tail = total[:, total.shape[1] - LANES :]
+    inv = lax.rsqrt(tail[:, heads : heads + 1] / MODEL_WIDTH + EPS)
+    proj = (total[:, : total.shape[1] - LANES] * inv).astype(bf16)
+    proj_done(proj)
+    proj = proj.astype(f32)
+    par = par_ref[layer]
+    inputs_x = silu(par[0:2] + proj[:, :width] * par[2:3])
+    bc_width = proj.shape[1] - 2 * width
+    inputs_bc = silu(par[4:6, :bc_width] + proj[:, 2 * width :] * par[6:7, :bc_width])
+    raw = tail * inv + par[7:8, :LANES]
+    step = jnp.maximum(raw, 0.0) + jnp.log1p(jnp.exp(-jnp.abs(raw)))
+    decay = jnp.exp(-step * par[7:8, LANES : 2 * LANES])
+    u_cols = columns(head_spread(step, HEAD_DIM, heads) * inputs_x)
+    decay_cols = columns(head_spread(decay, HEAD_DIM, heads))
+    skip = head_spread(par[7:8, 2 * LANES : 3 * LANES], HEAD_DIM, heads)
+    row = lax.broadcasted_iota(jnp.int32, (8, STATE_DIM), 0)
+    readouts = []
+    for s in range(seqs):
+        b_row = inputs_bc[s : s + 1, :STATE_DIM]
+        c_row = inputs_bc[s : s + 1, STATE_DIM:]
+        old = state_ref[layer, s].reshape(width, STATE_DIM)
+        new = old * decay_cols[:, s : s + 1] + u_cols[:, s : s + 1] * b_row
+        state_done(s, new.reshape(heads, HEAD_DIM, STATE_DIM))
+        c_high = c_row.astype(bf16).astype(f32)
+        c_rows = jnp.where(row == 0, c_high, jnp.where(row == 1, c_row - c_high, 0.0))
+        out = lax.dot_general(
+            c_rows.astype(bf16), new.astype(bf16), (((1,), (1,)), ((), ())),
+            preferred_element_type=f32,
+        )
+        readouts.append(out[0:1] + out[1:2])
+    readout = jnp.concatenate(readouts, axis=0) + skip * inputs_x
+    gated = readout * silu(proj[:, width : 2 * width])
+    mean = jnp.sum(gated * gated, axis=1, keepdims=True) / width
+    return (gated * lax.rsqrt(mean + EPS) * par[3:4]).astype(bf16)
+
+
+def scan_first(heads, got_ref, par_ref, state_ref, mixed_ref, new_ref, proj_ref):
+    def proj_done(proj):
+        proj_ref[...] = proj
+
+    def state_done(s, new):
+        new_ref[s] = new
+
+    mixed = scan(0, projected(got_ref), heads, par_ref, state_ref, proj_done, state_done)
+    for z in range(mixed_ref.shape[0]):
+        mixed_ref[z] = mixed
+
+
+def scan_last(
+    heads, got_ref, par_ref, state_ref, first_ref, first_proj_ref, conv_x_ref, conv_bc_ref,
+    mixed_ref, state_out, conv_x_out, conv_bc_out, new_buf, x_buf, bc_buf, sems,
+):
+    width = par_ref.shape[2]
+    seqs = got_ref.shape[1]
+    copies = [pltpu.make_async_copy(first_ref, state_out.at[0], sems.at[0])]
+    copies[0].start()
+
+    def proj_done(proj):
+        x_row = lax.broadcasted_iota(jnp.int32, (4, width), 0)
+        bc_row = lax.broadcasted_iota(jnp.int32, (2, STATE_DIM), 0)
+        for l, source in ((0, first_proj_ref[...]), (1, proj)):
+            source = source.astype(f32)
+            for s in range(seqs):
+                old = conv_x_ref[l, s].astype(f32)
+                rows = jnp.where(x_row == 2, old[3:4], source[s : s + 1, :width])
+                rows = jnp.where(x_row == 1, old[2:3], rows)
+                rows = jnp.where(x_row == 0, old[1:2], rows)
+                x_buf[l, s] = rows.astype(bf16)
+                for k in range(3):
+                    bc_buf[l, s, k] = conv_bc_ref[l, s, k + 1]
+                b_row = source[s : s + 1, 2 * width : 2 * width + STATE_DIM]
+                c_row = source[s : s + 1, 2 * width + STATE_DIM :]
+                bc_buf[l, s, 3] = jnp.where(bc_row == 0, b_row, c_row).astype(bf16)
+
+    def state_done(s, new):
+        new_buf[s] = new
+        copies.append(pltpu.make_async_copy(new_buf.at[s], state_out.at[1, s], sems.at[1 + s]))
+        copies[-1].start()
+
+    mixed = scan(1, projected(got_ref), heads, par_ref, state_ref, proj_done, state_done)
+    for buf, out in ((x_buf, conv_x_out), (bc_buf, conv_bc_out)):
+        copies.append(pltpu.make_async_copy(buf, out, sems.at[len(copies)]))
+        copies[-1].start()
+    for z in range(mixed_ref.shape[0]):
+        mixed_ref[z] = mixed
+    for copy in copies:
+        copy.wait()
 
 
 def shards(
@@ -235,8 +349,6 @@
     seq_count, heads_dev = scan_state.shape[1:3]
     x_width = x_weight.shape[2]
     bc_width = 2 * bc_weight.shape[3]
-    groups_dev = conv_bc_state.shape[4] // STATE_DIM
-    per_group = heads_dev // groups_dev
     seqs = n_z * seq_count
     in_blocks = (2 * x_width + bc_width) // LANES + 1
     out_blocks = x_width // LANES
@@ -247,7 +359,7 @@
     own = jnp.broadcast_to(
         stream.reshape(2, 1, half, cols_dev), (2, n_tp, half, cols_dev)
     )
-    rows = exchange_plane(own.reshape(2 * n_tp, half, cols_dev), CTP, plane)
+    hidden = exchange_plane(own.reshape(2 * n_tp, half, cols_dev), CTP, plane)
     packed = pack(
         pack_first, in_blocks + 1,
         x_weight, z_weight, step_weight, bc_weight, norm_gain,
@@ -262,14 +374,26 @@
     bc_tap = conv_bc_weight.astype(f32)
     x_base = jnp.sum(conv_x_state.astype(f32) * x_tap[:, None, :-1], axis=2)
     bc_base = jnp.sum(conv_bc_state.astype(f32) * bc_tap[:, None, :-1], axis=2)
-    rate = jnp.exp(decay_log)
-
-    states_list, xconv_list, bcconv_list = [], [], []
+    by_head = [
+        jnp.pad(v, ((0, 0), (0, LANES - heads_dev)))
+        for v in (step_bias, jnp.exp(decay_log), skip_gain)
+    ]
+    by_head = jnp.concatenate(by_head, axis=1)
+    rows = [
+        x_base,
+        x_tap[:, -1:],
+        group_gain[:, None],
+        bc_base.reshape(LAYERS, seq_count, bc_width),
+        bc_tap[:, -1].reshape(LAYERS, 1, bc_width),
+        by_head[:, None],
+    ]
+    rows = [jnp.pad(r, ((0, 0), (0, 0), (0, x_width - r.shape[2]))) for r in rows]
+    params = jnp.concatenate(rows, axis=1)
+
     result = None
-    hidden = None
     for l in range(LAYERS):
         if l == 0:
-            hidden = rows.reshape(2, seqs, cols_dev)
+            hidden = hidden.reshape(2, seqs, cols_dev)
             part = call(
                 functools.partial(project_first, in_blocks, heads_dev),
                 shape((seqs, wide), bf16), 3, 10000000, 1000000,
@@ -280,40 +404,43 @@
                 (shape((seqs, wide), bf16), shape((2, seqs, cols_dev), bf16)), 4, 10000000, 1000000,
             )(arrived, hidden, *w_rest)
         got = exchange_z(part.reshape(n_z, seq_count, wide), n_z)
-        got = got.astype(f32).sum(axis=0)
-        tail = wide - LANES
-        inv_rms = lax.rsqrt(got[:, tail + heads_dev : tail + heads_dev + 1] / MODEL_WIDTH + EPS)
-        proj_x = (got[:, :x_width] * inv_rms).astype(bf16)
-        proj_z = (got[:, x_width : 2 * x_width] * inv_rms).astype(bf16)
-        proj_bc = (got[:, 2 * x_width : tail] * inv_rms).astype(bf16).reshape(seq_count, 2, -1)
-        step_raw = got[:, tail : tail + heads_dev] * inv_rms
-        inputs_x = jax.nn.silu(x_base[l] + proj_x.astype(f32) * x_tap[l, -1])
-        inputs_bc = jax.nn.silu(bc_base[l] + proj_bc.astype(f32) * bc_tap[l, -1])
-        b_part = inputs_bc[:, 0].reshape(seq_count, groups_dev, STATE_DIM)
-        c_part = inputs_bc[:, 1].reshape(seq_count, groups_dev, STATE_DIM)
-        step_size = jax.nn.softplus(step_raw + step_bias[l])
-        decay_rate = jnp.exp(-step_size * rate[l])
-        heads_x = inputs_x.reshape(seq_count, groups_dev, per_group, HEAD_DIM)
-        step_heads = step_size.reshape(seq_count, groups_dev, per_group)
-        decay_heads = decay_rate.reshape(seq_count, groups_dev, per_group)
-        old_state = scan_state[l].reshape(seq_count, groups_dev, per_group, HEAD_DIM, STATE_DIM)
-        state_new = (
-            old_state * decay_heads[..., None, None]
-            + (step_heads[..., None] * heads_x)[..., None] * b_part[:, :, None, None, :]
-        )
-        readout = jnp.einsum("sgepn,sgn->sgep", state_new, c_part)
-        readout = (
-            readout + skip_gain[l].reshape(groups_dev, per_group)[None, :, :, None] * heads_x
-        )
-        gated_out = readout.reshape(seq_count, -1) * jax.nn.silu(proj_z.astype(f32))
-        grouped = gated_out.reshape(seq_count, groups_dev, -1)
-        normed = grouped * lax.rsqrt(jnp.mean(grouped * grouped, axis=2, keepdims=True) + EPS)
-        mixed_rows = (normed.reshape(seq_count, -1) * group_gain[l]).astype(bf16)
-        states_list.append(state_new.reshape(seq_count, heads_dev, HEAD_DIM, STATE_DIM))
-        xconv_list.append(proj_x)
-        bcconv_list.append(proj_bc)
-
-        mixed = exchange_z(to_all(mixed_rows, n_z), n_z).reshape(seqs, -1)
+        mixed_shape = shape((n_z, seq_count, x_width), bf16)
+        if l == 0:
+            mixed, state_first, proj_first = call(
+                functools.partial(scan_first, heads_dev),
+                (
+                    mixed_shape,
+                    shape(scan_state.shape[1:], f32),
+                    shape((seq_count, wide - LANES), bf16),
+                ),
+                3, 10000000, 1000000,
+            )(got, params, scan_state)
+        else:
+            hbm = pl.BlockSpec(memory_space=pl.ANY)
+            mixed, *outs = pl.pallas_call(
+                functools.partial(scan_last, heads_dev),
+                out_shape=(
+                    mixed_shape,
+                    shape(scan_state.shape, f32),
+                    shape(conv_x_state.shape, bf16),
+                    shape(conv_bc_state.shape, bf16),
+                ),
+                in_specs=[VMEM] * 7,
+                out_specs=(VMEM, hbm, hbm, hbm),
+                scratch_shapes=[
+                    pltpu.VMEM(scan_state.shape[1:], f32),
+                    pltpu.VMEM(conv_x_state.shape, bf16),
+                    pltpu.VMEM(conv_bc_state.shape, bf16),
+                    pltpu.SemaphoreType.DMA((seq_count + 3,)),
+                ],
+                name="scan_last",
+                compiler_params=pltpu.CompilerParams(vmem_limit_bytes=8 * 1024 * 1024),
+                cost_estimate=pl.CostEstimate(
+                    flops=10000000, bytes_accessed=1000000, transcendentals=0
+                ),
+            )(got, params, scan_state, state_first, proj_first, conv_x_state, conv_bc_state)
+
+        mixed = exchange_z(mixed, n_z).reshape(seqs, x_width)
         at = in_blocks + 1 + l * out_blocks
         if l + 1 < LAYERS:
             terms = call(
@@ -333,11 +460,6 @@
             got = exchange_plane(both, CTP, plane).reshape(2, n_tp, rows_dev, cols_dev).astype(f32)
             result = got[:, :, :half].sum(axis=1) + got[:, 0, half:]
             result = result.astype(bf16).reshape(rows_dev, cols_dev)
-    outs = (
-        jnp.stack(states_list),
-        jnp.concatenate([conv_x_state[:, :, 1:], jnp.stack(xconv_list)[:, :, None]], axis=2),
-        jnp.concatenate([conv_bc_state[:, :, 1:], jnp.stack(bcconv_list)[:, :, None]], axis=2),
-    )
     return (result, *outs)
 
 

time: 123 us -> 116 us (0.943)
  blocking collectives: 23.3 us -> 67.2 us
  starting transfers between devices: 69.9 us -> 33.1 us
  other arithmetic: 6.52 us -> 0.71 us
  waiting for transfers between devices: 9.04 us -> 3.55 us
  local copies, waits for them, and re-layouts: 8.33 us -> 3.47 us
  Pallas kernels: 3.39 us -> 5.98 us
    all_to_all x1 -> x3, blocking collectives: 13.7 us -> 42.7 us  [exchange_z(): lax.all_to_all(value, 'z', split_axis=0, concat_axis=0, axis_index_groups...]
    all_to_all x3 -> x1, starting transfers between devices: 39 us -> 14.8 us  [exchange_z(): lax.all_to_all(value, 'z', split_axis=0, concat_axis=0, axis_index_groups...]
    all_to_all x2 -> x1, starting transfers between devices: 26.5 us -> 7.14 us  [exchange_plane(): lax.all_to_all(value, axis, split_axis=0, concat_axis=0, axis_index_group...]
    all_to_all x1 -> x2, blocking collectives: 9.59 us -> 24.5 us  [exchange_plane(): lax.all_to_all(value, axis, split_axis=0, concat_axis=0, axis_index_group...]
    ppermute x2, starting transfers between devices: 4.46 us -> 11.1 us  [swap_cores(): return lax.ppermute(value, 'core', [(0, 1), (1, 0)])]
    all_to_all x3 -> x1, waiting for transfers between devices: 7.4 us -> 3.55 us  [exchange_z(): lax.all_to_all(value, 'z', split_axis=0, concat_axis=0, axis_index_groups...]
    pallas_call x0 -> x2, Pallas kernels: none -> 2.6 us  [the longest x1 1.58 us: shards(): pl.pallas_call(functools.partial(scan_last, heads_dev), out_shape=(mixed_...]
    unnamed x34 -> x22, local copies, waits for them, and re-layouts: 4.1 us -> 1.94 us
  transfers between devices with their start and end apart: 7 -> 4, of which waited for: 3 -> 1; matrix products, arithmetic and copies ran while one was open for 5% -> 1% of each run, Pallas kernels for 2% -> 2%
where the time goes in v6:
time: 116 us; the launch traced here: 115 us
  blocking collectives  67.2 us (58%)
  starting transfers between devices  33.1 us (29%)
  Pallas kernels  5.98 us (5%)
  waiting for transfers between devices  3.55 us (3%)
  local copies, waits for them, and re-layouts  3.47 us (3%)
    all_to_all x3, blocking collectives, exchange_z(): lax.all_to_all(value, 'z', split_axis=0, concat_axis=0, axis_index_groups...  42.7 us
    all_to_all x2, blocking collectives, exchange_plane(): lax.all_to_all(value, axis, split_axis=0, concat_axis=0, axis_index_group...  24.5 us
    all_to_all x1, starting transfers between devices, exchange_z(): lax.all_to_all(value, 'z', split_axis=0, concat_axis=0, axis_index_groups...  14.8 us
    ppermute x2, starting transfers between devices, swap_cores(): return lax.ppermute(value, 'core', [(0, 1), (1, 0)])  11.1 us
    all_to_all x1, starting transfers between devices, exchange_plane(): lax.all_to_all(value, axis, split_axis=0, concat_axis=0, axis_index_group...  7.14 us
    all_to_all x1, waiting for transfers between devices, exchange_z(): lax.all_to_all(value, 'z', split_axis=0, concat_axis=0, axis_index_groups...  3.55 us
    pallas_call x2, Pallas kernels, pack(): pl.pallas_call(body, out_shape=jax.ShapeDtypeStruct((count, rows, LANES),...  2.46 us
  transfers between devices with their start and end apart: 4, of which 1 were waited for; matrix products, arithmetic and copies ran while one was open for 1% of the time, Pallas kernels for 2%

profile of v6, /device:TPU:1, one launch (start us, length us, event | category | flops | bytes accessed | tf_op | source)
XLA Modules:
  0.0 114.9 jit_solution(10637287794049886785)
XLA Ops:
  0.6 1.2 %shard_map.183.own_ref = bf16[12,128,128]{2,1,0:T(8,128)(2,1)S(1)} custom-call(bf16[2,128,512]{2,1,0:T(8,128)(2,1)} %x_ref.3, bf16[2,128,512]{2,1,0:T(8,128)(2,1)} %z_ref.3, bf16[2,128,128]{2,1,0:T(8,128)(2,1)} %step_ref.3, bf16[2,128,2,128]{3,2,1,0:T(2,128)(2,1)} %bc_ref.3, f32[2,128]{1,0:T(2,128)} %gain_ref.3), custom_call_target="tpu_custom_call" | custom-call | flops 1000000 | bytes 1000000 | tf_op jit(solution)/shard_map/pallas_call | solution.py:120
  1.8 0.0 copy-start.7
  1.8 8.7 %collective-permute-start = (bf16[12,128,128]{2,1,0:T(8,128)(2,1)S(1)}, bf16[12,128,128]{2,1,0:T(8,128)(2,1)S(1)}, u32[]{:S(2)}, u32[]{:S(2)}) collective-permute-start(bf16[12,128,128]{2,1,0:T(8,128)(2,1)S(1)} %shard_map.183.own_ref), channel_id=1, source_target_pairs={{0,1},{1,0},{2,3},{3,2},{4,5},{5,4},{6,7},{7,6},{8,9},{9,8},{10,11... | collective-permute-start | bytes 1179656 | tf_op jit(solution)/shard_map/ppermute | solution.py:45
  10.6 0.0 copy-done.7
  10.6 0.6 broadcast_in_dim.16
  11.2 7.1 %all-to-all-start = ((bf16[32,2,128]{2,1,0:T(2,128)(2,1)}), bf16[32,2,128]{2,1,0:T(2,128)(2,1)S(1)}, u32[]{:S(2)}, u32[]{:S(2)}) async-start(bf16[32,2,128]{2,1,0:T(2,128)(2,1)} %bitcast.1), calls=%async_computation | async-start | bytes 32768 | tf_op jit(solution)/shard_map/all_to_all | solution.py:39
  18.4 0.0 copy-start.5
  18.4 0.0 copy-start.4
  18.4 0.0 copy-start.8
  18.4 1.3 %shard_map.186.own_ref = bf16[20,128,128]{2,1,0:T(8,128)(2,1)S(1)} custom-call(bf16[2,128,512]{2,1,0:T(8,128)(2,1)} %x_ref.3, bf16[2,128,512]{2,1,0:T(8,128)(2,1)} %z_ref.3, bf16[2,128,128]{2,1,0:T(8,128)(2,1)} %step_ref.3, bf16[2,512,128]{2,1,0:T(8,128)(2,1)} %w_ref.1, bf16[2,128,2,128]{3,2,1,0:T(2,128)(2,1)} %bc_ref.3, f32[2,128]{1,0:T(2,128)} %gain_ref.3), custom_call_target="tpu_custom_call" | custom-call | flops 1000000 | bytes 1000000 | tf_op jit(solution)/shard_map/pallas_call | solution.py:120
  19.7 0.0 copy-start
  19.7 2.4 %collective-permute-start.1 = (bf16[20,128,128]{2,1,0:T(8,128)(2,1)S(1)}, bf16[20,128,128]{2,1,0:T(8,128)(2,1)S(1)}, u32[]{:S(2)}, u32[]{:S(2)}) collective-permute-start(bf16[20,128,128]{2,1,0:T(8,128)(2,1)S(1)} %shard_map.186.own_ref), channel_id=1, source_target_pairs={{0,1},{1,0},{2,3},{3,2},{4,5},{5,4},{6,7},{7,6},{8,9},{9,8},{10,11... | collective-permute-start | bytes 1966088 | tf_op jit(solution)/shard_map/ppermute | solution.py:45
  22.1 0.0 copy-done.5
  22.1 0.0 copy-done.4
  22.1 0.0 copy-start.3
  22.2 0.6 copy-done.3
  22.7 0.0 copy-done.8
  22.7 0.0 all-to-all-done
  22.7 0.0 collective-permute-done.other_ref
  22.8 0.3 shard_map.184
  23.0 0.7 reshape.47
  23.7 0.0 copy-start.9
  23.7 0.0 copy-start.10
  23.7 14.8 %all-to-all-start.1 = ((bf16[16,2,1408]{2,1,0:T(2,128)(2,1)}), bf16[16,2,1408]{2,1,0:T(2,128)(2,1)S(1)}, u32[]{:S(2)}, u32[]{:S(2)}) async-start(bf16[16,2,1408]{2,1,0:T(2,128)(2,1)} %reshape.47), calls=%async_computation.1 | async-start | bytes 180224 | tf_op jit(solution)/shard_map/all_to_all | solution.py:29
  38.5 0.0 copy-done.9
  38.5 0.0 copy-done.10
  38.6 0.0 copy-start.6
  38.6 0.0 copy-start.2
  38.6 0.6 copy-done.6
  39.3 0.0 copy-done.2
  39.4 0.7 copy-done.1
  40.0 0.0 slice-done
  40.1 0.1 concatenate.10.par_ref
  40.1 3.5 %all-to-all-done.1.got_ref = bf16[16,2,1408]{2,1,0:T(2,128)(2,1)S(1)} async-done(((bf16[16,2,1408]{2,1,0:T(2,128)(2,1)}), bf16[16,2,1408]{2,1,0:T(2,128)(2,1)S(1)}, u32[]{:S(2)}, u32[]{:S(2)}) %all-to-all-start.1) | async-done | bytes 90144 | tf_op jit(solution)/shard_map/all_to_all | solution.py:29
  43.7 0.0 copy-done
  43.7 1.0 shard_map.185
  44.7 13.7 %all_to_all.35 = bf16[16,2,512]{2,1,0:T(2,128)(2,1)S(1)} all-to-all(bf16[16,2,512]{2,1,0:T(2,128)(2,1)S(1)} %get-tuple-element.13), channel_id=1, replica_groups={{16,18,20,22,24,26,28,30,0,2,4,6,8,10,12,14},{17,19,21,23,25,27,29,31,1..., dimensions={0} | all-to-all | bytes 65536 | tf_op jit(solution)/shard_map/all_to_all | solution.py:29
  58.4 0.0 collective-permute-done.1.other_ref
  58.4 0.2 shard_map.187
  58.6 9.6 %all_to_all.36.arrived_ref = bf16[16,2,32,128]{3,2,1,0:T(8,128)(2,1)S(1)} all-to-all(bf16[16,2,32,128]{3,2,1,0:T(8,128)(2,1)S(1)} %shard_map.187), channel_id=1, replica_groups={{320,352,256,288,448,480,384,416,64,96,0,32,192,224,128,160},{321,353,2..., dimensions={0} | all-to-all | bytes 524288 | tf_op jit(solution)/shard_map/all_to_all | solution.py:39
  68.2 0.3 shard_map.188
  68.6 15.3 %all_to_all.37.got_ref = bf16[16,2,1408]{2,1,0:T(2,128)(2,1)S(1)} all-to-all(bf16[16,2,1408]{2,1,0:T(2,128)(2,1)S(1)} %reshape.50), channel_id=1, replica_groups={{16,18,20,22,24,26,28,30,0,2,4,6,8,10,12,14},{17,19,21,23,25,27,29,31,1..., dimensions={0} | all-to-all | bytes 180224 | tf_op jit(solution)/shard_map/all_to_all | solution.py:29
  83.8 1.6 %scan_last.1 = (bf16[16,2,512]{2,1,0:T(2,128)(2,1)S(1)}, f32[2,2,8,64,128]{4,3,2,1,0:T(8,128)}, bf16[2,2,4,512]{3,2,1,0:T(4,128)(2,1)}, bf16[2,2,4,2,128]{4,3,2,1,0:T(2,128)(2,1)}) custom-call(bf16[16,2,1408]{2,1,0:T(2,128)(2,1)S(1)} %all_to_all.37.got_ref, f32[2,8,512]{2,1,0:T(8,128)S(1)} %concatenate.10.par_ref, f32[2,2,8,64,128]{4,3,2,1,0:T(8,128)S(1)} %copy-done, ...), custom_call_target="tpu_custom_call" | custom-call | flops 10000000 | bytes 1000000 | tf_op jit(solution)/shard_map/scan_last/pallas_call | solution.py:420
  85.4 13.7 %all_to_all.38 = bf16[16,2,512]{2,1,0:T(2,128)(2,1)S(1)} all-to-all(bf16[16,2,512]{2,1,0:T(2,128)(2,1)S(1)} %get-tuple-element.17), channel_id=1, replica_groups={{16,18,20,22,24,26,28,30,0,2,4,6,8,10,12,14},{17,19,21,23,25,27,29,31,1..., dimensions={0} | all-to-all | bytes 65536 | tf_op jit(solution)/shard_map/all_to_all | solution.py:29
  99.1 0.2 shard_map.189
  99.3 0.1 pad_maximum_fusion
  99.3 14.9 %all_to_all.39 = bf16[32,4,128]{2,1,0:T(4,128)(2,1)S(1)} all-to-all(bf16[32,4,128]{2,1,0:T(4,128)(2,1)S(1)} %pad_maximum_fusion), channel_id=1, replica_groups={{320,352,256,288,448,480,384,416,64,96,0,32,192,224,128,160,321,353,257..., dimensions={0} | all-to-all | bytes 65536 | tf_op jit(solution)/shard_map/all_to_all | solution.py:39
  114.3 0.6 add_convert_fusion
  (22 shorter events, 0.3 us)
Async XLA Ops:
  1.8 8.8 %copy-start.7 = (bf16[4,128]{1,0:T(4,128)(2,1)S(1)}, bf16[4,128]{1,0:T(4,128)(2,1)}, u32[]{:S(2)}) copy-start(bf16[4,128]{1,0:T(4,128)(2,1)} %param.16) | copy-start | bytes 3076
  1.8 20.9 %collective-permute-start = (bf16[12,128,128]{2,1,0:T(8,128)(2,1)S(1)}, bf16[12,128,128]{2,1,0:T(8,128)(2,1)S(1)}, u32[]{:S(2)}, u32[]{:S(2)}) collective-permute-start(bf16[12,128,128]{2,1,0:T(8,128)(2,1)S(1)} %shard_map.183.own_ref), channel_id=1, source_target_pairs={{0,1},{1,0},{2,3},{3,2},{4,5},{5,4},{6,7},{7,6},{8,9},{9,8},{10,11... | collective-permute-start | bytes 1179656 | tf_op jit(solution)/shard_map/ppermute | solution.py:45
  11.2 11.5 %all-to-all-start = ((bf16[32,2,128]{2,1,0:T(2,128)(2,1)}), bf16[32,2,128]{2,1,0:T(2,128)(2,1)S(1)}, u32[]{:S(2)}, u32[]{:S(2)}) async-start(bf16[32,2,128]{2,1,0:T(2,128)(2,1)} %bitcast.1), calls=%async_computation | async-start | bytes 32768 | tf_op jit(solution)/shard_map/all_to_all | solution.py:39
  18.4 3.7 %copy-start.5 = (bf16[2,5,512]{2,0,1:T(2,128)(2,1)S(1)}, bf16[2,5,512]{2,0,1:T(2,128)(2,1)}, u32[]{:S(2)}) copy-start(bf16[2,5,512]{2,0,1:T(2,128)(2,1)} %param.22) | copy-start | bytes 30724
  18.4 3.7 %copy-start.4 = (bf16[2,5,2,128]{3,2,1,0:T(2,128)(2,1)S(1)}, bf16[2,5,2,128]{3,2,1,0:T(2,128)(2,1)}, u32[]{:S(2)}) copy-start(bf16[2,5,2,128]{3,2,1,0:T(2,128)(2,1)} %param.23) | copy-start | bytes 15364
  18.4 4.3 %copy-start.8 = (f32[2,8]{1,0:T(2,128)S(1)}, f32[2,8]{1,0:T(2,128)}, u32[]{:S(2)}) copy-start(f32[2,8]{1,0:T(2,128)} %param.25) | copy-start | bytes 196
  19.7 24.0 %copy-start = (f32[2,2,8,64,128]{4,3,2,1,0:T(8,128)S(1)}, f32[2,2,8,64,128]{4,3,2,1,0:T(8,128)}, u32[]{:S(2)}) copy-start(f32[2,2,8,64,128]{4,3,2,1,0:T(8,128)} %state_ref.3) | copy-start | bytes 3145732
  19.7 38.7 %collective-permute-start.1 = (bf16[20,128,128]{2,1,0:T(8,128)(2,1)S(1)}, bf16[20,128,128]{2,1,0:T(8,128)(2,1)S(1)}, u32[]{:S(2)}, u32[]{:S(2)}) collective-permute-start(bf16[20,128,128]{2,1,0:T(8,128)(2,1)S(1)} %shard_map.186.own_ref), channel_id=1, source_target_pairs={{0,1},{1,0},{2,3},{3,2},{4,5},{5,4},{6,7},{7,6},{8,9},{9,8},{10,11... | collective-permute-start | bytes 1966088 | tf_op jit(solution)/shard_map/ppermute | solution.py:45
  22.1 0.6 copy-start.3
  23.7 14.8 %copy-start.9 = (f32[2,8]{1,0:T(2,128)S(1)}, f32[2,8]{1,0:T(2,128)}, u32[]{:S(2)}) copy-start(f32[2,8]{1,0:T(2,128)} %param.26) | copy-start | bytes 196
  23.7 14.8 %copy-start.10 = (f32[2,8]{1,0:T(2,128)S(1)}, f32[2,8]{1,0:T(2,128)}, u32[]{:S(2)}) copy-start(f32[2,8]{1,0:T(2,128)} %param.24) | copy-start | bytes 196
  23.7 19.9 %all-to-all-start.1 = ((bf16[16,2,1408]{2,1,0:T(2,128)(2,1)}), bf16[16,2,1408]{2,1,0:T(2,128)(2,1)S(1)}, u32[]{:S(2)}, u32[]{:S(2)}) async-start(bf16[16,2,1408]{2,1,0:T(2,128)(2,1)} %reshape.47), calls=%async_computation.1 | async-start | bytes 180224 | tf_op jit(solution)/shard_map/all_to_all | solution.py:29
  38.6 0.7 copy-start.6
  38.6 0.7 copy-start.2
  39.3 0.7 copy-start.1
  39.3 0.7 slice-start

commit v7 on v6

--- a/solution.py
+++ b/solution.py
@@ -70,14 +70,18 @@
     return copies, at
 
 
-def fill(layer, copies, x_ref, bc_ref, gain_ref, out_ref, gain_at, bc_buf, gain_buf, sems):
+def start_small(layer, bc_ref, gain_ref, bc_buf, gain_buf, sems):
     last = sems.shape[0] - 1
     small = [
         pltpu.make_async_copy(bc_ref.at[layer], bc_buf, sems.at[last - 1]),
         pltpu.make_async_copy(gain_ref, gain_buf, sems.at[last]),
     ]
-    for copy in small + copies:
+    for copy in small:
         copy.start()
+    return small
+
+
+def finish(layer, small, copies, x_ref, out_ref, gain_at, bc_buf, gain_buf):
     small[0].wait()
     at = 2 * (x_ref.shape[2] // LANES)
     for i in range(2):
@@ -98,12 +102,41 @@
     out_ref[at] = jnp.where(row == 0, first.astype(f32), pieces).astype(bf16)
 
 
-def pack_first(x_ref, z_ref, step_ref, bc_ref, gain_ref, out_ref, bc_buf, gain_buf, sems):
+def enter(
+    stream_ref, x_ref, z_ref, step_ref, bc_ref, gain_ref,
+    own_out, out_ref, stream_buf, own_buf, bc_buf, gain_buf, sems,
+):
     copies, at = projection_copies(0, x_ref, z_ref, step_ref, out_ref, sems)
-    fill(0, copies, x_ref, bc_ref, gain_ref, out_ref, at, bc_buf, gain_buf, sems)
-
-
-def pack_rest(x_ref, z_ref, step_ref, w_ref, bc_ref, gain_ref, out_ref, bc_buf, gain_buf, sems):
+    count = sems.shape[0]
+    into = pltpu.make_async_copy(stream_ref, stream_buf, sems.at[count - 4])
+    into.start()
+    small = start_small(0, bc_ref, gain_ref, bc_buf, gain_buf, sems)
+    for copy in copies:
+        copy.start()
+    into.wait()
+    half = own_buf.shape[1]
+    each = own_buf.shape[0] // 2
+    for c in range(2):
+        rows = stream_buf[c * half : (c + 1) * half]
+        for p in range(each):
+            own_buf[c * each + p] = rows
+    out = pltpu.make_async_copy(own_buf, own_out, sems.at[count - 3])
+    out.start()
+    finish(0, small, copies + [out], x_ref, out_ref, at, bc_buf, gain_buf)
+
+
+def pack_rest(
+    x_ref, z_ref, step_ref, w_ref, bc_ref, gain_ref,
+    tap_x_ref, tap_bc_ref, bias_ref, decay_ref, skip_ref, group_ref, conv_x_ref, conv_bc_ref,
+    out_ref, par_ref, bc_buf, gain_buf,
+    tap_x, tap_bc, bias, decay, skip, group, conv_x, conv_bc, sems, par_sems,
+):
+    sources = (tap_x_ref, tap_bc_ref, bias_ref, decay_ref, skip_ref, group_ref)
+    sources += (conv_x_ref, conv_bc_ref)
+    bufs = (tap_x, tap_bc, bias, decay, skip, group, conv_x, conv_bc)
+    loads = [
+        pltpu.make_async_copy(a, b, par_sems.at[k]) for k, (a, b) in enumerate(zip(sources, bufs))
+    ]
     copies, gain_at = projection_copies(1, x_ref, z_ref, step_ref, out_ref, sems)
     at = gain_at + 1
     for l in range(LAYERS):
@@ -111,22 +144,46 @@
             block = w_ref.at[l, pl.ds(k * LANES, LANES), :]
             copies.append(pltpu.make_async_copy(block, out_ref.at[at], sems.at[at]))
             at += 1
-    fill(1, copies, x_ref, bc_ref, gain_ref, out_ref, gain_at, bc_buf, gain_buf, sems)
-
-
-def pack(body, count, *arrays):
-    bc, gain = arrays[-2:]
-    rows = bc.shape[1]
+    for copy in loads:
+        copy.start()
+    small = start_small(1, bc_ref, gain_ref, bc_buf, gain_buf, sems)
+    for copy in copies:
+        copy.start()
+    for copy in loads:
+        copy.wait()
+    heads = bias.shape[1]
+    seqs = conv_x.shape[1]
+    taps = tap_x.shape[0] - 1
+    par_ref[...] = jnp.zeros(par_ref.shape, f32)
+    for l in range(LAYERS):
+        for s in range(seqs):
+            old = conv_x[l, s].astype(f32)
+            base = jnp.zeros((1, old.shape[1]), f32)
+            pair = jnp.zeros((2, LANES), f32)
+            for k in range(taps):
+                base = base + old[k : k + 1] * tap_x[k].astype(f32)[l : l + 1]
+                pair = pair + conv_bc[l, s, k].astype(f32) * tap_bc[l, k].astype(f32)
+            par_ref[l, s : s + 1, :] = base
+            par_ref[l, 4 + s : 5 + s, :LANES] = pair[0:1]
+            par_ref[l, 4 + s : 5 + s, LANES : 2 * LANES] = pair[1:2]
+        last = tap_bc[l, taps].astype(f32)
+        par_ref[l, 2:3, :] = tap_x[taps].astype(f32)[l : l + 1]
+        par_ref[l, 3:4, :] = group[l : l + 1, :]
+        par_ref[l, 6:7, :LANES] = last[0:1]
+        par_ref[l, 6:7, LANES : 2 * LANES] = last[1:2]
+        par_ref[l, 7:8, :heads] = bias[l : l + 1, :]
+        par_ref[l, 7:8, LANES : LANES + heads] = jnp.exp(decay[l : l + 1, :])
+        par_ref[l, 7:8, 2 * LANES : 2 * LANES + heads] = skip[l : l + 1, :]
+    finish(1, small, copies, x_ref, out_ref, gain_at, bc_buf, gain_buf)
+
+
+def pack(body, out_shape, out_specs, scratch, *arrays):
     return pl.pallas_call(
         body,
-        out_shape=jax.ShapeDtypeStruct((count, rows, LANES), bf16),
+        out_shape=out_shape,
         in_specs=[pl.BlockSpec(memory_space=pltpu.HBM)] * len(arrays),
-        out_specs=VMEM,
-        scratch_shapes=[
-            pltpu.VMEM(bc.shape[1:], bf16),
-            pltpu.VMEM(gain.shape, f32),
-            pltpu.SemaphoreType.DMA((count + 2,)),
-        ],
+        out_specs=out_specs,
+        scratch_shapes=scratch,
         compiler_params=pltpu.CompilerParams(vmem_limit_bytes=8 * 1024 * 1024),
         cost_estimate=pl.CostEstimate(flops=1000000, bytes_accessed=1000000, transcendentals=0),
     )(*(pltpu.with_memory_space_constraint(a, pltpu.HBM) for a in arrays))
@@ -356,39 +413,39 @@
     wide = in_blocks * LANES
     shape = jax.ShapeDtypeStruct
 
-    own = jnp.broadcast_to(
-        stream.reshape(2, 1, half, cols_dev), (2, n_tp, half, cols_dev)
-    )
-    hidden = exchange_plane(own.reshape(2 * n_tp, half, cols_dev), CTP, plane)
-    packed = pack(
-        pack_first, in_blocks + 1,
-        x_weight, z_weight, step_weight, bc_weight, norm_gain,
-    )
+    dma = pltpu.SemaphoreType.DMA
+    shared = [pltpu.VMEM(bc_weight.shape[1:], bf16), pltpu.VMEM(norm_gain.shape, f32)]
+    own, packed = pack(
+        enter,
+        (shape((2 * n_tp, half, cols_dev), bf16), shape((in_blocks + 1, cols_dev, LANES), bf16)),
+        (pl.BlockSpec(memory_space=pl.ANY), VMEM),
+        [
+            pltpu.VMEM(stream.shape, bf16),
+            pltpu.VMEM((2 * n_tp, half, cols_dev), bf16),
+            *shared,
+            dma((in_blocks + 4,)),
+        ],
+        stream, x_weight, z_weight, step_weight, bc_weight, norm_gain,
+    )
+    hidden = exchange_plane(own, CTP, plane)
     w_first = (packed, swap_cores(packed))
-    packed = pack(
-        pack_rest, rest,
-        x_weight, z_weight, step_weight, out_weight, bc_weight, norm_gain,
+    small = (
+        jnp.transpose(conv_x_weight, (1, 0, 2)), conv_bc_weight, step_bias, decay_log,
+        skip_gain, group_gain, conv_x_state, conv_bc_state,
+    )
+    packed, params = pack(
+        pack_rest,
+        (shape((rest, cols_dev, LANES), bf16), shape((LAYERS, 8, x_width), f32)),
+        (VMEM, VMEM),
+        [
+            *shared,
+            *(pltpu.VMEM(a.shape, a.dtype) for a in small),
+            dma((rest + 2,)),
+            dma((len(small),)),
+        ],
+        x_weight, z_weight, step_weight, out_weight, bc_weight, norm_gain, *small,
     )
     w_rest = (packed, swap_cores(packed))
-    x_tap = conv_x_weight.astype(f32)
-    bc_tap = conv_bc_weight.astype(f32)
-    x_base = jnp.sum(conv_x_state.astype(f32) * x_tap[:, None, :-1], axis=2)
-    bc_base = jnp.sum(conv_bc_state.astype(f32) * bc_tap[:, None, :-1], axis=2)
-    by_head = [
-        jnp.pad(v, ((0, 0), (0, LANES - heads_dev)))
-        for v in (step_bias, jnp.exp(decay_log), skip_gain)
-    ]
-    by_head = jnp.concatenate(by_head, axis=1)
-    rows = [
-        x_base,
-        x_tap[:, -1:],
-        group_gain[:, None],
-        bc_base.reshape(LAYERS, seq_count, bc_width),
-        bc_tap[:, -1].reshape(LAYERS, 1, bc_width),
-        by_head[:, None],
-    ]
-    rows = [jnp.pad(r, ((0, 0), (0, 0), (0, x_width - r.shape[2]))) for r in rows]
-    params = jnp.concatenate(rows, axis=1)
 
     result = None
     for l in range(LAYERS):

time: 116 us -> 116 us (level)
  blocking collectives: 67.2 us -> 97.1 us
  starting transfers between devices: 33.1 us -> 10.7 us
  waiting for transfers between devices: 3.55 us -> 0.01 us
  local copies, waits for them, and re-layouts: 3.47 us -> 0.15 us
    all_to_all x2 -> x0, starting transfers between devices: 21.9 us -> none  [the longest x1 14.8 us: exchange_z(): lax.all_to_all(value, 'z', split_axis=0, concat_axis=0, axis_index_groups...]
    all_to_all x3 -> x4, blocking collectives: 42.7 us -> 61.9 us  [exchange_z(): lax.all_to_all(value, 'z', split_axis=0, concat_axis=0, axis_index_groups...]
    all_to_all x2 -> x3, blocking collectives: 24.5 us -> 35.2 us  [exchange_plane(): lax.all_to_all(value, axis, split_axis=0, concat_axis=0, axis_index_group...]
    all_to_all x2 -> x0, waiting for transfers between devices: 3.55 us -> none  [the longest x1 3.55 us: exchange_z(): lax.all_to_all(value, 'z', split_axis=0, concat_axis=0, axis_index_groups...]
    unnamed x22 -> x6, local copies, waits for them, and re-layouts: 1.94 us -> 0.02 us
  transfers between devices with their start and end apart: 4 -> 2, of which waited for: 1 -> 0; matrix products, arithmetic and copies ran while one was open for 1% -> 0% of each run, Pallas kernels for 2% -> 3%
where the time goes in v7:
time: 116 us
  blocking collectives  97.1 us (84%)
  starting transfers between devices  10.7 us (9%)
  Pallas kernels  6.38 us (6%)
    all_to_all x4, blocking collectives, exchange_z(): lax.all_to_all(value, 'z', split_axis=0, concat_axis=0, axis_index_groups...  61.9 us
    all_to_all x3, blocking collectives, exchange_plane(): lax.all_to_all(value, axis, split_axis=0, concat_axis=0, axis_index_group...  35.2 us
    ppermute x2, starting transfers between devices, swap_cores(): return lax.ppermute(value, 'core', [(0, 1), (1, 0)])  10.7 us
    pallas_call x2, Pallas kernels, pack(): pl.pallas_call(body, out_shape=out_shape, in_specs=[pl.BlockSpec(memory_s...  2.86 us
  transfers between devices with their start and end apart: 2, of which 0 were waited for; matrix products, arithmetic and copies ran while one was open for 0% of the time, Pallas kernels for 3%

profile of v7, /device:TPU:1, one launch (start us, length us, event | category | flops | bytes accessed | tf_op | source)
XLA Modules:
  0.0 115.7 jit_solution(15500405245579020638)
XLA Ops:
  0.6 1.2 %shard_map.183 = (bf16[32,2,128]{2,1,0:T(2,128)(2,1)S(1)}, bf16[12,128,128]{2,1,0:T(8,128)(2,1)S(1)}) custom-call(bf16[4,128]{1,0:T(4,128)(2,1)} %stream_ref.1, bf16[2,128,512]{2,1,0:T(8,128)(2,1)} %x_ref.3, bf16[2,128,512]{2,1,0:T(8,128)(2,1)} %z_ref.3, bf16[2,128,128]{2,1,0:T(8,128)(2,1)} %step_ref.3, bf16[2,128,2,128]{3,2,1,0:T(2,128)(2,1)} %bc_ref.3, ...), custom_call_target="tpu_custom_call" | custom-call | flops 1000000 | bytes 1000000 | tf_op jit(solution)/shard_map/pallas_call | solution.py:181
  1.8 8.7 %collective-permute-start = (bf16[12,128,128]{2,1,0:T(8,128)(2,1)S(1)}, bf16[12,128,128]{2,1,0:T(8,128)(2,1)S(1)}, u32[]{:S(2)}, u32[]{:S(2)}) collective-permute-start(bf16[12,128,128]{2,1,0:T(8,128)(2,1)S(1)} %get-tuple-element.18.own_ref), channel_id=1, source_target_pairs={{0,1},{1,0},{2,3},{3,2},{4,5},{5,4},{6,7},{7,6},{8,9},{9,8},{10,11... | collective-permute-start | bytes 1179656 | tf_op jit(solution)/shard_map/ppermute | solution.py:45
  10.6 0.0 copy-start
  10.6 1.6 %shard_map.185 = (bf16[20,128,128]{2,1,0:T(8,128)(2,1)S(1)}, f32[2,8,512]{2,1,0:T(8,128)S(1)}) custom-call(bf16[2,128,512]{2,1,0:T(8,128)(2,1)} %x_ref.3, bf16[2,128,512]{2,1,0:T(8,128)(2,1)} %z_ref.3, bf16[2,128,128]{2,1,0:T(8,128)(2,1)} %step_ref.3, bf16[2,512,128]{2,1,0:T(8,128)(2,1)} %w_ref.1, bf16[2,128,2,128]{3,2,1,0:T(2,128)(2,1)} %bc_ref.3, ...), custom_call_target="tpu_custom_call" | custom-call | flops 1000000 | bytes 1000000 | tf_op jit(solution)/shard_map/pallas_call | solution.py:181
  12.3 1.9 %collective-permute-start.1 = (bf16[20,128,128]{2,1,0:T(8,128)(2,1)S(1)}, bf16[20,128,128]{2,1,0:T(8,128)(2,1)S(1)}, u32[]{:S(2)}, u32[]{:S(2)}) collective-permute-start(bf16[20,128,128]{2,1,0:T(8,128)(2,1)S(1)} %get-tuple-element.21.own_ref), channel_id=1, source_target_pairs={{0,1},{1,0},{2,3},{3,2},{4,5},{5,4},{6,7},{7,6},{8,9},{9,8},{10,11... | collective-permute-start | bytes 1966088 | tf_op jit(solution)/shard_map/ppermute | solution.py:45
  14.2 9.3 %all_to_all.35 = bf16[32,2,128]{2,1,0:T(2,128)(2,1)S(1)} all-to-all(bf16[32,2,128]{2,1,0:T(2,128)(2,1)S(1)} %get-tuple-element.17), channel_id=1, replica_groups={{320,352,256,288,448,480,384,416,64,96,0,32,192,224,128,160,321,353,257..., dimensions={0} | all-to-all | bytes 32768 | tf_op jit(solution)/shard_map/all_to_all | solution.py:39
  23.5 0.0 collective-permute-done.other_ref
  23.5 0.3 shard_map.184
  23.8 19.2 %all_to_all.36.got_ref = bf16[16,2,1408]{2,1,0:T(2,128)(2,1)S(1)} all-to-all(bf16[16,2,1408]{2,1,0:T(2,128)(2,1)S(1)} %reshape.36), channel_id=1, replica_groups={{16,18,20,22,24,26,28,30,0,2,4,6,8,10,12,14},{17,19,21,23,25,27,29,31,1..., dimensions={0} | all-to-all | bytes 180224 | tf_op jit(solution)/shard_map/all_to_all | solution.py:29
  43.1 0.0 copy-done
  43.1 1.0 shard_map.186
  44.1 13.7 %all_to_all.37 = bf16[16,2,512]{2,1,0:T(2,128)(2,1)S(1)} all-to-all(bf16[16,2,512]{2,1,0:T(2,128)(2,1)S(1)} %get-tuple-element.20), channel_id=1, replica_groups={{16,18,20,22,24,26,28,30,0,2,4,6,8,10,12,14},{17,19,21,23,25,27,29,31,1..., dimensions={0} | all-to-all | bytes 65536 | tf_op jit(solution)/shard_map/all_to_all | solution.py:29
  57.8 0.0 collective-permute-done.1.other_ref
  57.8 0.2 shard_map.187
  58.0 10.7 %all_to_all.38.arrived_ref = bf16[16,2,32,128]{3,2,1,0:T(8,128)(2,1)S(1)} all-to-all(bf16[16,2,32,128]{3,2,1,0:T(8,128)(2,1)S(1)} %shard_map.187), channel_id=1, replica_groups={{320,352,256,288,448,480,384,416,64,96,0,32,192,224,128,160},{321,353,2..., dimensions={0} | all-to-all | bytes 524288 | tf_op jit(solution)/shard_map/all_to_all | solution.py:39
  68.7 0.3 shard_map.188
  69.1 0.0 copy-start.1
  69.1 0.0 copy-start.2
  69.1 15.2 %all_to_all.39.got_ref = bf16[16,2,1408]{2,1,0:T(2,128)(2,1)S(1)} all-to-all(bf16[16,2,1408]{2,1,0:T(2,128)(2,1)S(1)} %reshape.38), channel_id=1, replica_groups={{16,18,20,22,24,26,28,30,0,2,4,6,8,10,12,14},{17,19,21,23,25,27,29,31,1..., dimensions={0} | all-to-all | bytes 180224 | tf_op jit(solution)/shard_map/all_to_all | solution.py:29
  84.3 0.0 copy-done.1
  84.3 0.0 copy-done.2
  84.3 1.6 %scan_last.1 = (bf16[16,2,512]{2,1,0:T(2,128)(2,1)S(1)}, f32[2,2,8,64,128]{4,3,2,1,0:T(8,128)}, bf16[2,2,4,512]{3,2,1,0:T(4,128)(2,1)}, bf16[2,2,4,2,128]{4,3,2,1,0:T(2,128)(2,1)}) custom-call(bf16[16,2,1408]{2,1,0:T(2,128)(2,1)S(1)} %all_to_all.39.got_ref, f32[2,8,512]{2,1,0:T(8,128)S(1)} %get-tuple-element.19.par_ref, f32[2,2,8,64,128]{4,3,2,1,0:T(8,128)S(1)} %copy-done, ...), custom_call_target="tpu_custom_call" | custom-call | flops 10000000 | bytes 1000000 | tf_op jit(solution)/shard_map/scan_last/pallas_call | solution.py:477
  85.9 13.7 %all_to_all.40 = bf16[16,2,512]{2,1,0:T(2,128)(2,1)S(1)} all-to-all(bf16[16,2,512]{2,1,0:T(2,128)(2,1)S(1)} %get-tuple-element.25), channel_id=1, replica_groups={{16,18,20,22,24,26,28,30,0,2,4,6,8,10,12,14},{17,19,21,23,25,27,29,31,1..., dimensions={0} | all-to-all | bytes 65536 | tf_op jit(solution)/shard_map/all_to_all | solution.py:29
  99.6 0.2 shard_map.189
  99.8 0.1 pad_maximum_fusion
  99.9 15.2 %all_to_all.41 = bf16[32,4,128]{2,1,0:T(4,128)(2,1)S(1)} all-to-all(bf16[32,4,128]{2,1,0:T(4,128)(2,1)S(1)} %pad_maximum_fusion), channel_id=1, replica_groups={{320,352,256,288,448,480,384,416,64,96,0,32,192,224,128,160,321,353,257..., dimensions={0} | all-to-all | bytes 65536 | tf_op jit(solution)/shard_map/all_to_all | solution.py:39
  115.1 0.6 add_convert_fusion
  (7 shorter events, 0.2 us)
Async XLA Ops:
  1.8 21.6 %collective-permute-start = (bf16[12,128,128]{2,1,0:T(8,128)(2,1)S(1)}, bf16[12,128,128]{2,1,0:T(8,128)(2,1)S(1)}, u32[]{:S(2)}, u32[]{:S(2)}) collective-permute-start(bf16[12,128,128]{2,1,0:T(8,128)(2,1)S(1)} %get-tuple-element.18.own_ref), channel_id=1, source_target_pairs={{0,1},{1,0},{2,3},{3,2},{4,5},{5,4},{6,7},{7,6},{8,9},{9,8},{10,11... | collective-permute-start | bytes 1179656 | tf_op jit(solution)/shard_map/ppermute | solution.py:45
  10.6 32.5 %copy-start = (f32[2,2,8,64,128]{4,3,2,1,0:T(8,128)S(1)}, f32[2,2,8,64,128]{4,3,2,1,0:T(8,128)}, u32[]{:S(2)}) copy-start(f32[2,2,8,64,128]{4,3,2,1,0:T(8,128)} %state_ref.3) | copy-start | bytes 3145732
  12.3 45.5 %collective-permute-start.1 = (bf16[20,128,128]{2,1,0:T(8,128)(2,1)S(1)}, bf16[20,128,128]{2,1,0:T(8,128)(2,1)S(1)}, u32[]{:S(2)}, u32[]{:S(2)}) collective-permute-start(bf16[20,128,128]{2,1,0:T(8,128)(2,1)S(1)} %get-tuple-element.21.own_ref), channel_id=1, source_target_pairs={{0,1},{1,0},{2,3},{3,2},{4,5},{5,4},{6,7},{7,6},{8,9},{9,8},{10,11... | collective-permute-start | bytes 1966088 | tf_op jit(solution)/shard_map/ppermute | solution.py:45
  69.1 15.3 %copy-start.1 = (bf16[2,2,4,512]{3,2,1,0:T(4,128)(2,1)S(1)}, bf16[2,2,4,512]{3,2,1,0:T(4,128)(2,1)}, u32[]{:S(2)}) copy-start(bf16[2,2,4,512]{3,2,1,0:T(4,128)(2,1)} %conv_x_ref.3) | copy-start | bytes 49156
  69.1 15.2 %copy-start.2 = (bf16[2,2,4,2,128]{4,3,2,1,0:T(2,128)(2,1)S(1)}, bf16[2,2,4,2,128]{4,3,2,1,0:T(2,128)(2,1)}, u32[]{:S(2)}) copy-start(bf16[2,2,4,2,128]{4,3,2,1,0:T(2,128)(2,1)} %conv_bc_ref.3) | copy-start | bytes 24580

commit v8 on v7

--- a/solution.py
+++ b/solution.py
@@ -56,6 +56,10 @@
     )
 
 
+def span(at, count=1):
+    return pl.ds(at * LANES, count * LANES)
+
+
 def projection_copies(layer, x_ref, z_ref, step_ref, out_ref, sems):
     copies = []
     at = 0
@@ -63,33 +67,22 @@
         if ref is None:
             at += 2
             continue
-        for k in range(ref.shape[2] // LANES):
-            block = ref.at[layer, :, pl.ds(k * LANES, LANES)]
-            copies.append(pltpu.make_async_copy(block, out_ref.at[at], sems.at[at]))
-            at += 1
+        count = ref.shape[2] // LANES
+        target = out_ref.at[:, span(at, count)]
+        copies.append(pltpu.make_async_copy(ref.at[layer], target, sems.at[at]))
+        at += count
     return copies, at
 
 
-def start_small(layer, bc_ref, gain_ref, bc_buf, gain_buf, sems):
-    last = sems.shape[0] - 1
-    small = [
-        pltpu.make_async_copy(bc_ref.at[layer], bc_buf, sems.at[last - 1]),
-        pltpu.make_async_copy(gain_ref, gain_buf, sems.at[last]),
-    ]
-    for copy in small:
-        copy.start()
-    return small
-
-
-def finish(layer, small, copies, x_ref, out_ref, gain_at, bc_buf, gain_buf):
-    small[0].wait()
-    at = 2 * (x_ref.shape[2] // LANES)
-    for i in range(2):
-        out_ref[at + i] = bc_buf[:, i, :]
-    small[1].wait()
-    put_gain(gain_buf[layer : layer + 1, :], out_ref, gain_at)
-    for copy in copies:
-        copy.wait()
+def put_pair(both, out_ref, at):
+    rows = both.shape[0]
+    to = lax.broadcasted_iota(jnp.int32, (rows, rows), 0)
+    source = lax.broadcasted_iota(jnp.int32, (rows, rows), 1)
+    want = 2 * (to % (rows // 2)) + to // (rows // 2)
+    pick = jnp.where(source == want, 1.0, 0.0).astype(bf16)
+    parted = jnp.dot(pick, both, preferred_element_type=f32).astype(bf16)
+    out_ref[:, span(at)] = parted[: rows // 2]
+    out_ref[:, span(at + 1)] = parted[rows // 2 :]
 
 
 def put_gain(gain, out_ref, at):
@@ -99,19 +92,36 @@
     third = (left - second.astype(f32)).astype(bf16)
     row = lax.broadcasted_iota(jnp.int32, (LANES, LANES), 0)
     pieces = jnp.where(row == 1, second.astype(f32), jnp.where(row == 2, third.astype(f32), 0.0))
-    out_ref[at] = jnp.where(row == 0, first.astype(f32), pieces).astype(bf16)
+    out_ref[:, span(at)] = jnp.where(row == 0, first.astype(f32), pieces).astype(bf16)
 
 
 def enter(
-    stream_ref, x_ref, z_ref, step_ref, bc_ref, gain_ref,
-    own_out, out_ref, stream_buf, own_buf, bc_buf, gain_buf, sems,
+    stream_ref, x_ref, z_ref, step_ref, w_ref, bc_ref, gain_ref,
+    tap_x_ref, tap_bc_ref, bias_ref, decay_ref, skip_ref, group_ref, conv_x_ref, conv_bc_ref,
+    own_out, out_ref, rest_ref, par_ref,
+    stream_buf, own_buf, bc_buf, gain_buf,
+    tap_x, tap_bc, bias, decay, skip, group, conv_x, conv_bc, sems, rest_sems, par_sems,
 ):
-    copies, at = projection_copies(0, x_ref, z_ref, step_ref, out_ref, sems)
-    count = sems.shape[0]
-    into = pltpu.make_async_copy(stream_ref, stream_buf, sems.at[count - 4])
+    into = pltpu.make_async_copy(stream_ref, stream_buf, par_sems.at[0])
     into.start()
-    small = start_small(0, bc_ref, gain_ref, bc_buf, gain_buf, sems)
-    for copy in copies:
+    sources = (tap_x_ref, tap_bc_ref, bias_ref, decay_ref, skip_ref, group_ref)
+    sources += (conv_x_ref, conv_bc_ref, bc_ref, gain_ref)
+    bufs = (tap_x, tap_bc, bias, decay, skip, group, conv_x, conv_bc, bc_buf, gain_buf)
+    loads = [
+        pltpu.make_async_copy(a, b, par_sems.at[2 + k])
+        for k, (a, b) in enumerate(zip(sources, bufs))
+    ]
+    for copy in loads[-2:]:
+        copy.start()
+    copies, gain_at = projection_copies(0, x_ref, z_ref, step_ref, out_ref, sems)
+    others, _ = projection_copies(1, x_ref, z_ref, step_ref, rest_ref, rest_sems)
+    at = gain_at + 1
+    for l in range(LAYERS):
+        for k in range(w_ref.shape[1] // LANES):
+            block = w_ref.at[l, pl.ds(k * LANES, LANES), :]
+            others.append(pltpu.make_async_copy(block, rest_ref.at[:, span(at)], rest_sems.at[at]))
+            at += 1
+    for copy in copies + loads[:-2] + others:
         copy.start()
     into.wait()
     half = own_buf.shape[1]
@@ -120,37 +130,14 @@
         rows = stream_buf[c * half : (c + 1) * half]
         for p in range(each):
             own_buf[c * each + p] = rows
-    out = pltpu.make_async_copy(own_buf, own_out, sems.at[count - 3])
+    out = pltpu.make_async_copy(own_buf, own_out, par_sems.at[1])
     out.start()
-    finish(0, small, copies + [out], x_ref, out_ref, at, bc_buf, gain_buf)
-
-
-def pack_rest(
-    x_ref, z_ref, step_ref, w_ref, bc_ref, gain_ref,
-    tap_x_ref, tap_bc_ref, bias_ref, decay_ref, skip_ref, group_ref, conv_x_ref, conv_bc_ref,
-    out_ref, par_ref, bc_buf, gain_buf,
-    tap_x, tap_bc, bias, decay, skip, group, conv_x, conv_bc, sems, par_sems,
-):
-    sources = (tap_x_ref, tap_bc_ref, bias_ref, decay_ref, skip_ref, group_ref)
-    sources += (conv_x_ref, conv_bc_ref)
-    bufs = (tap_x, tap_bc, bias, decay, skip, group, conv_x, conv_bc)
-    loads = [
-        pltpu.make_async_copy(a, b, par_sems.at[k]) for k, (a, b) in enumerate(zip(sources, bufs))
-    ]
-    copies, gain_at = projection_copies(1, x_ref, z_ref, step_ref, out_ref, sems)
-    at = gain_at + 1
-    for l in range(LAYERS):
-        for k in range(w_ref.shape[1] // LANES):
-            block = w_ref.at[l, pl.ds(k * LANES, LANES), :]
-            copies.append(pltpu.make_async_copy(block, out_ref.at[at], sems.at[at]))
-            at += 1
-    for copy in loads:
-        copy.start()
-    small = start_small(1, bc_ref, gain_ref, bc_buf, gain_buf, sems)
-    for copy in copies:
-        copy.start()
     for copy in loads:
         copy.wait()
+    shared_at = 2 * (x_ref.shape[2] // LANES)
+    for l, ref in ((0, out_ref), (1, rest_ref)):
+        put_pair(bc_buf[l], ref, shared_at)
+        put_gain(gain_buf[l : l + 1, :], ref, gain_at)
     heads = bias.shape[1]
     seqs = conv_x.shape[1]
     taps = tap_x.shape[0] - 1
@@ -174,7 +161,8 @@
         par_ref[l, 7:8, :heads] = bias[l : l + 1, :]
         par_ref[l, 7:8, LANES : LANES + heads] = jnp.exp(decay[l : l + 1, :])
         par_ref[l, 7:8, 2 * LANES : 2 * LANES + heads] = skip[l : l + 1, :]
-    finish(1, small, copies, x_ref, out_ref, gain_at, bc_buf, gain_buf)
+    for copy in copies + others + [out]:
+        copy.wait()
 
 
 def pack(body, out_shape, out_specs, scratch, *arrays):
@@ -198,7 +186,7 @@
     total = None
     place = (lax.axis_index("y") * lax.axis_size("x") + lax.axis_index("x")) * first
     for rows, w_ref in zip(normed, weights):
-        block = jnp.concatenate([w_ref[k] for k in range(blocks)], axis=1)
+        block = w_ref[:, : blocks * LANES]
         term = jnp.dot(rows, block, preferred_element_type=f32)
         total = term if total is None else total + term
     wide = (blocks - 1) * LANES
@@ -210,7 +198,7 @@
 
 
 def scaled(rows, w_ref, blocks):
-    pieces = w_ref[blocks, :8].astype(f32)
+    pieces = w_ref[:8, span(blocks)].astype(f32)
     gain = pieces[0:1] + pieces[1:2] + pieces[2:3]
     return (rows * gain).astype(bf16)
 
@@ -245,7 +233,7 @@
 
 
 def out_terms(mixed_ref, w_ref, at, blocks):
-    weights = jnp.concatenate([w_ref[at + k] for k in range(blocks)], axis=0)
+    weights = jnp.concatenate([w_ref[:, span(at + k)] for k in range(blocks)], axis=0)
     return swapped(jnp.dot(mixed_ref[...], weights, preferred_element_type=f32)).astype(bf16)
 
 
@@ -294,9 +282,8 @@
     seqs = total.shape[0]
     tail = total[:, total.shape[1] - LANES :]
     inv = lax.rsqrt(tail[:, heads : heads + 1] / MODEL_WIDTH + EPS)
-    proj = (total[:, : total.shape[1] - LANES] * inv).astype(bf16)
-    proj_done(proj)
-    proj = proj.astype(f32)
+    rounded = (total[:, : total.shape[1] - LANES] * inv).astype(bf16)
+    proj = rounded.astype(f32)
     par = par_ref[layer]
     inputs_x = silu(par[0:2] + proj[:, :width] * par[2:3])
     bc_width = proj.shape[1] - 2 * width
@@ -304,25 +291,33 @@
     raw = tail * inv + par[7:8, :LANES]
     step = jnp.maximum(raw, 0.0) + jnp.log1p(jnp.exp(-jnp.abs(raw)))
     decay = jnp.exp(-step * par[7:8, LANES : 2 * LANES])
-    u_cols = columns(head_spread(step, HEAD_DIM, heads) * inputs_x)
-    decay_cols = columns(head_spread(decay, HEAD_DIM, heads))
-    skip = head_spread(par[7:8, 2 * LANES : 3 * LANES], HEAD_DIM, heads)
+    u_rows = head_spread(step, HEAD_DIM, heads) * inputs_x
+    u_cols = columns(u_rows)
     row = lax.broadcasted_iota(jnp.int32, (8, STATE_DIM), 0)
-    readouts = []
+    b_rows, c_rows = inputs_bc[:, :STATE_DIM], inputs_bc[:, STATE_DIM:]
+    reads = []
     for s in range(seqs):
-        b_row = inputs_bc[s : s + 1, :STATE_DIM]
-        c_row = inputs_bc[s : s + 1, STATE_DIM:]
+        c_row = c_rows[s : s + 1]
+        c_high = c_row.astype(bf16).astype(f32)
+        c_both = jnp.where(row == 0, c_high, jnp.where(row == 1, c_row - c_high, 0.0))
         old = state_ref[layer, s].reshape(width, STATE_DIM)
-        new = old * decay_cols[:, s : s + 1] + u_cols[:, s : s + 1] * b_row
-        state_done(s, new.reshape(heads, HEAD_DIM, STATE_DIM))
-        c_high = c_row.astype(bf16).astype(f32)
-        c_rows = jnp.where(row == 0, c_high, jnp.where(row == 1, c_row - c_high, 0.0))
         out = lax.dot_general(
-            c_rows.astype(bf16), new.astype(bf16), (((1,), (1,)), ((), ())),
+            c_both.astype(bf16), old.astype(bf16), (((1,), (1,)), ((), ())),
             preferred_element_type=f32,
         )
-        readouts.append(out[0:1] + out[1:2])
-    readout = jnp.concatenate(readouts, axis=0) + skip * inputs_x
+        reads.append(out[0:1] + out[1:2])
+    for s in range(seqs):
+        new = []
+        for h in range(heads):
+            at = h * HEAD_DIM
+            keep = jnp.broadcast_to(decay[s : s + 1, h : h + 1], (HEAD_DIM, STATE_DIM))
+            add = u_cols[at : at + HEAD_DIM, s : s + 1] * b_rows[s : s + 1]
+            new.append(state_ref[layer, s, h] * keep + add)
+        state_done(s, new)
+    proj_done(rounded)
+    readout = head_spread(decay, HEAD_DIM, heads) * jnp.concatenate(reads, axis=0)
+    readout = readout + u_rows * jnp.sum(b_rows * c_rows, axis=1, keepdims=True)
+    readout = readout + head_spread(par[7:8, 2 * LANES : 3 * LANES], HEAD_DIM, heads) * inputs_x
     gated = readout * silu(proj[:, width : 2 * width])
     mean = jnp.sum(gated * gated, axis=1, keepdims=True) / width
     return (gated * lax.rsqrt(mean + EPS) * par[3:4]).astype(bf16)
@@ -333,7 +328,8 @@
         proj_ref[...] = proj
 
     def state_done(s, new):
-        new_ref[s] = new
+        for h in range(heads):
+            new_ref[s, h] = new[h]
 
     mixed = scan(0, projected(got_ref), heads, par_ref, state_ref, proj_done, state_done)
     for z in range(mixed_ref.shape[0]):
@@ -367,7 +363,8 @@
                 bc_buf[l, s, 3] = jnp.where(bc_row == 0, b_row, c_row).astype(bf16)
 
     def state_done(s, new):
-        new_buf[s] = new
+        for h in range(heads):
+            new_buf[s, h] = new[h]
         copies.append(pltpu.make_async_copy(new_buf.at[s], state_out.at[1, s], sems.at[1 + s]))
         copies[-1].start()
 
@@ -414,38 +411,35 @@
     shape = jax.ShapeDtypeStruct
 
     dma = pltpu.SemaphoreType.DMA
-    shared = [pltpu.VMEM(bc_weight.shape[1:], bf16), pltpu.VMEM(norm_gain.shape, f32)]
-    own, packed = pack(
+    bc_rows = bc_weight.reshape(LAYERS, 2 * cols_dev, LANES)
+    small = (
+        jnp.transpose(conv_x_weight, (1, 0, 2)), conv_bc_weight, step_bias, decay_log,
+        skip_gain, group_gain, conv_x_state, conv_bc_state,
+    )
+    own, packed, packed_rest, params = pack(
         enter,
-        (shape((2 * n_tp, half, cols_dev), bf16), shape((in_blocks + 1, cols_dev, LANES), bf16)),
-        (pl.BlockSpec(memory_space=pl.ANY), VMEM),
+        (
+            shape((2 * n_tp, half, cols_dev), bf16),
+            shape((cols_dev, (in_blocks + 1) * LANES), bf16),
+            shape((cols_dev, rest * LANES), bf16),
+            shape((LAYERS, 8, x_width), f32),
+        ),
+        (pl.BlockSpec(memory_space=pl.ANY), VMEM, VMEM, VMEM),
         [
             pltpu.VMEM(stream.shape, bf16),
             pltpu.VMEM((2 * n_tp, half, cols_dev), bf16),
-            *shared,
-            dma((in_blocks + 4,)),
+            pltpu.VMEM(bc_rows.shape, bf16),
+            pltpu.VMEM(norm_gain.shape, f32),
+            *(pltpu.VMEM(a.shape, a.dtype) for a in small),
+            dma((in_blocks + 1,)),
+            dma((rest,)),
+            dma((len(small) + 4,)),
         ],
-        stream, x_weight, z_weight, step_weight, bc_weight, norm_gain,
+        stream, x_weight, z_weight, step_weight, out_weight, bc_rows, norm_gain, *small,
     )
     hidden = exchange_plane(own, CTP, plane)
     w_first = (packed, swap_cores(packed))
-    small = (
-        jnp.transpose(conv_x_weight, (1, 0, 2)), conv_bc_weight, step_bias, decay_log,
-        skip_gain, group_gain, conv_x_state, conv_bc_state,
-    )
-    packed, params = pack(
-        pack_rest,
-        (shape((rest, cols_dev, LANES), bf16), shape((LAYERS, 8, x_width), f32)),
-        (VMEM, VMEM),
-        [
-            *shared,
-            *(pltpu.VMEM(a.shape, a.dtype) for a in small),
-            dma((rest + 2,)),
-            dma((len(small),)),
-        ],
-        x_weight, z_weight, step_weight, out_weight, bc_weight, norm_gain, *small,
-    )
-    w_rest = (packed, swap_cores(packed))
+    w_rest = (packed_rest, swap_cores(packed_rest))
 
     result = None
     for l in range(LAYERS):

time: 116 us -> 115 us (level)
  Pallas kernels: 6.38 us -> 4.89 us
    pallas_call x2 -> x1, Pallas kernels: 2.86 us -> 1.91 us  [pack(): pl.pallas_call(body, out_shape=out_shape, in_specs=[pl.BlockSpec(memory_s...]
  transfers between devices with their start and end apart: 2 -> 2, of which waited for: 0 -> 0; matrix products, arithmetic and copies ran while one was open for 0% -> 0% of each run, Pallas kernels for 3% -> 1%
where the time goes in v8:
time: 115 us; the launch traced here: 114 us
  blocking collectives  97.1 us (84%)
  starting transfers between devices  10.7 us (9%)
  Pallas kernels  4.89 us (4%)
    all_to_all x4, blocking collectives, exchange_z(): lax.all_to_all(value, 'z', split_axis=0, concat_axis=0, axis_index_groups...  61.9 us
    all_to_all x3, blocking collectives, exchange_plane(): lax.all_to_all(value, axis, split_axis=0, concat_axis=0, axis_index_group...  35.2 us
    ppermute x2, starting transfers between devices, swap_cores(): return lax.ppermute(value, 'core', [(0, 1), (1, 0)])  10.7 us
  transfers between devices with their start and end apart: 2, of which 0 were waited for; matrix products, arithmetic and copies ran while one was open for 0% of the time, Pallas kernels for 1%

profile of v8, /device:TPU:1, one launch (start us, length us, event | category | flops | bytes accessed | tf_op | source)
XLA Modules:
  0.0 114.2 jit_solution(11379765469243073333)
XLA Ops:
  0.6 0.0 copy-start
  0.6 1.9 %shard_map.183 = (bf16[32,2,128]{2,1,0:T(2,128)(2,1)S(1)}, bf16[128,1536]{1,0:T(8,128)(2,1)S(1)}, bf16[128,2560]{1,0:T(8,128)(2,1)S(1)}, f32[2,8,512]{2,1,0:T(8,128)S(1)}) custom-call(bf16[4,128]{1,0:T(4,128)(2,1)} %stream_ref.1, bf16[2,128,512]{2,1,0:T(8,128)(2,1)} %x_ref.1, bf16[2,128,512]{2,1,0:T(8,128)(2,1)} %z_ref.1, bf16[2,128,128]{2,1,0:T(8,128)(2,1)} %step_ref.1, ...), custom_call_target="tpu_custom_call" | custom-call | flops 1000000 | bytes 1000000 | tf_op jit(solution)/shard_map/pallas_call | solution.py:169
  2.6 8.7 %collective-permute-start = (bf16[128,1536]{1,0:T(8,128)(2,1)S(1)}, bf16[128,1536]{1,0:T(8,128)(2,1)S(1)}, u32[]{:S(2)}, u32[]{:S(2)}) collective-permute-start(bf16[128,1536]{1,0:T(8,128)(2,1)S(1)} %get-tuple-element.18.own_ref), channel_id=1, source_target_pairs={{0,1},{1,0},{2,3},{3,2},{4,5},{5,4},{6,7},{7,6},{8,9},{9,8},{10,11... | collective-permute-start | bytes 1179656 | tf_op jit(solution)/shard_map/ppermute | solution.py:45
  11.3 1.9 %collective-permute-start.1 = (bf16[128,2560]{1,0:T(8,128)(2,1)S(1)}, bf16[128,2560]{1,0:T(8,128)(2,1)S(1)}, u32[]{:S(2)}, u32[]{:S(2)}) collective-permute-start(bf16[128,2560]{1,0:T(8,128)(2,1)S(1)} %get-tuple-element.21.own_ref), channel_id=1, source_target_pairs={{0,1},{1,0},{2,3},{3,2},{4,5},{5,4},{6,7},{7,6},{8,9},{9,8},{10,11... | collective-permute-start | bytes 1966088 | tf_op jit(solution)/shard_map/ppermute | solution.py:45
  13.2 9.3 %all_to_all.35 = bf16[32,2,128]{2,1,0:T(2,128)(2,1)S(1)} all-to-all(bf16[32,2,128]{2,1,0:T(2,128)(2,1)S(1)} %get-tuple-element.17), channel_id=1, replica_groups={{320,352,256,288,448,480,384,416,64,96,0,32,192,224,128,160,321,353,257..., dimensions={0} | all-to-all | bytes 32768 | tf_op jit(solution)/shard_map/all_to_all | solution.py:39
  22.5 0.0 collective-permute-done.other_ref
  22.5 0.3 shard_map.184
  22.9 19.2 %all_to_all.36.got_ref = bf16[16,2,1408]{2,1,0:T(2,128)(2,1)S(1)} all-to-all(bf16[16,2,1408]{2,1,0:T(2,128)(2,1)S(1)} %reshape.40), channel_id=1, replica_groups={{16,18,20,22,24,26,28,30,0,2,4,6,8,10,12,14},{17,19,21,23,25,27,29,31,1..., dimensions={0} | all-to-all | bytes 180224 | tf_op jit(solution)/shard_map/all_to_all | solution.py:29
  42.1 0.0 copy-done
  42.1 0.6 shard_map.185
  42.8 13.7 %all_to_all.37 = bf16[16,2,512]{2,1,0:T(2,128)(2,1)S(1)} all-to-all(bf16[16,2,512]{2,1,0:T(2,128)(2,1)S(1)} %get-tuple-element.20), channel_id=1, replica_groups={{16,18,20,22,24,26,28,30,0,2,4,6,8,10,12,14},{17,19,21,23,25,27,29,31,1..., dimensions={0} | all-to-all | bytes 65536 | tf_op jit(solution)/shard_map/all_to_all | solution.py:29
  56.5 0.0 collective-permute-done.1.other_ref
  56.5 0.2 shard_map.186
  56.7 10.7 %all_to_all.38.arrived_ref = bf16[16,2,32,128]{3,2,1,0:T(8,128)(2,1)S(1)} all-to-all(bf16[16,2,32,128]{3,2,1,0:T(8,128)(2,1)S(1)} %shard_map.186), channel_id=1, replica_groups={{320,352,256,288,448,480,384,416,64,96,0,32,192,224,128,160},{321,353,2..., dimensions={0} | all-to-all | bytes 524288 | tf_op jit(solution)/shard_map/all_to_all | solution.py:39
  67.4 0.3 shard_map.187
  67.7 0.0 copy-start.1
  67.7 0.0 copy-start.2
  67.8 15.2 %all_to_all.39.got_ref = bf16[16,2,1408]{2,1,0:T(2,128)(2,1)S(1)} all-to-all(bf16[16,2,1408]{2,1,0:T(2,128)(2,1)S(1)} %reshape.42), channel_id=1, replica_groups={{16,18,20,22,24,26,28,30,0,2,4,6,8,10,12,14},{17,19,21,23,25,27,29,31,1..., dimensions={0} | all-to-all | bytes 180224 | tf_op jit(solution)/shard_map/all_to_all | solution.py:29
  83.0 0.0 copy-done.1
  83.0 0.0 copy-done.2
  83.0 1.4 %scan_last.1 = (bf16[16,2,512]{2,1,0:T(2,128)(2,1)S(1)}, f32[2,2,8,64,128]{4,3,2,1,0:T(8,128)}, bf16[2,2,4,512]{3,2,1,0:T(4,128)(2,1)}, bf16[2,2,4,2,128]{4,3,2,1,0:T(2,128)(2,1)}) custom-call(bf16[16,2,1408]{2,1,0:T(2,128)(2,1)S(1)} %all_to_all.39.got_ref, f32[2,8,512]{2,1,0:T(8,128)S(1)} %get-tuple-element.19.par_ref, f32[2,2,8,64,128]{4,3,2,1,0:T(8,128)S(1)} %copy-done, ...), custom_call_target="tpu_custom_call" | custom-call | flops 10000000 | bytes 1000000 | tf_op jit(solution)/shard_map/scan_last/pallas_call | solution.py:471
  84.4 13.7 %all_to_all.40 = bf16[16,2,512]{2,1,0:T(2,128)(2,1)S(1)} all-to-all(bf16[16,2,512]{2,1,0:T(2,128)(2,1)S(1)} %get-tuple-element.25), channel_id=1, replica_groups={{16,18,20,22,24,26,28,30,0,2,4,6,8,10,12,14},{17,19,21,23,25,27,29,31,1..., dimensions={0} | all-to-all | bytes 65536 | tf_op jit(solution)/shard_map/all_to_all | solution.py:29
  98.2 0.1 shard_map.188
  98.3 0.1 pad_maximum_fusion
  98.4 15.2 %all_to_all.41 = bf16[32,4,128]{2,1,0:T(4,128)(2,1)S(1)} all-to-all(bf16[32,4,128]{2,1,0:T(4,128)(2,1)S(1)} %pad_maximum_fusion), channel_id=1, replica_groups={{320,352,256,288,448,480,384,416,64,96,0,32,192,224,128,160,321,353,257..., dimensions={0} | all-to-all | bytes 65536 | tf_op jit(solution)/shard_map/all_to_all | solution.py:39
  113.6 0.6 add_convert_fusion
  (7 shorter events, 0.2 us)
Async XLA Ops:
  0.6 41.5 %copy-start = (f32[2,2,8,64,128]{4,3,2,1,0:T(8,128)S(1)}, f32[2,2,8,64,128]{4,3,2,1,0:T(8,128)}, u32[]{:S(2)}) copy-start(f32[2,2,8,64,128]{4,3,2,1,0:T(8,128)} %state_ref.3) | copy-start | bytes 3145732
  2.6 20.0 %collective-permute-start = (bf16[128,1536]{1,0:T(8,128)(2,1)S(1)}, bf16[128,1536]{1,0:T(8,128)(2,1)S(1)}, u32[]{:S(2)}, u32[]{:S(2)}) collective-permute-start(bf16[128,1536]{1,0:T(8,128)(2,1)S(1)} %get-tuple-element.18.own_ref), channel_id=1, source_target_pairs={{0,1},{1,0},{2,3},{3,2},{4,5},{5,4},{6,7},{7,6},{8,9},{9,8},{10,11... | collective-permute-start | bytes 1179656 | tf_op jit(solution)/shard_map/ppermute | solution.py:45
  11.3 45.1 %collective-permute-start.1 = (bf16[128,2560]{1,0:T(8,128)(2,1)S(1)}, bf16[128,2560]{1,0:T(8,128)(2,1)S(1)}, u32[]{:S(2)}, u32[]{:S(2)}) collective-permute-start(bf16[128,2560]{1,0:T(8,128)(2,1)S(1)} %get-tuple-element.21.own_ref), channel_id=1, source_target_pairs={{0,1},{1,0},{2,3},{3,2},{4,5},{5,4},{6,7},{7,6},{8,9},{9,8},{10,11... | collective-permute-start | bytes 1966088 | tf_op jit(solution)/shard_map/ppermute | solution.py:45
  67.7 15.3 %copy-start.1 = (bf16[2,2,4,512]{3,2,1,0:T(4,128)(2,1)S(1)}, bf16[2,2,4,512]{3,2,1,0:T(4,128)(2,1)}, u32[]{:S(2)}) copy-start(bf16[2,2,4,512]{3,2,1,0:T(4,128)(2,1)} %conv_x_ref.3) | copy-start | bytes 49156
  67.7 15.2 %copy-start.2 = (bf16[2,2,4,2,128]{4,3,2,1,0:T(2,128)(2,1)S(1)}, bf16[2,2,4,2,128]{4,3,2,1,0:T(2,128)(2,1)}, u32[]{:S(2)}) copy-start(bf16[2,2,4,2,128]{4,3,2,1,0:T(2,128)(2,1)} %conv_bc_ref.3) | copy-start | bytes 24580

commit v9 on v8

--- a/solution.py
+++ b/solution.py
@@ -34,7 +34,7 @@
 def exchange_plane(value, axis, sizes):
     order = [0]
     for name, size in zip(axis, sizes):
-        inner = from_middle(size) if name != "core" else range(size)
+        inner = from_middle(size)
         order = [at * size + k for at in order for k in inner]
     return lax.all_to_all(
         value, axis, split_axis=0, concat_axis=0, axis_index_groups=[order], tiled=True
@@ -127,7 +127,7 @@
     half = own_buf.shape[1]
     each = own_buf.shape[0] // 2
     for c in range(2):
-        rows = stream_buf[c * half : (c + 1) * half]
+        rows = stream_buf[(1 - c) * half : (2 - c) * half]
         for p in range(each):
             own_buf[c * each + p] = rows
     out = pltpu.make_async_copy(own_buf, own_out, par_sems.at[1])
@@ -204,7 +204,7 @@
 
 
 def project_first(blocks, heads, hidden_ref, own_ref, other_ref, out_ref):
-    core = lax.axis_index("core")
+    core = 1 - lax.axis_index("core")
     rows = [hidden_ref[core], hidden_ref[1 - core]]
     wide = [swapped(r.astype(f32)) for r in rows]
     squares = jnp.sum(wide[0] * wide[0] + wide[1] * wide[1], axis=1, keepdims=True)
@@ -216,7 +216,7 @@
 def project_next(
     blocks, heads, arrived_ref, hidden_ref, own_ref, other_ref, out_ref, next_ref
 ):
-    core = lax.axis_index("core")
+    core = 1 - lax.axis_index("core")
     rows = []
     weights = (own_ref, other_ref)
     for c in (core, 1 - core):
@@ -238,7 +238,7 @@
 
 
 def mix_to_all(at, blocks, mixed_ref, own_ref, other_ref, out_ref):
-    core = lax.axis_index("core")
+    core = 1 - lax.axis_index("core")
     for c, w_ref in ((core, own_ref), (1 - core, other_ref)):
         terms = out_terms(mixed_ref, w_ref, at, blocks)
         for j in range(out_ref.shape[0]):
@@ -246,7 +246,7 @@
 
 
 def mix_last(at, blocks, mixed_ref, own_ref, other_ref, out_ref):
-    core = lax.axis_index("core")
+    core = 1 - lax.axis_index("core")
     for c, w_ref in ((core, own_ref), (1 - core, other_ref)):
         out_ref[c] = out_terms(mixed_ref, w_ref, at, blocks)
 
@@ -510,7 +510,7 @@
             )
             got = exchange_plane(both, CTP, plane).reshape(2, n_tp, rows_dev, cols_dev).astype(f32)
             result = got[:, :, :half].sum(axis=1) + got[:, 0, half:]
-            result = result.astype(bf16).reshape(rows_dev, cols_dev)
+            result = result[::-1].astype(bf16).reshape(rows_dev, cols_dev)
     return (result, *outs)
 
 

time: 115 us -> 114 us (level)
  no operation moved by 1% of the time
where the time goes in v9:
time: 114 us
  blocking collectives  96.6 us (85%)
  starting transfers between devices  10.7 us (9%)
  Pallas kernels  4.89 us (4%)
    all_to_all x4, blocking collectives, exchange_z(): lax.all_to_all(value, 'z', split_axis=0, concat_axis=0, axis_index_groups...  61.9 us
    all_to_all x3, blocking collectives, exchange_plane(): lax.all_to_all(value, axis, split_axis=0, concat_axis=0, axis_index_group...  34.7 us
    ppermute x2, starting transfers between devices, swap_cores(): return lax.ppermute(value, 'core', [(0, 1), (1, 0)])  10.7 us
  transfers between devices with their start and end apart: 2, of which 0 were waited for; matrix products, arithmetic and copies ran while one was open for 0% of the time, Pallas kernels for 1%

profile of v9, /device:TPU:1, one launch (start us, length us, event | category | flops | bytes accessed | tf_op | source)
XLA Modules:
  0.0 113.7 jit_solution(5690363866991776143)
XLA Ops:
  0.6 0.0 copy-start
  0.6 1.9 %shard_map.183 = (bf16[32,2,128]{2,1,0:T(2,128)(2,1)S(1)}, bf16[128,1536]{1,0:T(8,128)(2,1)S(1)}, bf16[128,2560]{1,0:T(8,128)(2,1)S(1)}, f32[2,8,512]{2,1,0:T(8,128)S(1)}) custom-call(bf16[4,128]{1,0:T(4,128)(2,1)} %stream_ref.1, bf16[2,128,512]{2,1,0:T(8,128)(2,1)} %x_ref.1, bf16[2,128,512]{2,1,0:T(8,128)(2,1)} %z_ref.1, bf16[2,128,128]{2,1,0:T(8,128)(2,1)} %step_ref.1, ...), custom_call_target="tpu_custom_call" | custom-call | flops 1000000 | bytes 1000000 | tf_op jit(solution)/shard_map/pallas_call | solution.py:169
  2.6 8.7 %collective-permute-start = (bf16[128,1536]{1,0:T(8,128)(2,1)S(1)}, bf16[128,1536]{1,0:T(8,128)(2,1)S(1)}, u32[]{:S(2)}, u32[]{:S(2)}) collective-permute-start(bf16[128,1536]{1,0:T(8,128)(2,1)S(1)} %get-tuple-element.18.own_ref), channel_id=1, source_target_pairs={{0,1},{1,0},{2,3},{3,2},{4,5},{5,4},{6,7},{7,6},{8,9},{9,8},{10,11... | collective-permute-start | bytes 1179656 | tf_op jit(solution)/shard_map/ppermute | solution.py:45
  11.3 1.9 %collective-permute-start.1 = (bf16[128,2560]{1,0:T(8,128)(2,1)S(1)}, bf16[128,2560]{1,0:T(8,128)(2,1)S(1)}, u32[]{:S(2)}, u32[]{:S(2)}) collective-permute-start(bf16[128,2560]{1,0:T(8,128)(2,1)S(1)} %get-tuple-element.21.own_ref), channel_id=1, source_target_pairs={{0,1},{1,0},{2,3},{3,2},{4,5},{5,4},{6,7},{7,6},{8,9},{9,8},{10,11... | collective-permute-start | bytes 1966088 | tf_op jit(solution)/shard_map/ppermute | solution.py:45
  13.2 9.0 %all_to_all.35 = bf16[32,2,128]{2,1,0:T(2,128)(2,1)S(1)} all-to-all(bf16[32,2,128]{2,1,0:T(2,128)(2,1)S(1)} %get-tuple-element.17), channel_id=1, replica_groups={{321,353,257,289,449,481,385,417,65,97,1,33,193,225,129,161,320,352,256..., dimensions={0} | all-to-all | bytes 32768 | tf_op jit(solution)/shard_map/all_to_all | solution.py:39
  22.3 0.0 collective-permute-done.other_ref
  22.3 0.3 shard_map.184
  22.6 19.2 %all_to_all.36.got_ref = bf16[16,2,1408]{2,1,0:T(2,128)(2,1)S(1)} all-to-all(bf16[16,2,1408]{2,1,0:T(2,128)(2,1)S(1)} %reshape.40), channel_id=1, replica_groups={{16,18,20,22,24,26,28,30,0,2,4,6,8,10,12,14},{17,19,21,23,25,27,29,31,1..., dimensions={0} | all-to-all | bytes 180224 | tf_op jit(solution)/shard_map/all_to_all | solution.py:29
  41.9 0.0 copy-done
  41.9 0.6 shard_map.185
  42.5 13.7 %all_to_all.37 = bf16[16,2,512]{2,1,0:T(2,128)(2,1)S(1)} all-to-all(bf16[16,2,512]{2,1,0:T(2,128)(2,1)S(1)} %get-tuple-element.20), channel_id=1, replica_groups={{16,18,20,22,24,26,28,30,0,2,4,6,8,10,12,14},{17,19,21,23,25,27,29,31,1..., dimensions={0} | all-to-all | bytes 65536 | tf_op jit(solution)/shard_map/all_to_all | solution.py:29
  56.2 0.0 collective-permute-done.1.other_ref
  56.2 0.2 shard_map.186
  56.4 10.7 %all_to_all.38.arrived_ref = bf16[16,2,32,128]{3,2,1,0:T(8,128)(2,1)S(1)} all-to-all(bf16[16,2,32,128]{3,2,1,0:T(8,128)(2,1)S(1)} %shard_map.186), channel_id=1, replica_groups={{320,352,256,288,448,480,384,416,64,96,0,32,192,224,128,160},{321,353,2..., dimensions={0} | all-to-all | bytes 524288 | tf_op jit(solution)/shard_map/all_to_all | solution.py:39
  67.1 0.3 shard_map.187
  67.5 0.0 copy-start.1
  67.5 0.0 copy-start.2
  67.5 15.2 %all_to_all.39.got_ref = bf16[16,2,1408]{2,1,0:T(2,128)(2,1)S(1)} all-to-all(bf16[16,2,1408]{2,1,0:T(2,128)(2,1)S(1)} %reshape.42), channel_id=1, replica_groups={{16,18,20,22,24,26,28,30,0,2,4,6,8,10,12,14},{17,19,21,23,25,27,29,31,1..., dimensions={0} | all-to-all | bytes 180224 | tf_op jit(solution)/shard_map/all_to_all | solution.py:29
  82.8 0.0 copy-done.1
  82.8 0.0 copy-done.2
  82.8 1.4 %scan_last.1 = (bf16[16,2,512]{2,1,0:T(2,128)(2,1)S(1)}, f32[2,2,8,64,128]{4,3,2,1,0:T(8,128)}, bf16[2,2,4,512]{3,2,1,0:T(4,128)(2,1)}, bf16[2,2,4,2,128]{4,3,2,1,0:T(2,128)(2,1)}) custom-call(bf16[16,2,1408]{2,1,0:T(2,128)(2,1)S(1)} %all_to_all.39.got_ref, f32[2,8,512]{2,1,0:T(8,128)S(1)} %get-tuple-element.19.par_ref, f32[2,2,8,64,128]{4,3,2,1,0:T(8,128)S(1)} %copy-done, ...), custom_call_target="tpu_custom_call" | custom-call | flops 10000000 | bytes 1000000 | tf_op jit(solution)/shard_map/scan_last/pallas_call | solution.py:471
  84.2 13.7 %all_to_all.40 = bf16[16,2,512]{2,1,0:T(2,128)(2,1)S(1)} all-to-all(bf16[16,2,512]{2,1,0:T(2,128)(2,1)S(1)} %get-tuple-element.25), channel_id=1, replica_groups={{16,18,20,22,24,26,28,30,0,2,4,6,8,10,12,14},{17,19,21,23,25,27,29,31,1..., dimensions={0} | all-to-all | bytes 65536 | tf_op jit(solution)/shard_map/all_to_all | solution.py:29
  97.9 0.1 shard_map.188
  98.1 0.1 pad_maximum_fusion
  98.1 15.0 %all_to_all.41 = bf16[32,4,128]{2,1,0:T(4,128)(2,1)S(1)} all-to-all(bf16[32,4,128]{2,1,0:T(4,128)(2,1)S(1)} %pad_maximum_fusion), channel_id=1, replica_groups={{321,353,257,289,449,481,385,417,65,97,1,33,193,225,129,161,320,352,256..., dimensions={0} | all-to-all | bytes 65536 | tf_op jit(solution)/shard_map/all_to_all | solution.py:39
  113.2 0.6 rev.5
  (7 shorter events, 0.2 us)
Async XLA Ops:
  0.6 41.2 %copy-start = (f32[2,2,8,64,128]{4,3,2,1,0:T(8,128)S(1)}, f32[2,2,8,64,128]{4,3,2,1,0:T(8,128)}, u32[]{:S(2)}) copy-start(f32[2,2,8,64,128]{4,3,2,1,0:T(8,128)} %state_ref.3) | copy-start | bytes 3145732
  2.6 19.7 %collective-permute-start = (bf16[128,1536]{1,0:T(8,128)(2,1)S(1)}, bf16[128,1536]{1,0:T(8,128)(2,1)S(1)}, u32[]{:S(2)}, u32[]{:S(2)}) collective-permute-start(bf16[128,1536]{1,0:T(8,128)(2,1)S(1)} %get-tuple-element.18.own_ref), channel_id=1, source_target_pairs={{0,1},{1,0},{2,3},{3,2},{4,5},{5,4},{6,7},{7,6},{8,9},{9,8},{10,11... | collective-permute-start | bytes 1179656 | tf_op jit(solution)/shard_map/ppermute | solution.py:45
  11.3 44.9 %collective-permute-start.1 = (bf16[128,2560]{1,0:T(8,128)(2,1)S(1)}, bf16[128,2560]{1,0:T(8,128)(2,1)S(1)}, u32[]{:S(2)}, u32[]{:S(2)}) collective-permute-start(bf16[128,2560]{1,0:T(8,128)(2,1)S(1)} %get-tuple-element.21.own_ref), channel_id=1, source_target_pairs={{0,1},{1,0},{2,3},{3,2},{4,5},{5,4},{6,7},{7,6},{8,9},{9,8},{10,11... | collective-permute-start | bytes 1966088 | tf_op jit(solution)/shard_map/ppermute | solution.py:45
  67.5 15.3 %copy-start.1 = (bf16[2,2,4,512]{3,2,1,0:T(4,128)(2,1)S(1)}, bf16[2,2,4,512]{3,2,1,0:T(4,128)(2,1)}, u32[]{:S(2)}) copy-start(bf16[2,2,4,512]{3,2,1,0:T(4,128)(2,1)} %conv_x_ref.3) | copy-start | bytes 49156
  67.5 15.2 %copy-start.2 = (bf16[2,2,4,2,128]{4,3,2,1,0:T(2,128)(2,1)S(1)}, bf16[2,2,4,2,128]{4,3,2,1,0:T(2,128)(2,1)}, u32[]{:S(2)}) copy-start(bf16[2,2,4,2,128]{4,3,2,1,0:T(2,128)(2,1)} %conv_bc_ref.3) | copy-start | bytes 24580

commit v10 on v9

--- a/solution.py
+++ b/solution.py
@@ -251,6 +251,17 @@
         out_ref[c] = out_terms(mixed_ref, w_ref, at, blocks)
 
 
+def leave(count, got_ref, out_ref):
+    half = got_ref.shape[1] // 2
+    sums = []
+    for c in range(2):
+        total = got_ref[c * count].astype(f32)
+        for p in range(1, count):
+            total = total + got_ref[c * count + p].astype(f32)
+        sums.append(total[:half] + got_ref[c * count].astype(f32)[half:])
+    out_ref[...] = jnp.concatenate([sums[1], sums[0]], axis=0).astype(bf16)
+
+
 def head_spread(values, head_dim, count):
     lane = lax.broadcasted_iota(jnp.int32, (values.shape[0], LANES), 1)
     pieces = []
@@ -508,9 +519,11 @@
                 [terms.reshape(2 * n_tp, half, cols_dev), hidden.reshape(2 * n_tp, half, cols_dev)],
                 axis=1,
             )
-            got = exchange_plane(both, CTP, plane).reshape(2, n_tp, rows_dev, cols_dev).astype(f32)
-            result = got[:, :, :half].sum(axis=1) + got[:, 0, half:]
-            result = result[::-1].astype(bf16).reshape(rows_dev, cols_dev)
+            got = exchange_plane(both, CTP, plane)
+            result = call(
+                functools.partial(leave, n_tp), shape((rows_dev, cols_dev), bf16),
+                1, 100000, 100000,
+            )(got)
     return (result, *outs)
 
 

time: 114 us -> 114 us (level)
  no operation moved by 1% of the time
where the time goes in v10:
time: 114 us
  blocking collectives  96.6 us (85%)
  starting transfers between devices  10.7 us (9%)
  Pallas kernels  5.47 us (5%)
    all_to_all x4, blocking collectives, exchange_z(): lax.all_to_all(value, 'z', split_axis=0, concat_axis=0, axis_index_groups...  61.9 us
    all_to_all x3, blocking collectives, exchange_plane(): lax.all_to_all(value, axis, split_axis=0, concat_axis=0, axis_index_group...  34.7 us
    ppermute x2, starting transfers between devices, swap_cores(): return lax.ppermute(value, 'core', [(0, 1), (1, 0)])  10.7 us
  transfers between devices with their start and end apart: 2, of which 0 were waited for; matrix products, arithmetic and copies ran while one was open for 0% of the time, Pallas kernels for 1%

profile of v10, /device:TPU:1, one launch (start us, length us, event | category | flops | bytes accessed | tf_op | source)
XLA Modules:
  0.0 113.7 jit_solution(4613080668795382939)
XLA Ops:
  0.6 0.0 copy-start
  0.6 1.9 %shard_map.183 = (bf16[32,2,128]{2,1,0:T(2,128)(2,1)S(1)}, bf16[128,1536]{1,0:T(8,128)(2,1)S(1)}, bf16[128,2560]{1,0:T(8,128)(2,1)S(1)}, f32[2,8,512]{2,1,0:T(8,128)S(1)}) custom-call(bf16[4,128]{1,0:T(4,128)(2,1)} %stream_ref.1, bf16[2,128,512]{2,1,0:T(8,128)(2,1)} %x_ref.1, bf16[2,128,512]{2,1,0:T(8,128)(2,1)} %z_ref.1, bf16[2,128,128]{2,1,0:T(8,128)(2,1)} %step_ref.1, ...), custom_call_target="tpu_custom_call" | custom-call | flops 1000000 | bytes 1000000 | tf_op jit(solution)/shard_map/pallas_call | solution.py:169
  2.6 8.7 %collective-permute-start = (bf16[128,1536]{1,0:T(8,128)(2,1)S(1)}, bf16[128,1536]{1,0:T(8,128)(2,1)S(1)}, u32[]{:S(2)}, u32[]{:S(2)}) collective-permute-start(bf16[128,1536]{1,0:T(8,128)(2,1)S(1)} %get-tuple-element.18.own_ref), channel_id=1, source_target_pairs={{0,1},{1,0},{2,3},{3,2},{4,5},{5,4},{6,7},{7,6},{8,9},{9,8},{10,11... | collective-permute-start | bytes 1179656 | tf_op jit(solution)/shard_map/ppermute | solution.py:45
  11.3 1.9 %collective-permute-start.1 = (bf16[128,2560]{1,0:T(8,128)(2,1)S(1)}, bf16[128,2560]{1,0:T(8,128)(2,1)S(1)}, u32[]{:S(2)}, u32[]{:S(2)}) collective-permute-start(bf16[128,2560]{1,0:T(8,128)(2,1)S(1)} %get-tuple-element.21.own_ref), channel_id=1, source_target_pairs={{0,1},{1,0},{2,3},{3,2},{4,5},{5,4},{6,7},{7,6},{8,9},{9,8},{10,11... | collective-permute-start | bytes 1966088 | tf_op jit(solution)/shard_map/ppermute | solution.py:45
  13.2 9.0 %all_to_all.35 = bf16[32,2,128]{2,1,0:T(2,128)(2,1)S(1)} all-to-all(bf16[32,2,128]{2,1,0:T(2,128)(2,1)S(1)} %get-tuple-element.17), channel_id=1, replica_groups={{321,353,257,289,449,481,385,417,65,97,1,33,193,225,129,161,320,352,256..., dimensions={0} | all-to-all | bytes 32768 | tf_op jit(solution)/shard_map/all_to_all | solution.py:39
  22.3 0.0 collective-permute-done.other_ref
  22.3 0.3 shard_map.184
  22.6 19.2 %all_to_all.36.got_ref = bf16[16,2,1408]{2,1,0:T(2,128)(2,1)S(1)} all-to-all(bf16[16,2,1408]{2,1,0:T(2,128)(2,1)S(1)} %reshape.34), channel_id=1, replica_groups={{16,18,20,22,24,26,28,30,0,2,4,6,8,10,12,14},{17,19,21,23,25,27,29,31,1..., dimensions={0} | all-to-all | bytes 180224 | tf_op jit(solution)/shard_map/all_to_all | solution.py:29
  41.9 0.0 copy-done
  41.9 0.6 shard_map.185
  42.5 13.7 %all_to_all.37 = bf16[16,2,512]{2,1,0:T(2,128)(2,1)S(1)} all-to-all(bf16[16,2,512]{2,1,0:T(2,128)(2,1)S(1)} %get-tuple-element.20), channel_id=1, replica_groups={{16,18,20,22,24,26,28,30,0,2,4,6,8,10,12,14},{17,19,21,23,25,27,29,31,1..., dimensions={0} | all-to-all | bytes 65536 | tf_op jit(solution)/shard_map/all_to_all | solution.py:29
  56.2 0.0 collective-permute-done.1.other_ref
  56.2 0.2 shard_map.186
  56.4 10.7 %all_to_all.38.arrived_ref = bf16[16,2,32,128]{3,2,1,0:T(8,128)(2,1)S(1)} all-to-all(bf16[16,2,32,128]{3,2,1,0:T(8,128)(2,1)S(1)} %shard_map.186), channel_id=1, replica_groups={{320,352,256,288,448,480,384,416,64,96,0,32,192,224,128,160},{321,353,2..., dimensions={0} | all-to-all | bytes 524288 | tf_op jit(solution)/shard_map/all_to_all | solution.py:39
  67.1 0.3 shard_map.187
  67.5 0.0 copy-start.1
  67.5 0.0 copy-start.2
  67.5 15.2 %all_to_all.39.got_ref = bf16[16,2,1408]{2,1,0:T(2,128)(2,1)S(1)} all-to-all(bf16[16,2,1408]{2,1,0:T(2,128)(2,1)S(1)} %reshape.36), channel_id=1, replica_groups={{16,18,20,22,24,26,28,30,0,2,4,6,8,10,12,14},{17,19,21,23,25,27,29,31,1..., dimensions={0} | all-to-all | bytes 180224 | tf_op jit(solution)/shard_map/all_to_all | solution.py:29
  82.8 0.0 copy-done.1
  82.8 0.0 copy-done.2
  82.8 1.4 %scan_last.1 = (bf16[16,2,512]{2,1,0:T(2,128)(2,1)S(1)}, f32[2,2,8,64,128]{4,3,2,1,0:T(8,128)}, bf16[2,2,4,512]{3,2,1,0:T(4,128)(2,1)}, bf16[2,2,4,2,128]{4,3,2,1,0:T(2,128)(2,1)}) custom-call(bf16[16,2,1408]{2,1,0:T(2,128)(2,1)S(1)} %all_to_all.39.got_ref, f32[2,8,512]{2,1,0:T(8,128)S(1)} %get-tuple-element.19.par_ref, f32[2,2,8,64,128]{4,3,2,1,0:T(8,128)S(1)} %copy-done, ...), custom_call_target="tpu_custom_call" | custom-call | flops 10000000 | bytes 1000000 | tf_op jit(solution)/shard_map/scan_last/pallas_call | solution.py:482
  84.2 13.7 %all_to_all.40 = bf16[16,2,512]{2,1,0:T(2,128)(2,1)S(1)} all-to-all(bf16[16,2,512]{2,1,0:T(2,128)(2,1)S(1)} %get-tuple-element.25), channel_id=1, replica_groups={{16,18,20,22,24,26,28,30,0,2,4,6,8,10,12,14},{17,19,21,23,25,27,29,31,1..., dimensions={0} | all-to-all | bytes 65536 | tf_op jit(solution)/shard_map/all_to_all | solution.py:29
  97.9 0.1 shard_map.188
  98.1 0.1 pad_maximum_fusion
  98.1 15.0 %all_to_all.41.got_ref = bf16[32,4,128]{2,1,0:T(4,128)(2,1)S(1)} all-to-all(bf16[32,4,128]{2,1,0:T(4,128)(2,1)S(1)} %pad_maximum_fusion), channel_id=1, replica_groups={{321,353,257,289,449,481,385,417,65,97,1,33,193,225,129,161,320,352,256..., dimensions={0} | all-to-all | bytes 65536 | tf_op jit(solution)/shard_map/all_to_all | solution.py:39
  113.1 0.6 shard_map.189
  (4 shorter events, 0.1 us)
Async XLA Ops:
  0.6 41.2 %copy-start = (f32[2,2,8,64,128]{4,3,2,1,0:T(8,128)S(1)}, f32[2,2,8,64,128]{4,3,2,1,0:T(8,128)}, u32[]{:S(2)}) copy-start(f32[2,2,8,64,128]{4,3,2,1,0:T(8,128)} %state_ref.3) | copy-start | bytes 3145732
  2.6 19.7 %collective-permute-start = (bf16[128,1536]{1,0:T(8,128)(2,1)S(1)}, bf16[128,1536]{1,0:T(8,128)(2,1)S(1)}, u32[]{:S(2)}, u32[]{:S(2)}) collective-permute-start(bf16[128,1536]{1,0:T(8,128)(2,1)S(1)} %get-tuple-element.18.own_ref), channel_id=1, source_target_pairs={{0,1},{1,0},{2,3},{3,2},{4,5},{5,4},{6,7},{7,6},{8,9},{9,8},{10,11... | collective-permute-start | bytes 1179656 | tf_op jit(solution)/shard_map/ppermute | solution.py:45
  11.3 44.9 %collective-permute-start.1 = (bf16[128,2560]{1,0:T(8,128)(2,1)S(1)}, bf16[128,2560]{1,0:T(8,128)(2,1)S(1)}, u32[]{:S(2)}, u32[]{:S(2)}) collective-permute-start(bf16[128,2560]{1,0:T(8,128)(2,1)S(1)} %get-tuple-element.21.own_ref), channel_id=1, source_target_pairs={{0,1},{1,0},{2,3},{3,2},{4,5},{5,4},{6,7},{7,6},{8,9},{9,8},{10,11... | collective-permute-start | bytes 1966088 | tf_op jit(solution)/shard_map/ppermute | solution.py:45
  67.5 15.3 %copy-start.1 = (bf16[2,2,4,512]{3,2,1,0:T(4,128)(2,1)S(1)}, bf16[2,2,4,512]{3,2,1,0:T(4,128)(2,1)}, u32[]{:S(2)}) copy-start(bf16[2,2,4,512]{3,2,1,0:T(4,128)(2,1)} %conv_x_ref.3) | copy-start | bytes 49156
  67.5 15.2 %copy-start.2 = (bf16[2,2,4,2,128]{4,3,2,1,0:T(2,128)(2,1)S(1)}, bf16[2,2,4,2,128]{4,3,2,1,0:T(2,128)(2,1)}, u32[]{:S(2)}) copy-start(bf16[2,2,4,2,128]{4,3,2,1,0:T(2,128)(2,1)} %conv_bc_ref.3) | copy-start | bytes 24580
